TPU v7x, 32 devices: a whole 2x2x4 slice. The times are simulated.
32 devices in a mesh: sp: 8 (over z, y), tp: 4 (over x, core).
Axes of the slice: x: 2, y: 2, z: 4, core: 2. Of those that a mesh axis runs over, the one named last changes fastest.
Arguments:
- block_input: bfloat16 [8192, 2048], P('sp'), may hold values from -6 to 6
- out_grad: bfloat16 [8192, 2048], P('sp'), may hold values from -6 to 6
- w_value: bfloat16 [2048, 1024], P(None, 'tp'), may hold values from -0.125 to 0.125
- w_gate: bfloat16 [2048, 1024], P(None, 'tp'), may hold values from -0.125 to 0.125
- conv_taps: float32 [31, 1024], P(None, 'tp'), may hold values from -4 to 4
- norm_gain: float32 [1024], P('tp'), may hold values from 0.1 to 1.9
- norm_shift: float32 [1024], P('tp'), may hold values from -3 to 3
- w_proj: bfloat16 [1024, 2048], P('tp'), may hold values from -0.1875 to 0.1875
Outputs:
- input_grad: bfloat16 [8192, 2048], P('sp', 'tp')
- value_wgrad: float32 [2048, 1024], P('sp', 'tp')
- gate_wgrad: float32 [2048, 1024], P('sp', 'tp')
- proj_wgrad: float32 [1024, 2048], P('tp', 'sp')
- taps_grad: float32 [31, 1024], P(None, 'tp')
- gain_grad: float32 [1024], P('tp')
- shift_grad: float32 [1024], P('tp')
All inputs are finite; a program needn't handle non-finite values.
Results may differ from a plain program's by a relative error of at most 0.014.
Values may be sent and summed in bfloat16 or wider, within the bound.
No kernel may reach another device: no remote copies, remote signals or barrier semaphores. Data moves between devices by JAX's collectives and lax.ppermute only.
A program may use at most 128 MiB of HBM per device.

v0:
```python
import functools
import math

import jax
import jax.numpy as jnp
from jax import lax
from jax.experimental import pallas as pl
from jax.experimental.pallas import tpu as pltpu
from jax.sharding import PartitionSpec as P


EPS = 0.05
HALO = 32
LANE = 128
bf16 = jnp.bfloat16
f32 = jnp.float32


VMEM_SPEC = pl.BlockSpec(memory_space=pltpu.VMEM)
SMEM_SPEC = pl.BlockSpec(memory_space=pltpu.SMEM)


def limit(mib):
    return pltpu.CompilerParams(vmem_limit_bytes=mib * 1024 * 1024)


def send(block, axis, target):
    devices = range(lax.axis_size(axis))
    route = [(i, target(i)) for i in devices if 0 <= target(i) < len(devices)]
    return lax.ppermute(block, axis, route)


def all_sum(block, axis):
    step = 1
    while step < lax.axis_size(axis):
        block = block + send(block, axis, lambda i, b=step: i ^ b)
        step *= 2
    return block


def in_hbm(block):
    return pltpu.with_memory_space_constraint(block, pltpu.HBM)


def radices(size):
    out = []
    for r in (2, 4):
        if size % r == 0 and size > 1:
            out.append(r)
            size //= r
    if size > 1:
        out.append(size)
    return out


def right_product(left, right):
    return lax.dot_general(left, right, (((1,), (1,)), ((), ())), preferred_element_type=f32)


def blocks_kernel(ids_ref, left_ref, right_ref, *refs, gives):
    rider = refs[: -gives - 1]
    outs = refs[-gives - 1 : -1]
    own = refs[-1]
    rows = left_ref.shape[0]
    width = own.shape[2]
    count = own.shape[0]
    left = left_ref[...]

    def block(i):
        start = pl.multiple_of(ids_ref[i] * width, LANE)
        return jnp.dot(left, right_ref[:, pl.ds(start, width)], preferred_element_type=f32)

    for i, out in enumerate(outs):
        for j in range(count):
            out[pl.ds(j * rows, rows), :] = block(i * count + j).astype(bf16)
        for m, extra in enumerate(rider):
            size = extra.shape[0]
            out[pl.ds(count * rows + m * size, size), :] = extra[...]
    for j in range(count):
        own[j] = block(len(outs) * count + j)


def grad_blocks(left, right, ids, n, rider):
    rows, tok = left.shape
    width = right.shape[1] // n
    count = ids[0].shape[0]
    gives = len(ids) - 1
    extra = sum(a.shape[0] for a in rider)
    if width % LANE:
        full = jnp.dot(left, right, preferred_element_type=f32).reshape(rows, n, width)
        full = full.transpose(1, 0, 2)
        outs = [jnp.take(full, some, axis=0) for some in ids]
        below = [a.reshape(-1, width) for a in rider]
        return [
            jnp.concatenate([o.astype(bf16).reshape(-1, width)] + below, axis=0) for o in outs[:-1]
        ] + outs[-1:]
    return pl.pallas_call(
        functools.partial(blocks_kernel, gives=gives),
        in_specs=[SMEM_SPEC] + [VMEM_SPEC] * (2 + len(rider)),
        out_specs=[VMEM_SPEC] * (gives + 1),
        out_shape=[jax.ShapeDtypeStruct((count * rows + extra, width), bf16)] * gives
        + [jax.ShapeDtypeStruct((count, rows, width), f32)],
        compiler_params=limit(10),
        cost_estimate=pl.CostEstimate(
            flops=2 * rows * tok * count * width * len(ids),
            transcendentals=0,
            bytes_accessed=2 * tok * (rows + count * width * len(ids)) + 4 * rows * count * width * len(ids),
        ),
        name="grad_blocks",
    )(jnp.concatenate(ids).astype(jnp.int32), left, right, *rider)


def shift(k, radix, stride):
    def target(i):
        own = (i // stride) % radix
        return i + ((own + k) % radix - own) * stride

    return target


def two_parts(block):
    high = block.astype(bf16)
    return [high, (block - high.astype(f32)).astype(bf16)]


def reduce_blocks(left, right, small=None, last_first=False):
    n = lax.axis_size("sp")
    me = lax.axis_index("sp")
    stages = []
    stride = 1
    for r in radices(n):
        stages.append((r, stride, (me // stride) % r))
        stride *= r
    if last_first:
        stages.reverse()
    base = jnp.zeros((1,), jnp.int32)
    for r, stride, _ in stages[1:]:
        base = (base[:, None] + stride * jnp.arange(r)[None]).reshape(-1)
    rest = tuple(r for r, _, _ in stages[1:])
    r, stride, digit = stages[0]
    rows = left.shape[0]
    width = right.shape[1] // n

    def ids(k):
        return base + (digit + k) % r * stride

    def whole(parts):
        return (parts[0].astype(f32) + parts[1].astype(f32)).reshape(small.shape)

    def split(message, above):
        rider = message[above:]
        half = rider.shape[0] // 2
        return message[:above], whole([rider[:half], rider[half:]])

    def total(own, got, digit, r):
        if r == 2:
            return own + got[0]
        pile = jnp.stack([own] + got)
        order = [
            lax.dynamic_index_in_dim(pile, (digit - j) % r, 0, keepdims=False) for j in range(r)
        ]
        return sum(order[1:], order[0])

    rider = [] if small is None else two_parts(small)
    *outs, own = grad_blocks(left, right, [ids(k) for k in range(1, r)] + [ids(0)], n, rider)
    got = [send(o, "sp", shift(k + 1, r, stride)) for k, o in enumerate(outs)]
    if small is not None:
        pairs = [split(g, base.shape[0] * rows) for g in got]
        got = [p[0] for p in pairs]
        small = total(whole(rider), [p[1] for p in pairs], digit, r)
    parts = [own.reshape(rest + (rows, width))] + [g.reshape(rest + (rows, width)) for g in got]
    for r, stride, digit in stages[1:]:

        def pick(k):
            return sum(
                lax.dynamic_index_in_dim(p, (digit + k) % r, 0, keepdims=False).astype(f32) for p in parts
            )

        sent = [pick(k).astype(bf16) for k in range(1, r)]
        shape = sent[0].shape
        if small is not None:
            rider = [a.reshape(-1, width) for a in two_parts(small)]
            sent = [jnp.concatenate([x.reshape(-1, width)] + rider, axis=0) for x in sent]
        got = [send(x, "sp", shift(k + 1, r, stride)) for k, x in enumerate(sent)]
        if small is not None:
            pairs = [split(g, g.shape[0] - 2 * rider[0].shape[0]) for g in got]
            got = [p[0].reshape(shape) for p in pairs]
            small = total(whole(rider), [p[1] for p in pairs], digit, r)
        parts = [pick(0)] + got
    return parts, small


def project_kernel(
    x_hbm, wv_hbm, wg_hbm, g_hbm, wp_hbm, v_out, s_out, u_out, m_out, x_buf, g_buf, wv_buf, wg_buf, wp_buf, sems
):
    count, block, _ = x_buf.shape

    def copies(at, hbm, buf):
        return [
            pltpu.make_async_copy(hbm.at[pl.ds(k * block, block), :], buf.at[k], sems.at[at, k])
            for k in range(count)
        ]

    weights = [
        pltpu.make_async_copy(hbm, buf, sems.at[2, k])
        for k, (hbm, buf) in enumerate(((wv_hbm, wv_buf), (wg_hbm, wg_buf), (wp_hbm, wp_buf)))
    ]
    inputs = copies(0, x_hbm, x_buf)
    grads = copies(1, g_hbm, g_buf)
    for copy in weights[:2] + inputs + weights[2:] + grads:
        copy.start()
    weights[0].wait()
    weights[1].wait()
    for k in range(count):
        inputs[k].wait()
        rows = pl.ds(k * block, block)
        v = jnp.dot(x_buf[k], wv_buf[...], preferred_element_type=f32).astype(bf16)
        s = jnp.dot(x_buf[k], wg_buf[...], preferred_element_type=f32).astype(bf16)
        v_out[rows, :] = v
        s_out[rows, :] = s
        u_out[rows, :] = (v.astype(f32) * jax.nn.sigmoid(s.astype(f32))).astype(bf16)
    weights[2].wait()
    for k in range(count):
        grads[k].wait()
        m_out[pl.ds(k * block, block), :] = right_product(g_buf[k], wp_buf[...])


def project(x, wv, wg, g, wp, count):
    t, d = x.shape
    c = wv.shape[1]
    hbm = pl.BlockSpec(memory_space=pl.ANY)
    return pl.pallas_call(
        project_kernel,
        in_specs=[hbm] * 5,
        out_specs=[VMEM_SPEC] * 4,
        out_shape=[jax.ShapeDtypeStruct((t, c), bf16)] * 3 + [jax.ShapeDtypeStruct((t, c), f32)],
        scratch_shapes=[
            pltpu.VMEM((count, t // count, d), bf16),
            pltpu.VMEM((count, t // count, d), bf16),
            pltpu.VMEM((d, c), bf16),
            pltpu.VMEM((d, c), bf16),
            pltpu.VMEM((c, d), bf16),
            pltpu.SemaphoreType.DMA((3, max(3, count))),
        ],
        compiler_params=limit(20),
        cost_estimate=pl.CostEstimate(
            flops=6 * t * d * c, transcendentals=t * c, bytes_accessed=2 * (2 * t * d + 3 * d * c + 5 * t * c)
        ),
        name="project",
    )(*(in_hbm(a) for a in (x, wv, wg, g, wp)))


def chunk_of(rows, most):
    return max(c for c in range(16, most + 1, 16) if rows % c == 0)


def fill_extended(ext_ref, before, glu, after, tok):
    ext_ref[pl.ds(0, HALO), :] = before.astype(f32)
    ext_ref[pl.ds(HALO, tok), :] = glu.astype(f32)
    ext_ref[pl.ds(HALO + tok, HALO), :] = after


def tap_rows(taps_ref, taps):
    return [jnp.broadcast_to(taps_ref[pl.ds(k, 1), :], (8, LANE)) for k in range(taps)]


def conv_rows(ext_ref, weights, base, chunk):
    x = ext_ref[pl.ds(base, chunk + HALO), :]
    acc = [None] * (chunk // 8)
    for r in range(8):
        moved = x if r == 0 else pltpu.roll(x, r, 0)
        for k in range(r, len(weights), 8):
            for j in range(chunk // 8):
                low = HALO + 8 * j - (k - r)
                part = weights[k] * moved[low : low + 8]
                acc[j] = part if acc[j] is None else acc[j] + part
    return acc


def conv_kernel(glu_ref, taps_ref, out_ref, wide_ref):
    tok = glu_ref.shape[0]
    rows = tok - HALO
    chunk = chunk_of(rows, 96)
    wide_ref[...] = glu_ref[...].astype(f32)
    weights = tap_rows(taps_ref, taps_ref.shape[0])

    def step(i, carry):
        base = pl.multiple_of(i * chunk, chunk)
        for j, part in enumerate(conv_rows(wide_ref, weights, base, chunk)):
            out_ref[pl.ds(base + HALO + 8 * j, 8), :] = part
        return carry

    lax.fori_loop(0, rows // chunk, step, 0)


def convolve(glu, conv_taps):
    tok, ch = glu.shape
    taps = conv_taps.shape[0]
    column = lambda i: (0, i)
    return pl.pallas_call(
        conv_kernel,
        grid=(ch // LANE,),
        in_specs=[pl.BlockSpec((tok, LANE), column), pl.BlockSpec((taps, LANE), column)],
        out_specs=pl.BlockSpec((tok + HALO, LANE), column),
        out_shape=jax.ShapeDtypeStruct((tok + HALO, ch), f32),
        scratch_shapes=[pltpu.VMEM((tok, LANE), f32)],
        compiler_params=limit(6),
        cost_estimate=pl.CostEstimate(
            flops=20 * taps * tok * ch, transcendentals=0, bytes_accessed=6 * tok * ch
        ),
        name="convolve",
    )(glu, conv_taps)


def ends_kernel(before_ref, head_ref, tail_ref, after_ref, taps_ref, main_ref, out_ref, ext_ref):
    ch = head_ref.shape[1]
    rows = main_ref.shape[0]
    for h in range(ch // LANE):
        cols = pl.ds(h * LANE, LANE)
        weights = [jnp.broadcast_to(taps_ref[pl.ds(k, 1), cols], (8, LANE)) for k in range(taps_ref.shape[0])]
        for m, (first, second) in enumerate(((before_ref, head_ref), (tail_ref, after_ref))):
            ext_ref[pl.ds(0, HALO), :] = first[:, cols].astype(f32)
            ext_ref[pl.ds(HALO, HALO), :] = second[pl.ds(0, HALO), cols].astype(f32)
            for j, part in enumerate(conv_rows(ext_ref, weights, 0, HALO)):
                out_ref[pl.ds(m * (rows - HALO) + 8 * j, 8), cols] = part


def convolve_ends(main, before, glu, after, conv_taps):
    return pl.pallas_call(
        ends_kernel,
        in_specs=[VMEM_SPEC] * 6,
        out_specs=VMEM_SPEC,
        out_shape=jax.ShapeDtypeStruct(main.shape, f32),
        input_output_aliases={5: 0},
        scratch_shapes=[pltpu.VMEM((2 * HALO, LANE), f32)],
        compiler_params=limit(4),
        cost_estimate=pl.CostEstimate(
            flops=80 * conv_taps.size * HALO, transcendentals=0, bytes_accessed=16 * HALO * main.shape[1]
        ),
        name="convolve_ends",
    )(before, glu[:HALO], glu[glu.shape[0] - HALO :], after, conv_taps, main)


def row_sums(first, second):
    pair = jnp.stack([jnp.sum(first, axis=1), jnp.sum(second, axis=1)])
    return jnp.pad(pair, ((0, 0), (0, -pair.shape[1] % LANE)))


def as_columns(rows):
    return jnp.pad(jnp.stack(rows), ((0, 8 - len(rows)), (0, 0)))


def act_kernel(
    filtered_ref, stats_ref, mixed_ref, edge_ref, gain_ref, shift_ref,
    normed_ref, grad_ref, turned_ref, sums_ref, col_ref, out_ref,
):
    ch = filtered_ref.shape[1]
    tok = mixed_ref.shape[0]
    col_ref[...] = stats_ref[...].T
    chunk = chunk_of(tok, 64)

    def some_rows(base, count, mixed, own):
        here = pl.ds(base, count)
        mean = jnp.broadcast_to(col_ref[here, pl.ds(0, 1)], (count, LANE))
        scale = jnp.broadcast_to(col_ref[here, pl.ds(1, 1)], (count, LANE))
        sums = []
        for h in range(ch // LANE):
            cols = pl.ds(h * LANE, LANE)
            normed = (filtered_ref[here, cols] - mean) * scale
            gain = gain_ref[:, cols]
            active = normed * gain + shift_ref[:, cols]
            s = jax.nn.sigmoid(active)
            act = mixed[:, h * LANE : (h + 1) * LANE] * s * (1.0 + active * (1.0 - s))
            normed_ref[here, cols] = normed
            grad_ref[here, cols] = act * gain
            if own:
                out_ref[here, cols] = (active * s).astype(bf16)
                sums.append(fold(act * normed))
                sums.append(fold(act))
        return sums

    def fold(x):
        total = x[0:8]
        for j in range(8, x.shape[0], 8):
            total = total + x[j : j + 8]
        return total

    def step(i, sums):
        base = pl.multiple_of(i * chunk, chunk)
        more = some_rows(base, chunk, mixed_ref[pl.ds(base, chunk), :], True)
        return tuple(a + b for a, b in zip(sums, more))

    zero = jnp.zeros((8, LANE), f32)
    sums = lax.fori_loop(0, tok // chunk, step, (zero,) * (2 * (ch // LANE)))
    some_rows(tok, HALO, edge_ref[...], False)
    sums_ref[...] = jnp.zeros_like(sums_ref)
    for h in range(ch // LANE):
        for m in range(2):
            sums_ref[pl.ds(m, 1), pl.ds(h * LANE, LANE)] = jnp.sum(sums[2 * h + m], axis=0, keepdims=True)
    for i in range(0, tok, LANE):
        turned_ref[:, pl.ds(i, LANE)] = out_ref[pl.ds(i, LANE), :].T


def activate(filtered, stats, mixed, after, gain, shift_row):
    rows, ch = filtered.shape
    tok = mixed.shape[0]
    wide = stats.shape[1]
    whole = lambda i: (0, 0)
    return pl.pallas_call(
        act_kernel,
        grid=(1,),
        in_specs=[
            pl.BlockSpec((rows, ch), whole),
            pl.BlockSpec((8, wide), whole),
            pl.BlockSpec((tok, ch), whole),
            pl.BlockSpec((HALO, ch), lambda i: (1, 0)),
            pl.BlockSpec((1, ch), whole),
            pl.BlockSpec((1, ch), whole),
        ],
        out_specs=[
            pl.BlockSpec((rows, ch), whole),
            pl.BlockSpec((rows, ch), whole),
            pl.BlockSpec((ch, tok), whole),
            pl.BlockSpec((16, ch), whole),
        ],
        out_shape=[
            jax.ShapeDtypeStruct((rows, ch), f32),
            jax.ShapeDtypeStruct((rows, ch), f32),
            jax.ShapeDtypeStruct((ch, tok), bf16),
            jax.ShapeDtypeStruct((16, ch), f32),
        ],
        scratch_shapes=[pltpu.VMEM((wide, 8), f32), pltpu.VMEM((tok, ch), bf16)],
        compiler_params=limit(12),
        cost_estimate=pl.CostEstimate(
            flops=200 * tok * ch, transcendentals=2 * tok * ch, bytes_accessed=18 * tok * ch
        ),
        name="activate",
    )(filtered, stats, mixed, after, gain, shift_row)


def back_conv_kernel(
    normed_ref, gn_ref, stats_ref, before_ref, glu_ref, after_ref, v_ref, s_ref, taps_ref,
    out_ref, turned_ref, small_ref, ext_ref, grad_ref, col_ref,
):
    tok = glu_ref.shape[0]
    rows = tok + HALO
    taps = taps_ref.shape[0]
    col_ref[...] = stats_ref[...].T
    fill_extended(ext_ref, before_ref[...], glu_ref[...], after_ref[...], tok)
    part_rows = chunk_of(rows, 96)

    def filtered_grad(i, carry):
        here = pl.ds(pl.multiple_of(i * part_rows, part_rows), part_rows)
        scale, first, second = (
            jnp.broadcast_to(col_ref[here, pl.ds(m, 1)], (part_rows, LANE)) for m in range(3)
        )
        grad_ref[here, :] = scale * (gn_ref[here, :] - first - normed_ref[here, :] * second)
        return carry

    lax.fori_loop(0, rows // part_rows, filtered_grad, 0)
    weights = tap_rows(taps_ref, taps)
    chunk = chunk_of(tok, 64)

    def spread(i, carry):
        base = pl.multiple_of(i * chunk, chunk)
        x = grad_ref[pl.ds(base, chunk + HALO), :]
        acc = [None] * (chunk // 8)
        for r in range(8):
            moved = x if r == 0 else pltpu.roll(x, chunk + HALO - r, 0)
            for k in range(r, taps, 8):
                for j in range(chunk // 8):
                    low = 8 * j + k - r
                    part = weights[k] * moved[low : low + 8]
                    acc[j] = part if acc[j] is None else acc[j] + part
        glu = jnp.concatenate(acc, axis=0)
        v = v_ref[pl.ds(base, chunk), :].astype(f32)
        s = jax.nn.sigmoid(s_ref[pl.ds(base, chunk), :].astype(f32))
        through = glu * s
        out_ref[pl.ds(base, chunk), pl.ds(0, LANE)] = through.astype(bf16)
        out_ref[pl.ds(base, chunk), pl.ds(LANE, LANE)] = (through * v * (1.0 - s)).astype(bf16)
        return carry

    lax.fori_loop(0, tok // chunk, spread, 0)
    for i in range(0, tok, LANE):
        turned_ref[:, pl.ds(i, LANE)] = out_ref[pl.ds(i, LANE), :].T

    width = chunk_of(tok, 32)

    def gather(i, sums):
        base = pl.multiple_of(i * width, width)
        g = grad_ref[pl.ds(base, width), :]
        x = ext_ref[pl.ds(base, width + HALO), :]
        sums = list(sums)
        for r in range(8):
            moved = x if r == 0 else pltpu.roll(x, r, 0)
            for k in range(r, taps, 8):
                for j in range(width // 8):
                    low = HALO + 8 * j - (k - r)
                    sums[k] = sums[k] + g[8 * j : 8 * j + 8] * moved[low : low + 8]
        return tuple(sums)

    zero = jnp.zeros((8, LANE), f32)
    sums = lax.fori_loop(0, tok // width, gather, (zero,) * taps)
    for k in range(taps):
        small_ref[pl.ds(k, 1), :] = jnp.sum(sums[k], axis=0, keepdims=True)
    for k in range(taps, small_ref.shape[0]):
        small_ref[pl.ds(k, 1), :] = jnp.zeros((1, LANE), f32)


def back_convolve(normed, gn, stats, before, glu, after, v, s, conv_taps, h):
    tok, _ = glu.shape
    taps = conv_taps.shape[0]
    wide = stats.shape[1]
    column = lambda i: (0, h)
    first = lambda i: (0, 0)
    kept = -(-taps // 8) * 8
    return pl.pallas_call(
        back_conv_kernel,
        grid=(1,),
        in_specs=[
            pl.BlockSpec((tok + HALO, LANE), column),
            pl.BlockSpec((tok + HALO, LANE), column),
            pl.BlockSpec((8, wide), first),
            pl.BlockSpec((HALO, LANE), column),
            pl.BlockSpec((tok, LANE), column),
            pl.BlockSpec((HALO, LANE), column),
            pl.BlockSpec((tok, LANE), column),
            pl.BlockSpec((tok, LANE), column),
            pl.BlockSpec((taps, LANE), column),
        ],
        out_specs=[
            pl.BlockSpec((tok, 2 * LANE), first),
            pl.BlockSpec((2 * LANE, tok), first),
            pl.BlockSpec((kept, LANE), first),
        ],
        out_shape=[
            jax.ShapeDtypeStruct((tok, 2 * LANE), bf16),
            jax.ShapeDtypeStruct((2 * LANE, tok), bf16),
            jax.ShapeDtypeStruct((kept, LANE), f32),
        ],
        scratch_shapes=[
            pltpu.VMEM((tok + 2 * HALO, LANE), f32),
            pltpu.VMEM((tok + HALO, LANE), f32),
            pltpu.VMEM((wide, 8), f32),
        ],
        compiler_params=limit(12),
        cost_estimate=pl.CostEstimate(
            flops=40 * taps * tok * LANE, transcendentals=0, bytes_accessed=16 * tok * LANE
        ),
        name="back_convolve",
    )(normed, gn, stats, before, glu, after, v, s, conv_taps)


def input_kernel(index_ref, *refs, halves, count, add):
    grads = refs[:halves]
    value_ref, gate_ref = refs[halves : halves + 2]
    out_ref = refs[-1]
    width = out_ref.shape[2]
    tok = out_ref.shape[1]
    block = tok // 4
    for i in range(count):
        rows = pl.ds(pl.multiple_of(index_ref[i] * width, 16), width)
        weight = []
        for h in range(halves):
            cols = pl.ds(h * LANE, LANE)
            weight += [value_ref[rows, cols], gate_ref[rows, cols]]
        weight = jnp.concatenate(weight, axis=1)
        for k in range(4):
            here = pl.ds(k * block, block)
            total = right_product(jnp.concatenate([g[here, :] for g in grads], axis=1), weight)
            if add:
                total = total + refs[halves + 2][index_ref[count + i], here, :].astype(f32)
            out_ref[i, here, :] = total.astype(bf16)


def input_blocks(grads, w_value, w_gate, blocks, n, got=None, got_block=None):
    halves = len(grads)
    t = grads[0].shape[0]
    d, c = w_value.shape
    width = d // n
    count = blocks.shape[0]
    index = blocks
    add = got is not None
    if add:
        index = jnp.concatenate([blocks, got_block])
    return pl.pallas_call(
        functools.partial(input_kernel, halves=halves, count=count, add=add),
        in_specs=[SMEM_SPEC] + [VMEM_SPEC] * (halves + 2 + add),
        out_specs=VMEM_SPEC,
        out_shape=jax.ShapeDtypeStruct((count, t, width), bf16),
        compiler_params=limit(16),
        cost_estimate=pl.CostEstimate(
            flops=4 * t * c * count * width,
            transcendentals=0,
            bytes_accessed=2 * (2 * t * c + 2 * count * width * c + count * t * width),
        ),
        name="input_blocks",
    )(index.astype(jnp.int32), *grads, w_value, w_gate, *([got] if add else []))


def input_gradient(grads, w_value, w_gate):
    n = lax.axis_size("tp")
    me = lax.axis_index("tp")
    half = n // 2
    high = jnp.arange(half)
    out = input_blocks(grads, w_value, w_gate, 2 * high + (me % 2 ^ 1), n)
    got = send(out, "tp", lambda i: i ^ 1)
    own = (me // 2).reshape(1)
    parts = []
    for k in range(1, half):
        other = (me // 2 ^ k).reshape(1)
        part = input_blocks(grads, w_value, w_gate, 2 * other + me % 2, n, got, other)
        parts.append(send(part, "tp", lambda i, k=k: i ^ (2 * k)))
    total = input_blocks(grads, w_value, w_gate, 2 * own + me % 2, n, got, own)[0].astype(f32)
    for part in parts:
        total = total + part[0].astype(f32)
    return total.astype(bf16)


def last_kernel(*refs, halves, pieces, scale):
    value_ref, gate_ref = refs[-2:]
    for h in range(halves):
        total = refs[h * pieces][...]
        for p in range(1, pieces):
            total = total + refs[h * pieces + p][...].astype(f32)
        total = total * scale
        cols = pl.ds(h * LANE, LANE)
        value_ref[:, cols] = total[:LANE].T
        gate_ref[:, cols] = total[LANE:].T


def last_sums(sums, scale):
    halves = len(sums)
    width = sums[0][0].shape[1]
    ch = halves * LANE
    if width % LANE:
        totals = [sum(p.astype(f32) for p in pieces) * scale for pieces in sums]
        return tuple(
            jnp.concatenate([t[m * LANE : (m + 1) * LANE] for t in totals], axis=0).T for m in range(2)
        )
    return pl.pallas_call(
        functools.partial(last_kernel, halves=halves, pieces=len(sums[0]), scale=scale),
        out_shape=[jax.ShapeDtypeStruct((width, ch), f32)] * 2,
        compiler_params=limit(10),
        name="last_sums",
    )(*(p for pieces in sums for p in pieces))


def work(block_input, out_grad, w_value, w_gate, conv_taps, norm_gain, norm_shift, w_proj):
    tok, _ = block_input.shape
    taps = conv_taps.shape[0]
    ch = w_value.shape[1]
    n_tp = lax.axis_size("tp")
    n_sp = lax.axis_size("sp")
    channels = ch * n_tp
    loss_scale = 1.0 / math.sqrt(tok * n_sp)
    value_proj, gate_proj, gated_input, own_mixed = project(
        block_input, w_value, w_gate, out_grad, w_proj, 4
    )
    after = send(jnp.concatenate([gated_input[:HALO].astype(f32), own_mixed[:HALO]], axis=0), "sp", lambda i: i - 1)
    before = send(gated_input[tok - HALO :], "sp", lambda i: i + 1)
    inner = convolve(gated_input, conv_taps)
    filtered = convolve_ends(inner, before, gated_input, after, conv_taps)
    stats = all_sum(row_sums(filtered, filtered * filtered), "tp")
    row_mean = stats[0] / channels
    row_scale = lax.rsqrt(stats[1] / channels - row_mean * row_mean + EPS)
    normed, grad_normed, turned, edge_sums = activate(
        filtered, as_columns([row_mean, row_scale]), own_mixed, after, norm_gain[None], norm_shift[None]
    )
    back = all_sum(row_sums(grad_normed, grad_normed * normed), "tp") / channels
    stats = as_columns([row_scale, back[0], back[1]])
    proj_parts, _ = reduce_blocks(turned, out_grad, last_first=True)
    halves = ch // LANE
    grads = []
    sums = []
    small = []
    for h in range(halves):
        grad, turn, tap_sums = back_convolve(
            normed, grad_normed, stats, before, gated_input, after, value_proj, gate_proj, conv_taps, h
        )
        grads.append(grad)
        small.append(tap_sums)
        rider = None
        if h == halves - 1:
            rider = jnp.concatenate([jnp.concatenate(small, axis=1), edge_sums], axis=0)
        parts, small_sum = reduce_blocks(turn, block_input, rider)
        sums.append(parts)
    kept = small[0].shape[0]
    input_grad = input_gradient(grads, w_value, w_gate)
    proj_wgrad = sum(p.astype(f32) for p in proj_parts) * loss_scale
    value_wgrad, gate_wgrad = last_sums(sums, loss_scale)
    return (
        input_grad,
        value_wgrad,
        gate_wgrad,
        proj_wgrad,
        small_sum[:taps] * loss_scale,
        small_sum[kept] * loss_scale,
        small_sum[kept + 1] * loss_scale,
    )


def solution(mesh):
    return mapped(mesh)


def mapped(mesh):
    return jax.shard_map(
        work,
        mesh=mesh,
        in_specs=(
            P("sp", None),
            P("sp", None),
            P(None, "tp"),
            P(None, "tp"),
            P(None, "tp"),
            P("tp"),
            P("tp"),
            P("tp", None),
        ),
        out_specs=(
            P("sp", "tp"),
            P("sp", "tp"),
            P("sp", "tp"),
            P("tp", "sp"),
            P(None, "tp"),
            P("tp"),
            P("tp"),
        ),
        check_vma=False,
    )
```

profile of v0, /device:TPU:0, one launch (start us, length us, event | category | flops | bytes accessed | tf_op | source)
XLA Modules:
  0.0 156.0 jit_solution(10323933052666306052)
XLA Ops:
  0.6 7.7 %project.1 = (bf16[1024,256]{1,0:T(8,128)(2,1)S(1)}, bf16[1024,256]{1,0:T(8,128)(2,1)S(1)}, bf16[1024,256]{1,0:T(8,128)(2,1)S(1)}, f32[1024,256]{1,0:T(8,128)S(1)}) custom-call(bf16[1024,2048]{1,0:T(8,128)(2,1)} %right_ref.4, bf16[2048,256]{1,0:T(8,128)(2,1)} %refs_2_.5, bf16[2048,256]{1,0:T(8,128)(2,1)} %refs_3_.5, bf16[1024,2048]{1,0:T(8,128)(2,1)} %right_ref.5, ...), custom_call_target="tpu_custom_call" | custom-call | flops 3221225472 | bytes 14155776 | tf_op jit(solution)/shard_map/project/pallas_call | solution.py:232
  8.4 0.8 copy-done.13
  10.0 1.0 copy-done.18
  11.0 1.3 collective-permute-start.1
  12.3 5.5 %collective-permute-start = (bf16[32,256]{1,0:T(8,128)(2,1)S(1)}, bf16[32,256]{1,0:T(8,128)(2,1)S(1)}, u32[]{:S(2)}, u32[]{:S(2)}) collective-permute-start(bf16[32,256]{1,0:T(8,128)(2,1)S(1)} %get-tuple-element.74.tail_ref), channel_id=1, source_target_pairs={{0,4},{4,8},{8,12},{12,16},{16,20},{20,24},{24,28},{1,5},{5,9},{9,... | collective-permute-start | bytes 49160 | tf_op jit(solution)/shard_map/ppermute | solution.py:30
  17.9 4.0 %convolve.1.main_ref = f32[1056,256]{1,0:T(8,128)S(1)} custom-call(bf16[1024,256]{1,0:T(8,128)(2,1)S(1)} %get-tuple-element.31.glu_ref, f32[31,256]{1,0:T(8,128)S(1)} %copy-done.22), custom_call_target="tpu_custom_call" | custom-call | flops 162529280 | bytes 1572864 | tf_op jit(solution)/shard_map/convolve/pallas_call | solution.py:300
  22.7 1.1 collective-permute-done.2
  23.9 2.1 %collective-permute-start.3 = (f32[2,1152]{1,0:T(2,128)S(1)}, f32[2,1152]{1,0:T(2,128)S(1)}, u32[]{:S(2)}, u32[]{:S(2)}) collective-permute-start(f32[2,1152]{1,0:T(2,128)S(1)} %fusion.19), channel_id=1, source_target_pairs={{0,2},{1,3},{2,0},{3,1},{4,6},{5,7},{6,4},{7,5},{8,10},{9,11},{10,... | collective-permute-start | bytes 27656 | tf_op jit(solution)/shard_map/ppermute | solution.py:30
  25.9 1.7 %collective-permute-done.3 = f32[2,1152]{1,0:T(2,128)S(1)} collective-permute-done((f32[2,1152]{1,0:T(2,128)S(1)}, f32[2,1152]{1,0:T(2,128)S(1)}, u32[]{:S(2)}, u32[]{:S(2)}) %collective-permute-start.3) | collective-permute-done | bytes 9248 | tf_op jit(solution)/shard_map/ppermute | solution.py:30
  27.7 1.2 copy-done.19
  28.9 2.4 %activate.1 = (f32[1056,256]{1,0:T(8,128)S(1)}, f32[1056,256]{1,0:T(8,128)S(1)}, bf16[256,1024]{1,0:T(8,128)(2,1)S(1)}, f32[16,256]{1,0:T(8,128)S(1)}) custom-call(f32[1056,256]{1,0:T(8,128)S(1)} %convolve_ends.1.filtered_ref, f32[8,1152]{1,0:T(8,128)S(1)} %select_maximum_fusion.1.stats_ref, f32[1024,256]{1,0:T(8,128)S(1)} %copy-done.19, ...), custom_call_target="tpu_custom_call" | custom-call | flops 52428800 | bytes 4718592 | tf_op jit(solution)/shard_map/activate/pallas_call | solution.py:409
  32.7 1.1 collective-permute-done.4
  33.8 2.1 %collective-permute-start.5 = (f32[2,1152]{1,0:T(2,128)S(1)}, f32[2,1152]{1,0:T(2,128)S(1)}, u32[]{:S(2)}, u32[]{:S(2)}) collective-permute-start(f32[2,1152]{1,0:T(2,128)S(1)} %fusion.20), channel_id=1, source_target_pairs={{0,2},{1,3},{2,0},{3,1},{4,6},{5,7},{6,4},{7,5},{8,10},{9,11},{10,... | collective-permute-start | bytes 27656 | tf_op jit(solution)/shard_map/ppermute | solution.py:30
  35.9 1.7 %collective-permute-done.5 = f32[2,1152]{1,0:T(2,128)S(1)} collective-permute-done((f32[2,1152]{1,0:T(2,128)S(1)}, f32[2,1152]{1,0:T(2,128)S(1)}, u32[]{:S(2)}, u32[]{:S(2)}) %collective-permute-start.5) | collective-permute-done | bytes 9248 | tf_op jit(solution)/shard_map/ppermute | solution.py:30
  37.6 1.0 copy-done.17
  38.6 5.5 %back_convolve.3 = (bf16[1024,256]{1,0:T(8,128)(2,1)S(1)}, bf16[256,1024]{1,0:T(8,128)(2,1)S(1)}, f32[32,128]{1,0:T(8,128)S(1)}) custom-call(f32[1056,256]{1,0:T(8,128)S(1)} %get-tuple-element.33.normed_ref, f32[1056,256]{1,0:T(8,128)S(1)} %get-tuple-element.34.gn_ref, f32[8,1152]{1,0:T(8,128)S(1)} %select_maximum_fusion.stats_ref, ...), custom_call_target="tpu_custom_call" | custom-call | flops 162529280 | bytes 2097152 | tf_op jit(solution)/shard_map/back_convolve/pallas_call | solution.py:517
  45.0 5.5 %back_convolve.2 = (bf16[1024,256]{1,0:T(8,128)(2,1)S(1)}, bf16[256,1024]{1,0:T(8,128)(2,1)S(1)}, f32[32,128]{1,0:T(8,128)S(1)}) custom-call(f32[1056,256]{1,0:T(8,128)S(1)} %get-tuple-element.33.normed_ref, f32[1056,256]{1,0:T(8,128)S(1)} %get-tuple-element.34.gn_ref, f32[8,1152]{1,0:T(8,128)S(1)} %select_maximum_fusion.stats_ref, ...), custom_call_target="tpu_custom_call" | custom-call | flops 162529280 | bytes 2097152 | tf_op jit(solution)/shard_map/back_convolve/pallas_call | solution.py:517
  50.6 0.8 copy-done.23
  51.4 3.3 %input_blocks.3 = bf16[2,1024,512]{2,1,0:T(8,128)(2,1)} custom-call(s32[2]{0:T(128)S(1)} %multiply_add_fusion.index_ref, bf16[1024,256]{1,0:T(8,128)(2,1)S(1)} %get-tuple-element.37.refs_0_, bf16[1024,256]{1,0:T(8,128)(2,1)S(1)} %get-tuple-element.38.refs_1_, bf16[2048,256]{1,0:T(8,128)(2,1)S(1)} %copy-done.2, bf16[2048,256]{1,0:T(8,128)(2,1)S(1)} %copy-done.3), custom_call_target="tpu_custom_call" | custom-call | flops 1073741824 | bytes 4194304 | tf_op jit(solution)/shard_map/input_blocks/pallas_call | solution.py:586
  54.8 2.2 %copy-done = bf16[1024,2048]{1,0:T(8,128)(2,1)S(1)} copy-done((bf16[1024,2048]{1,0:T(8,128)(2,1)S(1)}, bf16[1024,2048]{1,0:T(8,128)(2,1)}, u32[]{:S(2)}) %copy-start) | copy-done | bytes 4194328
  56.9 1.0 copy-done.28
  58.0 2.5 %grad_blocks.4 = (bf16[1120,256]{1,0:T(8,128)(2,1)}, f32[4,256,256]{2,1,0:T(8,128)S(1)}) custom-call(s32[8]{0:T(128)S(1)} %pad_add_fusion.2.ids_ref, bf16[256,1024]{1,0:T(8,128)(2,1)S(1)} %copy-done.28, bf16[1024,2048]{1,0:T(8,128)(2,1)S(1)} %copy-done, bf16[48,256]{1,0:T(8,128)(2,1)S(1)} %get-tuple-element.63.refs_0_, ...), custom_call_target="tpu_custom_call" | custom-call | flops 1073741824 | bytes 6815744 | tf_op jit(solution)/shard_map/grad_blocks/pallas_call | solution.py:97
  60.5 1.0 copy-done.20
  61.5 2.9 %collective-permute-start.12 = (bf16[1120,256]{1,0:T(8,128)(2,1)}, bf16[1120,256]{1,0:T(8,128)(2,1)}, u32[]{:S(2)}, u32[]{:S(2)}) collective-permute-start(bf16[1120,256]{1,0:T(8,128)(2,1)} %get-tuple-element.47), channel_id=1, source_target_pairs={{0,4},{4,0},{8,12},{12,8},{16,20},{20,16},{24,28},{28,24},{1,5},{5... | collective-permute-start | bytes 1720328 | tf_op jit(solution)/shard_map/ppermute | solution.py:30
  64.5 2.2 %copy-done.12 = bf16[1024,2048]{1,0:T(8,128)(2,1)S(1)} copy-done((bf16[1024,2048]{1,0:T(8,128)(2,1)S(1)}, bf16[1024,2048]{1,0:T(8,128)(2,1)}, u32[]{:S(2)}) %copy-start.12) | copy-done | bytes 4194328
  66.7 1.0 copy-done.26
  67.7 2.4 %grad_blocks.5 = (bf16[512,256]{1,0:T(8,128)(2,1)}, bf16[512,256]{1,0:T(8,128)(2,1)}, bf16[512,256]{1,0:T(8,128)(2,1)S(1)}, f32[2,256,256]{2,1,0:T(8,128)S(1)}) custom-call(s32[8]{0:T(128)S(1)} %pad_add_fusion.3.ids_ref, bf16[256,1024]{1,0:T(8,128)(2,1)S(1)} %copy-done.26, bf16[1024,2048]{1,0:T(8,128)(2,1)S(1)} %copy-done.12), custom_call_target="tpu_custom_call" | custom-call | flops 1073741824 | bytes 6815744 | tf_op jit(solution)/shard_map/grad_blocks/pallas_call | solution.py:97
  70.9 1.6 %collective-permute-start.16 = (bf16[512,256]{1,0:T(8,128)(2,1)}, bf16[512,256]{1,0:T(8,128)(2,1)}, u32[]{:S(2)}, u32[]{:S(2)}) collective-permute-start(bf16[512,256]{1,0:T(8,128)(2,1)} %get-tuple-element.52), channel_id=1, source_target_pairs={{0,8},{4,12},{8,16},{12,20},{16,24},{20,28},{24,0},{28,4},{1,9},{5... | collective-permute-start | bytes 786440 | tf_op jit(solution)/shard_map/ppermute | solution.py:30
  72.5 1.0 collective-permute-start.17
  73.5 2.9 %collective-permute-start.18 = (bf16[512,256]{1,0:T(8,128)(2,1)S(1)}, bf16[512,256]{1,0:T(8,128)(2,1)}, u32[]{:S(2)}, u32[]{:S(2)}) collective-permute-start(bf16[512,256]{1,0:T(8,128)(2,1)S(1)} %get-tuple-element.54), channel_id=1, source_target_pairs={{0,24},{4,28},{8,0},{12,4},{16,8},{20,12},{24,16},{28,20},{1,25},{... | collective-permute-start | bytes 786440 | tf_op jit(solution)/shard_map/ppermute | solution.py:30
  76.6 2.2 %copy-done.1 = bf16[1024,2048]{1,0:T(8,128)(2,1)S(1)} copy-done((bf16[1024,2048]{1,0:T(8,128)(2,1)S(1)}, bf16[1024,2048]{1,0:T(8,128)(2,1)}, u32[]{:S(2)}) %copy-start.1) | copy-done | bytes 4194328
  78.8 1.0 copy-done.24
  79.8 1.8 %grad_blocks.3 = (bf16[1024,256]{1,0:T(8,128)(2,1)S(1)}, f32[4,256,256]{2,1,0:T(8,128)S(1)}) custom-call(s32[8]{0:T(128)S(1)} %pad_add_fusion.2.ids_ref, bf16[256,1024]{1,0:T(8,128)(2,1)S(1)} %copy-done.24, bf16[1024,2048]{1,0:T(8,128)(2,1)S(1)} %copy-done.1), custom_call_target="tpu_custom_call" | custom-call | flops 1073741824 | bytes 6815744 | tf_op jit(solution)/shard_map/grad_blocks/pallas_call | solution.py:97
  82.3 10.5 %collective-permute-done.17 = bf16[512,256]{1,0:T(8,128)(2,1)} collective-permute-done((bf16[512,256]{1,0:T(8,128)(2,1)}, bf16[512,256]{1,0:T(8,128)(2,1)}, u32[]{:S(2)}, u32[]{:S(2)}) %collective-permute-start.17) | collective-permute-done | bytes 262176 | tf_op jit(solution)/shard_map/ppermute | solution.py:30
  92.8 1.1 fusion.8
  95.0 1.1 slice.102
  96.3 7.3 %collective-permute-start.15 = (bf16[352,256]{1,0:T(8,128)(2,1)S(1)}, bf16[352,256]{1,0:T(8,128)(2,1)S(1)}, u32[]{:S(2)}, u32[]{:S(2)}) collective-permute-start(bf16[352,256]{1,0:T(8,128)(2,1)S(1)} %get-tuple-element.77), channel_id=1, source_target_pairs={{0,24},{4,28},{8,0},{12,4},{16,8},{20,12},{24,16},{28,20},{1,25},{... | collective-permute-start | bytes 540680 | tf_op jit(solution)/shard_map/ppermute | solution.py:30
  103.6 1.8 %fusion.1 = f32[256,256]{1,0:T(8,128)} fusion(bf16[256,256]{1,0:T(8,128)(2,1)S(1)} %collective-permute-done.19, f32[2,256,256]{2,1,0:T(8,128)S(1)} %copy-done.30, s32[]{:T(128)S(6)} %select_n.196, bf16[2,256,256]{2,1,0:T(8,128)(2,1)} %bitcast.18, bf16[2,256,256]{2,1,0:T(8,128)(2,1)} %bitcast.17, bf16[2,256,256]{2,1,0:T(8,128)(2,1)} %bitcast.16), kind=kLoop, calls=%fused_computation.11 | loop fusion | flops 589824 | bytes 1048580 | tf_op jit(solution)/shard_map/mul | solution.py:690
  105.6 2.7 %collective-permute-start.10 = (bf16[256,256]{1,0:T(8,128)(2,1)S(1)}, bf16[256,256]{1,0:T(8,128)(2,1)S(1)}, u32[]{:S(2)}, u32[]{:S(2)}) collective-permute-start(bf16[256,256]{1,0:T(8,128)(2,1)S(1)} %get-tuple-element.69), channel_id=1, source_target_pairs={{0,16},{4,20},{8,24},{12,28},{16,0},{20,4},{24,8},{28,12},{1,17},{... | collective-permute-start | bytes 393224 | tf_op jit(solution)/shard_map/ppermute | solution.py:30
  108.2 1.7 %collective-permute-start.11 = (bf16[256,256]{1,0:T(8,128)(2,1)S(1)}, bf16[256,256]{1,0:T(8,128)(2,1)S(1)}, u32[]{:S(2)}, u32[]{:S(2)}) collective-permute-start(bf16[256,256]{1,0:T(8,128)(2,1)S(1)} %get-tuple-element.68), channel_id=1, source_target_pairs={{0,24},{4,28},{8,0},{12,4},{16,8},{20,12},{24,16},{28,20},{1,25},{... | collective-permute-start | bytes 393224 | tf_op jit(solution)/shard_map/ppermute | solution.py:30
  110.6 3.8 %collective-permute-start.13 = (bf16[352,256]{1,0:T(8,128)(2,1)S(1)}, bf16[352,256]{1,0:T(8,128)(2,1)S(1)}, u32[]{:S(2)}, u32[]{:S(2)}) collective-permute-start(bf16[352,256]{1,0:T(8,128)(2,1)S(1)} %get-tuple-element.79), channel_id=1, source_target_pairs={{0,8},{4,12},{8,16},{12,20},{16,24},{20,28},{24,0},{28,4},{1,9},{5... | collective-permute-start | bytes 540680 | tf_op jit(solution)/shard_map/ppermute | solution.py:30
  114.4 1.3 input_blocks.5
  115.7 15.4 %collective-permute-done.14 = bf16[352,256]{1,0:T(8,128)(2,1)S(1)} collective-permute-done((bf16[352,256]{1,0:T(8,128)(2,1)S(1)}, bf16[352,256]{1,0:T(8,128)(2,1)S(1)}, u32[]{:S(2)}, u32[]{:S(2)}) %collective-permute-start.14) | collective-permute-done | bytes 180256 | tf_op jit(solution)/shard_map/ppermute | solution.py:30
  131.0 1.5 collective-permute-start.7
  132.6 1.0 last_sums.1
  134.9 1.3 input_blocks.4
  136.2 18.5 %collective-permute-done.7 = bf16[1,1024,512]{2,1,0:T(8,128)(2,1)S(1)} collective-permute-done((bf16[1,1024,512]{2,1,0:T(8,128)(2,1)S(1)}, bf16[1,1024,512]{2,1,0:T(8,128)(2,1)S(1)}, u32[]{:S(2)}, u32[]{:S(2)}) %collective-permute-start.7) | collective-permute-done | bytes 1048608 | tf_op jit(solution)/shard_map/ppermute | solution.py:30
  154.7 1.3 fusion
  (117 shorter events, 9.0 us)
Async XLA Ops:
  0.6 17.3 %copy-start.22 = (f32[31,256]{1,0:T(8,128)S(1)}, f32[31,256]{1,0:T(8,128)}, u32[]{:S(2)}) copy-start(f32[31,256]{1,0:T(8,128)} %taps_ref.7) | copy-start | bytes 95236
  10.0 12.1 %copy-start.5 = (bf16[1024,256]{1,0:T(8,128)(2,1)}, bf16[1024,256]{1,0:T(8,128)(2,1)S(1)}, u32[]{:S(2)}) copy-start(bf16[1024,256]{1,0:T(8,128)(2,1)S(1)} %get-tuple-element.31.glu_ref) | copy-start | bytes 1572868
  10.0 1.0 copy-start.18
  11.0 10.9 %collective-permute-start.1 = (f32[64,256]{1,0:T(8,128)S(1)}, f32[64,256]{1,0:T(8,128)S(1)}, u32[]{:S(2)}, u32[]{:S(2)}) collective-permute-start(f32[64,256]{1,0:T(8,128)S(1)} %pad_maximum_fusion.7), channel_id=1, source_target_pairs={{4,0},{8,4},{12,8},{16,12},{20,16},{24,20},{28,24},{5,1},{9,5},{13... | collective-permute-start | bytes 196616 | tf_op jit(solution)/shard_map/ppermute | solution.py:30
  12.3 9.6 %collective-permute-start = (bf16[32,256]{1,0:T(8,128)(2,1)S(1)}, bf16[32,256]{1,0:T(8,128)(2,1)S(1)}, u32[]{:S(2)}, u32[]{:S(2)}) collective-permute-start(bf16[32,256]{1,0:T(8,128)(2,1)S(1)} %get-tuple-element.74.tail_ref), channel_id=1, source_target_pairs={{0,4},{4,8},{8,12},{12,16},{16,20},{20,24},{24,28},{1,5},{5,9},{9,... | collective-permute-start | bytes 49160 | tf_op jit(solution)/shard_map/ppermute | solution.py:30
  22.2 5.5 %copy-start.31 = (f32[256]{0:T(256)S(1)}, f32[256]{0:T(256)}, u32[]{:S(2)}) copy-start(f32[256]{0:T(256)} %param.13) | copy-start | bytes 3076
  22.2 5.5 %copy-start.32 = (f32[256]{0:T(256)S(1)}, f32[256]{0:T(256)}, u32[]{:S(2)}) copy-start(f32[256]{0:T(256)} %param.14) | copy-start | bytes 3076
  22.6 1.2 collective-permute-start.2
  23.9 3.7 %collective-permute-start.3 = (f32[2,1152]{1,0:T(2,128)S(1)}, f32[2,1152]{1,0:T(2,128)S(1)}, u32[]{:S(2)}, u32[]{:S(2)}) collective-permute-start(f32[2,1152]{1,0:T(2,128)S(1)} %fusion.19), channel_id=1, source_target_pairs={{0,2},{1,3},{2,0},{3,1},{4,6},{5,7},{6,4},{7,5},{8,10},{9,11},{10,... | collective-permute-start | bytes 27656 | tf_op jit(solution)/shard_map/ppermute | solution.py:30
  27.7 1.2 copy-start.19
  32.1 5.5 %copy-start.6 = (bf16[1024,256]{1,0:T(8,128)(2,1)S(1)}, bf16[1024,256]{1,0:T(8,128)(2,1)}, u32[]{:S(2)}) copy-start(bf16[1024,256]{1,0:T(8,128)(2,1)} %copy-done.5) | copy-start | bytes 1572868
  32.1 5.5 %copy-start.14 = (bf16[1024,256]{1,0:T(8,128)(2,1)S(1)}, bf16[1024,256]{1,0:T(8,128)(2,1)}, u32[]{:S(2)}) copy-start(bf16[1024,256]{1,0:T(8,128)(2,1)} %copy-done.13) | copy-start | bytes 1572868
  32.6 1.2 collective-permute-start.4
  33.8 3.7 %collective-permute-start.5 = (f32[2,1152]{1,0:T(2,128)S(1)}, f32[2,1152]{1,0:T(2,128)S(1)}, u32[]{:S(2)}, u32[]{:S(2)}) collective-permute-start(f32[2,1152]{1,0:T(2,128)S(1)} %fusion.20), channel_id=1, source_target_pairs={{0,2},{1,3},{2,0},{3,1},{4,6},{5,7},{6,4},{7,5},{8,10},{9,11},{10,... | collective-permute-start | bytes 27656 | tf_op jit(solution)/shard_map/ppermute | solution.py:30
  37.6 1.0 copy-start.17
  38.6 6.3 %copy-start.7 = (bf16[1024,256]{1,0:T(8,128)(2,1)S(1)}, bf16[1024,256]{1,0:T(8,128)(2,1)}, u32[]{:S(2)}) copy-start(bf16[1024,256]{1,0:T(8,128)(2,1)} %copy-done.5) | copy-start | bytes 1572868
  38.6 6.3 %copy-start.15 = (bf16[1024,256]{1,0:T(8,128)(2,1)S(1)}, bf16[1024,256]{1,0:T(8,128)(2,1)}, u32[]{:S(2)}) copy-start(bf16[1024,256]{1,0:T(8,128)(2,1)} %copy-done.13) | copy-start | bytes 1572868
  45.0 6.4 %copy-start.8 = (bf16[1024,256]{1,0:T(8,128)(2,1)}, bf16[1024,256]{1,0:T(8,128)(2,1)S(1)}, u32[]{:S(2)}) copy-start(bf16[1024,256]{1,0:T(8,128)(2,1)S(1)} %get-tuple-element.38.refs_1_) | copy-start | bytes 1572868
  45.0 6.4 %copy-start.2 = (bf16[2048,256]{1,0:T(8,128)(2,1)S(1)}, bf16[2048,256]{1,0:T(8,128)(2,1)}, u32[]{:S(2)}) copy-start(bf16[2048,256]{1,0:T(8,128)(2,1)} %refs_2_.5) | copy-start | bytes 3145732
  45.0 6.4 %copy-start.3 = (bf16[2048,256]{1,0:T(8,128)(2,1)S(1)}, bf16[2048,256]{1,0:T(8,128)(2,1)}, u32[]{:S(2)}) copy-start(bf16[2048,256]{1,0:T(8,128)(2,1)} %refs_3_.5) | copy-start | bytes 3145732
  50.6 0.8 copy-start.23
  51.4 3.3 %copy-start.10 = (bf16[1024,256]{1,0:T(8,128)(2,1)}, bf16[1024,256]{1,0:T(8,128)(2,1)S(1)}, u32[]{:S(2)}) copy-start(bf16[1024,256]{1,0:T(8,128)(2,1)S(1)} %get-tuple-element.37.refs_0_) | copy-start | bytes 1572868
  54.7 55.9 %collective-permute-start.6 = (bf16[2,1024,512]{2,1,0:T(8,128)(2,1)}, bf16[2,1024,512]{2,1,0:T(8,128)(2,1)S(1)}, u32[]{:S(2)}, u32[]{:S(2)}) collective-permute-start(bf16[2,1024,512]{2,1,0:T(8,128)(2,1)} %input_blocks.3), channel_id=1, source_target_pairs={{0,1},{1,0},{2,3},{3,2},{4,5},{5,4},{6,7},{7,6},{8,9},{9,8},{10,11... | collective-permute-start | bytes 6291464 | tf_op jit(solution)/shard_map/ppermute | solution.py:30
  54.8 2.2 %copy-start = (bf16[1024,2048]{1,0:T(8,128)(2,1)S(1)}, bf16[1024,2048]{1,0:T(8,128)(2,1)}, u32[]{:S(2)}) copy-start(bf16[1024,2048]{1,0:T(8,128)(2,1)} %right_ref.4) | copy-start | bytes 12582916
  56.9 1.0 copy-start.28
  60.5 1.0 copy-start.20
  61.5 32.8 %collective-permute-start.12 = (bf16[1120,256]{1,0:T(8,128)(2,1)}, bf16[1120,256]{1,0:T(8,128)(2,1)}, u32[]{:S(2)}, u32[]{:S(2)}) collective-permute-start(bf16[1120,256]{1,0:T(8,128)(2,1)} %get-tuple-element.47), channel_id=1, source_target_pairs={{0,4},{4,0},{8,12},{12,8},{16,20},{20,16},{24,28},{28,24},{1,5},{5... | collective-permute-start | bytes 1720328 | tf_op jit(solution)/shard_map/ppermute | solution.py:30
  64.5 2.2 %copy-start.12 = (bf16[1024,2048]{1,0:T(8,128)(2,1)S(1)}, bf16[1024,2048]{1,0:T(8,128)(2,1)}, u32[]{:S(2)}) copy-start(bf16[1024,2048]{1,0:T(8,128)(2,1)} %right_ref.5) | copy-start | bytes 12582916
  66.7 1.0 copy-start.26
  70.9 11.4 %collective-permute-start.16 = (bf16[512,256]{1,0:T(8,128)(2,1)}, bf16[512,256]{1,0:T(8,128)(2,1)}, u32[]{:S(2)}, u32[]{:S(2)}) collective-permute-start(bf16[512,256]{1,0:T(8,128)(2,1)} %get-tuple-element.52), channel_id=1, source_target_pairs={{0,8},{4,12},{8,16},{12,20},{16,24},{20,28},{24,0},{28,4},{1,9},{5... | collective-permute-start | bytes 786440 | tf_op jit(solution)/shard_map/ppermute | solution.py:30
  72.5 20.3 %collective-permute-start.17 = (bf16[512,256]{1,0:T(8,128)(2,1)}, bf16[512,256]{1,0:T(8,128)(2,1)}, u32[]{:S(2)}, u32[]{:S(2)}) collective-permute-start(bf16[512,256]{1,0:T(8,128)(2,1)} %get-tuple-element.53), channel_id=1, source_target_pairs={{0,16},{4,20},{8,24},{12,28},{16,0},{20,4},{24,8},{28,12},{1,17},{... | collective-permute-start | bytes 786440 | tf_op jit(solution)/shard_map/ppermute | solution.py:30
  73.5 19.3 %collective-permute-start.18 = (bf16[512,256]{1,0:T(8,128)(2,1)S(1)}, bf16[512,256]{1,0:T(8,128)(2,1)}, u32[]{:S(2)}, u32[]{:S(2)}) collective-permute-start(bf16[512,256]{1,0:T(8,128)(2,1)S(1)} %get-tuple-element.54), channel_id=1, source_target_pairs={{0,24},{4,28},{8,0},{12,4},{16,8},{20,12},{24,16},{28,20},{1,25},{... | collective-permute-start | bytes 786440 | tf_op jit(solution)/shard_map/ppermute | solution.py:30
  76.6 2.2 %copy-start.1 = (bf16[1024,2048]{1,0:T(8,128)(2,1)S(1)}, bf16[1024,2048]{1,0:T(8,128)(2,1)}, u32[]{:S(2)}) copy-start(bf16[1024,2048]{1,0:T(8,128)(2,1)} %right_ref.4) | copy-start | bytes 12582916
  78.8 1.0 copy-start.24
  79.8 13.0 %copy-start.30 = (f32[2,256,256]{2,1,0:T(8,128)S(1)}, f32[2,256,256]{2,1,0:T(8,128)}, u32[]{:S(2)}) copy-start(f32[2,256,256]{2,1,0:T(8,128)} %copy-done.29) | copy-start | bytes 1572868
  81.6 14.5 %copy-start.21 = (f32[4,256,256]{2,1,0:T(8,128)S(1)}, f32[4,256,256]{2,1,0:T(8,128)}, u32[]{:S(2)}) copy-start(f32[4,256,256]{2,1,0:T(8,128)} %copy-done.20) | copy-start | bytes 3145732
  82.3 23.1 %collective-permute-start.8 = (bf16[1024,256]{1,0:T(8,128)(2,1)S(1)}, bf16[1024,256]{1,0:T(8,128)(2,1)S(1)}, u32[]{:S(2)}, u32[]{:S(2)}) collective-permute-start(bf16[1024,256]{1,0:T(8,128)(2,1)S(1)} %get-tuple-element.41), channel_id=1, source_target_pairs={{0,4},{4,0},{8,12},{12,8},{16,20},{20,16},{24,28},{28,24},{1,5},{5... | collective-permute-start | bytes 1572872 | tf_op jit(solution)/shard_map/ppermute | solution.py:30
  93.9 9.7 %collective-permute-start.19 = (bf16[256,256]{1,0:T(8,128)(2,1)S(1)}, bf16[256,256]{1,0:T(8,128)(2,1)S(1)}, u32[]{:S(2)}, u32[]{:S(2)}) collective-permute-start(bf16[256,256]{1,0:T(8,128)(2,1)S(1)} %fusion.8), channel_id=1, source_target_pairs={{0,4},{4,0},{8,12},{12,8},{16,20},{20,16},{24,28},{28,24},{1,5},{5... | collective-permute-start | bytes 393224 | tf_op jit(solution)/shard_map/ppermute | solution.py:30
  96.3 13.9 %collective-permute-start.15 = (bf16[352,256]{1,0:T(8,128)(2,1)S(1)}, bf16[352,256]{1,0:T(8,128)(2,1)S(1)}, u32[]{:S(2)}, u32[]{:S(2)}) collective-permute-start(bf16[352,256]{1,0:T(8,128)(2,1)S(1)} %get-tuple-element.77), channel_id=1, source_target_pairs={{0,24},{4,28},{8,0},{12,4},{16,8},{20,12},{24,16},{28,20},{1,25},{... | collective-permute-start | bytes 540680 | tf_op jit(solution)/shard_map/ppermute | solution.py:30
  105.4 9.0 %copy-start.4 = (bf16[2048,256]{1,0:T(8,128)(2,1)S(1)}, bf16[2048,256]{1,0:T(8,128)(2,1)}, u32[]{:S(2)}) copy-start(bf16[2048,256]{1,0:T(8,128)(2,1)} %refs_3_.5) | copy-start | bytes 3145732
  105.4 9.0 %copy-start.9 = (bf16[1024,256]{1,0:T(8,128)(2,1)S(1)}, bf16[1024,256]{1,0:T(8,128)(2,1)}, u32[]{:S(2)}) copy-start(bf16[1024,256]{1,0:T(8,128)(2,1)} %copy-done.8) | copy-start | bytes 1572868
  105.4 8.9 %copy-start.11 = (bf16[1024,256]{1,0:T(8,128)(2,1)S(1)}, bf16[1024,256]{1,0:T(8,128)(2,1)}, u32[]{:S(2)}) copy-start(bf16[1024,256]{1,0:T(8,128)(2,1)} %copy-done.10) | copy-start | bytes 1572868
  105.6 27.0 %collective-permute-start.10 = (bf16[256,256]{1,0:T(8,128)(2,1)S(1)}, bf16[256,256]{1,0:T(8,128)(2,1)S(1)}, u32[]{:S(2)}, u32[]{:S(2)}) collective-permute-start(bf16[256,256]{1,0:T(8,128)(2,1)S(1)} %get-tuple-element.69), channel_id=1, source_target_pairs={{0,16},{4,20},{8,24},{12,28},{16,0},{20,4},{24,8},{28,12},{1,17},{... | collective-permute-start | bytes 393224 | tf_op jit(solution)/shard_map/ppermute | solution.py:30
  108.2 24.4 %collective-permute-start.11 = (bf16[256,256]{1,0:T(8,128)(2,1)S(1)}, bf16[256,256]{1,0:T(8,128)(2,1)S(1)}, u32[]{:S(2)}, u32[]{:S(2)}) collective-permute-start(bf16[256,256]{1,0:T(8,128)(2,1)S(1)} %get-tuple-element.68), channel_id=1, source_target_pairs={{0,24},{4,28},{8,0},{12,4},{16,8},{20,12},{24,16},{28,20},{1,25},{... | collective-permute-start | bytes 393224 | tf_op jit(solution)/shard_map/ppermute | solution.py:30
  109.9 22.7 %collective-permute-start.9 = (bf16[256,256]{1,0:T(8,128)(2,1)S(1)}, bf16[256,256]{1,0:T(8,128)(2,1)S(1)}, u32[]{:S(2)}, u32[]{:S(2)}) collective-permute-start(bf16[256,256]{1,0:T(8,128)(2,1)S(1)} %get-tuple-element.70), channel_id=1, source_target_pairs={{0,8},{4,12},{8,16},{12,20},{16,24},{20,28},{24,0},{28,4},{1,9},{5... | collective-permute-start | bytes 393224 | tf_op jit(solution)/shard_map/ppermute | solution.py:30
  110.3 20.8 %collective-permute-start.14 = (bf16[352,256]{1,0:T(8,128)(2,1)S(1)}, bf16[352,256]{1,0:T(8,128)(2,1)S(1)}, u32[]{:S(2)}, u32[]{:S(2)}) collective-permute-start(bf16[352,256]{1,0:T(8,128)(2,1)S(1)} %get-tuple-element.78), channel_id=1, source_target_pairs={{0,16},{4,20},{8,24},{12,28},{16,0},{20,4},{24,8},{28,12},{1,17},{... | collective-permute-start | bytes 540680 | tf_op jit(solution)/shard_map/ppermute | solution.py:30
  110.6 22.0 %collective-permute-start.13 = (bf16[352,256]{1,0:T(8,128)(2,1)S(1)}, bf16[352,256]{1,0:T(8,128)(2,1)S(1)}, u32[]{:S(2)}, u32[]{:S(2)}) collective-permute-start(bf16[352,256]{1,0:T(8,128)(2,1)S(1)} %get-tuple-element.79), channel_id=1, source_target_pairs={{0,8},{4,12},{8,16},{12,20},{16,24},{20,28},{24,0},{28,4},{1,9},{5... | collective-permute-start | bytes 540680 | tf_op jit(solution)/shard_map/ppermute | solution.py:30
  131.0 23.7 %collective-permute-start.7 = (bf16[1,1024,512]{2,1,0:T(8,128)(2,1)S(1)}, bf16[1,1024,512]{2,1,0:T(8,128)(2,1)S(1)}, u32[]{:S(2)}, u32[]{:S(2)}) collective-permute-start(bf16[1,1024,512]{2,1,0:T(8,128)(2,1)S(1)} %input_blocks.5), channel_id=1, source_target_pairs={{0,2},{1,3},{2,0},{3,1},{4,6},{5,7},{6,4},{7,5},{8,10},{9,11},{10,... | collective-permute-start | bytes 3145736 | tf_op jit(solution)/shard_map/ppermute | solution.py:30
  (5 other events, 4.0 us)
where the time goes:
time: 157 us; the launch traced here: 156 us
  waiting for transfers between devices  50.7 us (32%)
  Pallas kernels  38.9 us (25%)
  starting transfers between devices  37.3 us (24%)
  local copies, waits for them, and re-layouts  19.9 us (13%)
  other arithmetic  7.81 us (5%)
    ppermute x20, waiting for transfers between devices, send(): return lax.ppermute(block, axis, route)  50.7 us
    ppermute x20, starting transfers between devices, send(): return lax.ppermute(block, axis, route)  37.3 us
    unnamed x66, local copies, waits for them, and re-layouts  18.8 us
    pallas_call x2, Pallas kernels, back_convolve(): pl.pallas_call(back_conv_kernel, grid=(1,), in_specs=[pl.BlockSpec((tok +...  11.1 us
    pallas_call x1, Pallas kernels, project(): pl.pallas_call(project_kernel, in_specs=[hbm] * 5, out_specs=[VMEM_SPEC]...  7.74 us
    pallas_call x3, Pallas kernels, grad_blocks(): pl.pallas_call(functools.partial(blocks_kernel, gives=gives), in_specs=[S...  6.74 us
    pallas_call x3, Pallas kernels, input_blocks(): pl.pallas_call(functools.partial(input_kernel, halves=halves, count=count...  5.83 us
    pallas_call x1, Pallas kernels, convolve(): pl.pallas_call(conv_kernel, grid=(ch // LANE,), in_specs=[pl.BlockSpec((t...  3.95 us
  transfers between devices with their start and end apart: 20, of which 8 were waited for; matrix products, arithmetic and copies ran while one was open for 4% of the time, Pallas kernels for 9%

commit v1 on v0

--- a/solution.py
+++ b/solution.py
@@ -18,6 +18,7 @@
 
 VMEM_SPEC = pl.BlockSpec(memory_space=pltpu.VMEM)
 SMEM_SPEC = pl.BlockSpec(memory_space=pltpu.SMEM)
+HBM_SPEC = pl.BlockSpec(memory_space=pltpu.HBM)
 
 
 def limit(mib):
@@ -58,26 +59,29 @@
 
 
 def blocks_kernel(ids_ref, left_ref, right_ref, *refs, gives):
-    rider = refs[: -gives - 1]
-    outs = refs[-gives - 1 : -1]
-    own = refs[-1]
+    rider = refs[: -gives - 3]
+    outs = refs[-gives - 3 : -3]
+    own_hbm, own, sems = refs[-3:]
     rows = left_ref.shape[0]
-    width = own.shape[2]
-    count = own.shape[0]
+    count, _, width = own.shape
     left = left_ref[...]
 
     def block(i):
         start = pl.multiple_of(ids_ref[i] * width, LANE)
         return jnp.dot(left, right_ref[:, pl.ds(start, width)], preferred_element_type=f32)
 
+    leaving = [pltpu.make_async_copy(own.at[j], own_hbm.at[j], sems.at[j]) for j in range(count)]
+    for j in range(count):
+        own[j] = block(len(outs) * count + j)
+        leaving[j].start()
     for i, out in enumerate(outs):
         for j in range(count):
             out[pl.ds(j * rows, rows), :] = block(i * count + j).astype(bf16)
         for m, extra in enumerate(rider):
             size = extra.shape[0]
             out[pl.ds(count * rows + m * size, size), :] = extra[...]
-    for j in range(count):
-        own[j] = block(len(outs) * count + j)
+    for copy in leaving:
+        copy.wait()
 
 
 def grad_blocks(left, right, ids, n, rider):
@@ -97,9 +101,10 @@
     return pl.pallas_call(
         functools.partial(blocks_kernel, gives=gives),
         in_specs=[SMEM_SPEC] + [VMEM_SPEC] * (2 + len(rider)),
-        out_specs=[VMEM_SPEC] * (gives + 1),
+        out_specs=[VMEM_SPEC] * gives + [HBM_SPEC],
         out_shape=[jax.ShapeDtypeStruct((count * rows + extra, width), bf16)] * gives
-        + [jax.ShapeDtypeStruct((count, rows, width), f32)],
+        + [pltpu.HBM((count, rows, width), f32)],
+        scratch_shapes=[pltpu.VMEM((count, rows, width), f32), pltpu.SemaphoreType.DMA((count,))],
         compiler_params=limit(10),
         cost_estimate=pl.CostEstimate(
             flops=2 * rows * tok * count * width * len(ids),
@@ -116,11 +121,6 @@
         return i + ((own + k) % radix - own) * stride
 
     return target
-
-
-def two_parts(block):
-    high = block.astype(bf16)
-    return [high, (block - high.astype(f32)).astype(bf16)]
 
 
 def reduce_blocks(left, right, small=None, last_first=False):
@@ -144,13 +144,8 @@
     def ids(k):
         return base + (digit + k) % r * stride
 
-    def whole(parts):
-        return (parts[0].astype(f32) + parts[1].astype(f32)).reshape(small.shape)
-
     def split(message, above):
-        rider = message[above:]
-        half = rider.shape[0] // 2
-        return message[:above], whole([rider[:half], rider[half:]])
+        return message[above:].astype(f32).reshape(small.shape)
 
     def total(own, got, digit, r):
         if r == 2:
@@ -161,37 +156,36 @@
         ]
         return sum(order[1:], order[0])
 
-    rider = [] if small is None else two_parts(small)
+    rider = [] if small is None else [small.astype(bf16)]
     *outs, own = grad_blocks(left, right, [ids(k) for k in range(1, r)] + [ids(0)], n, rider)
     got = [send(o, "sp", shift(k + 1, r, stride)) for k, o in enumerate(outs)]
+    left_blocks = base.shape[0]
     if small is not None:
-        pairs = [split(g, base.shape[0] * rows) for g in got]
-        got = [p[0] for p in pairs]
-        small = total(whole(rider), [p[1] for p in pairs], digit, r)
-    parts = [own.reshape(rest + (rows, width))] + [g.reshape(rest + (rows, width)) for g in got]
+        riders = [split(g, left_blocks * rows) for g in got]
+        small = total(rider[0].astype(f32), riders, digit, r)
+    parts = [own.reshape(-1, width)] + got
     for r, stride, digit in stages[1:]:
+        left_blocks //= r
+        size = left_blocks * rows
 
         def pick(k):
-            return sum(
-                lax.dynamic_index_in_dim(p, (digit + k) % r, 0, keepdims=False).astype(f32) for p in parts
-            )
+            start = (digit + k) % r * size
+            return sum(lax.dynamic_slice_in_dim(p, start, size, 0).astype(f32) for p in parts)
 
         sent = [pick(k).astype(bf16) for k in range(1, r)]
-        shape = sent[0].shape
         if small is not None:
-            rider = [a.reshape(-1, width) for a in two_parts(small)]
-            sent = [jnp.concatenate([x.reshape(-1, width)] + rider, axis=0) for x in sent]
+            rider = small.astype(bf16)
+            below = rider.reshape(-1, width)
+            sent = [jnp.concatenate([x, below], axis=0) for x in sent]
         got = [send(x, "sp", shift(k + 1, r, stride)) for k, x in enumerate(sent)]
         if small is not None:
-            pairs = [split(g, g.shape[0] - 2 * rider[0].shape[0]) for g in got]
-            got = [p[0].reshape(shape) for p in pairs]
-            small = total(whole(rider), [p[1] for p in pairs], digit, r)
+            small = total(rider.astype(f32), [split(g, size) for g in got], digit, r)
         parts = [pick(0)] + got
-    return parts, small
+    return [p[:rows] for p in parts], small
 
 
 def project_kernel(
-    x_hbm, wv_hbm, wg_hbm, g_hbm, wp_hbm, v_out, s_out, u_out, m_out, x_buf, g_buf, wv_buf, wg_buf, wp_buf, sems
+    x_hbm, wv_hbm, wg_hbm, g_hbm, wp_hbm, v_hbm, s_hbm, u_out, m_hbm, x_buf, g_buf, wv_buf, wg_buf, wp_buf, v_out, s_out, m_out, sems
 ):
     count, block, _ = x_buf.shape
 
@@ -219,10 +213,21 @@
         v_out[rows, :] = v
         s_out[rows, :] = s
         u_out[rows, :] = (v.astype(f32) * jax.nn.sigmoid(s.astype(f32))).astype(bf16)
+    leaving = [
+        pltpu.make_async_copy(v_out, v_hbm, sems.at[3, 0]),
+        pltpu.make_async_copy(s_out, s_hbm, sems.at[3, 1]),
+    ]
+    for copy in leaving:
+        copy.start()
     weights[2].wait()
     for k in range(count):
         grads[k].wait()
-        m_out[pl.ds(k * block, block), :] = right_product(g_buf[k], wp_buf[...])
+        rows = pl.ds(k * block, block)
+        m_out[rows, :] = right_product(g_buf[k], wp_buf[...])
+        leaving.append(pltpu.make_async_copy(m_out.at[rows, :], m_hbm.at[rows, :], sems.at[4, k]))
+        leaving[-1].start()
+    for copy in leaving:
+        copy.wait()
 
 
 def project(x, wv, wg, g, wp, count):
@@ -232,15 +237,18 @@
     return pl.pallas_call(
         project_kernel,
         in_specs=[hbm] * 5,
-        out_specs=[VMEM_SPEC] * 4,
-        out_shape=[jax.ShapeDtypeStruct((t, c), bf16)] * 3 + [jax.ShapeDtypeStruct((t, c), f32)],
+        out_specs=[HBM_SPEC] * 2 + [VMEM_SPEC, HBM_SPEC],
+        out_shape=[pltpu.HBM((t, c), bf16)] * 2 + [jax.ShapeDtypeStruct((t, c), bf16), pltpu.HBM((t, c), f32)],
         scratch_shapes=[
             pltpu.VMEM((count, t // count, d), bf16),
             pltpu.VMEM((count, t // count, d), bf16),
             pltpu.VMEM((d, c), bf16),
             pltpu.VMEM((d, c), bf16),
             pltpu.VMEM((c, d), bf16),
-            pltpu.SemaphoreType.DMA((3, max(3, count))),
+            pltpu.VMEM((t, c), bf16),
+            pltpu.VMEM((t, c), bf16),
+            pltpu.VMEM((t, c), f32),
+            pltpu.SemaphoreType.DMA((5, max(3, count))),
         ],
         compiler_params=limit(20),
         cost_estimate=pl.CostEstimate(
@@ -440,8 +448,9 @@
 
 def back_conv_kernel(
     normed_ref, gn_ref, stats_ref, before_ref, glu_ref, after_ref, v_ref, s_ref, taps_ref,
-    out_ref, turned_ref, small_ref, ext_ref, grad_ref, col_ref,
+    out_ref, turned_out, small_ref, ext_ref, grad_ref, col_ref, *leave,
 ):
+    turned_ref = leave[0] if leave else turned_out
     tok = glu_ref.shape[0]
     rows = tok + HALO
     taps = taps_ref.shape[0]
@@ -483,6 +492,9 @@
     lax.fori_loop(0, tok // chunk, spread, 0)
     for i in range(0, tok, LANE):
         turned_ref[:, pl.ds(i, LANE)] = out_ref[pl.ds(i, LANE), :].T
+    if leave:
+        leaving = pltpu.make_async_copy(turned_ref, turned_out, leave[1])
+        leaving.start()
 
     width = chunk_of(tok, 32)
 
@@ -505,9 +517,11 @@
         small_ref[pl.ds(k, 1), :] = jnp.sum(sums[k], axis=0, keepdims=True)
     for k in range(taps, small_ref.shape[0]):
         small_ref[pl.ds(k, 1), :] = jnp.zeros((1, LANE), f32)
-
-
-def back_convolve(normed, gn, stats, before, glu, after, v, s, conv_taps, h):
+    if leave:
+        leaving.wait()
+
+
+def back_convolve(normed, gn, stats, before, glu, after, v, s, conv_taps, h, leave):
     tok, _ = glu.shape
     taps = conv_taps.shape[0]
     wide = stats.shape[1]
@@ -530,19 +544,20 @@
         ],
         out_specs=[
             pl.BlockSpec((tok, 2 * LANE), first),
-            pl.BlockSpec((2 * LANE, tok), first),
+            HBM_SPEC if leave else pl.BlockSpec((2 * LANE, tok), first),
             pl.BlockSpec((kept, LANE), first),
         ],
         out_shape=[
             jax.ShapeDtypeStruct((tok, 2 * LANE), bf16),
-            jax.ShapeDtypeStruct((2 * LANE, tok), bf16),
+            (pltpu.HBM if leave else jax.ShapeDtypeStruct)((2 * LANE, tok), bf16),
             jax.ShapeDtypeStruct((kept, LANE), f32),
         ],
         scratch_shapes=[
             pltpu.VMEM((tok + 2 * HALO, LANE), f32),
             pltpu.VMEM((tok + HALO, LANE), f32),
             pltpu.VMEM((wide, 8), f32),
-        ],
+        ]
+        + ([pltpu.VMEM((2 * LANE, tok), bf16), pltpu.SemaphoreType.DMA] if leave else []),
         compiler_params=limit(12),
         cost_estimate=pl.CostEstimate(
             flops=40 * taps * tok * LANE, transcendentals=0, bytes_accessed=16 * tok * LANE
@@ -551,69 +566,73 @@
     )(normed, gn, stats, before, glu, after, v, s, conv_taps)
 
 
-def input_kernel(index_ref, *refs, halves, count, add):
+def input_kernel(index_ref, *refs, halves, fetch):
     grads = refs[:halves]
-    value_ref, gate_ref = refs[halves : halves + 2]
-    out_ref = refs[-1]
-    width = out_ref.shape[2]
-    tok = out_ref.shape[1]
-    block = tok // 4
-    for i in range(count):
-        rows = pl.ds(pl.multiple_of(index_ref[i] * width, 16), width)
-        weight = []
-        for h in range(halves):
-            cols = pl.ds(h * LANE, LANE)
-            weight += [value_ref[rows, cols], gate_ref[rows, cols]]
-        weight = jnp.concatenate(weight, axis=1)
-        for k in range(4):
-            here = pl.ds(k * block, block)
-            total = right_product(jnp.concatenate([g[here, :] for g in grads], axis=1), weight)
-            if add:
-                total = total + refs[halves + 2][index_ref[count + i], here, :].astype(f32)
-            out_ref[i, here, :] = total.astype(bf16)
-
-
-def input_blocks(grads, w_value, w_gate, blocks, n, got=None, got_block=None):
-    halves = len(grads)
+    if fetch:
+        value_hbm, gate_hbm, add_ref, out_ref, value_ref, gate_ref, sems = refs[halves:]
+        copies = []
+        for m, (hbm, ref) in enumerate(((value_hbm, value_ref), (gate_hbm, gate_ref))):
+            start = pl.multiple_of(index_ref[0] * ref.shape[0], 16)
+            copies.append(pltpu.make_async_copy(hbm.at[pl.ds(start, ref.shape[0]), :], ref, sems.at[m]))
+        for copy in copies:
+            copy.start()
+        for copy in copies:
+            copy.wait()
+        rows = slice(None)
+    else:
+        value_ref, gate_ref, out_ref = refs[halves:]
+        rows = pl.ds(pl.multiple_of(index_ref[0] * out_ref.shape[1], 16), out_ref.shape[1])
+    weight = []
+    for h in range(halves):
+        cols = pl.ds(h * LANE, LANE)
+        weight += [value_ref[rows, cols], gate_ref[rows, cols]]
+    total = right_product(
+        jnp.concatenate([g[...] for g in grads], axis=1), jnp.concatenate(weight, axis=1)
+    )
+    if fetch:
+        total = total + add_ref[...]
+    out_ref[...] = total.astype(out_ref.dtype)
+
+
+def input_block(grads, value, gate, block, n, add=None):
     t = grads[0].shape[0]
-    d, c = w_value.shape
+    d, c = value.shape
     width = d // n
-    count = blocks.shape[0]
-    index = blocks
-    add = got is not None
-    if add:
-        index = jnp.concatenate([blocks, got_block])
+    fetch = add is not None
+    weights = [pl.BlockSpec(memory_space=pl.ANY)] * 2 + [VMEM_SPEC] if fetch else [VMEM_SPEC] * 2
+    scratch = [
+        pltpu.VMEM((width, c), bf16),
+        pltpu.VMEM((width, c), bf16),
+        pltpu.SemaphoreType.DMA((2,)),
+    ]
     return pl.pallas_call(
-        functools.partial(input_kernel, halves=halves, count=count, add=add),
-        in_specs=[SMEM_SPEC] + [VMEM_SPEC] * (halves + 2 + add),
+        functools.partial(input_kernel, halves=len(grads), fetch=fetch),
+        in_specs=[SMEM_SPEC] + [VMEM_SPEC] * len(grads) + weights,
         out_specs=VMEM_SPEC,
-        out_shape=jax.ShapeDtypeStruct((count, t, width), bf16),
-        compiler_params=limit(16),
+        out_shape=jax.ShapeDtypeStruct((t, width), bf16 if fetch else f32),
+        scratch_shapes=scratch if fetch else [],
+        compiler_params=limit(14),
         cost_estimate=pl.CostEstimate(
-            flops=4 * t * c * count * width,
-            transcendentals=0,
-            bytes_accessed=2 * (2 * t * c + 2 * count * width * c + count * t * width),
-        ),
-        name="input_blocks",
-    )(index.astype(jnp.int32), *grads, w_value, w_gate, *([got] if add else []))
-
-
-def input_gradient(grads, w_value, w_gate):
+            flops=4 * t * c * width, transcendentals=0, bytes_accessed=2 * (2 * t * c + 2 * width * c + 3 * t * width)
+        ),
+        name="input_block",
+    )(block.reshape(1).astype(jnp.int32), *grads, value, gate, *([add] if fetch else []))
+
+
+def input_gradient(grads, pair_grads, weights, pair_weights):
     n = lax.axis_size("tp")
     me = lax.axis_index("tp")
-    half = n // 2
-    high = jnp.arange(half)
-    out = input_blocks(grads, w_value, w_gate, 2 * high + (me % 2 ^ 1), n)
-    got = send(out, "tp", lambda i: i ^ 1)
-    own = (me // 2).reshape(1)
+
+    def both(block):
+        own = input_block(grads, *weights, block, n)
+        return input_block(pair_grads, *pair_weights, block, n, own)
+
     parts = []
-    for k in range(1, half):
-        other = (me // 2 ^ k).reshape(1)
-        part = input_blocks(grads, w_value, w_gate, 2 * other + me % 2, n, got, other)
-        parts.append(send(part, "tp", lambda i, k=k: i ^ (2 * k)))
-    total = input_blocks(grads, w_value, w_gate, 2 * own + me % 2, n, got, own)[0].astype(f32)
+    for k in range(1, n // 2):
+        parts.append(send(both(me ^ (2 * k)), "tp", lambda i, k=k: i ^ (2 * k)))
+    total = both(me)
     for part in parts:
-        total = total + part[0].astype(f32)
+        total = total.astype(f32) + part.astype(f32)
     return total.astype(bf16)
 
 
@@ -659,6 +678,8 @@
     )
     after = send(jnp.concatenate([gated_input[:HALO].astype(f32), own_mixed[:HALO]], axis=0), "sp", lambda i: i - 1)
     before = send(gated_input[tok - HALO :], "sp", lambda i: i + 1)
+    pair_value = send(w_value, "tp", lambda i: i ^ 1)
+    pair_gate = send(w_gate, "tp", lambda i: i ^ 1)
     inner = convolve(gated_input, conv_taps)
     filtered = convolve_ends(inner, before, gated_input, after, conv_taps)
     stats = all_sum(row_sums(filtered, filtered * filtered), "tp")
@@ -672,13 +693,15 @@
     proj_parts, _ = reduce_blocks(turned, out_grad, last_first=True)
     halves = ch // LANE
     grads = []
+    pair_grads = []
     sums = []
     small = []
     for h in range(halves):
         grad, turn, tap_sums = back_convolve(
-            normed, grad_normed, stats, before, gated_input, after, value_proj, gate_proj, conv_taps, h
+            normed, grad_normed, stats, before, gated_input, after, value_proj, gate_proj, conv_taps, h, h > 0
         )
         grads.append(grad)
+        pair_grads.append(send(grad, "tp", lambda i: i ^ 1))
         small.append(tap_sums)
         rider = None
         if h == halves - 1:
@@ -686,7 +709,7 @@
         parts, small_sum = reduce_blocks(turn, block_input, rider)
         sums.append(parts)
     kept = small[0].shape[0]
-    input_grad = input_gradient(grads, w_value, w_gate)
+    input_grad = input_gradient(grads, pair_grads, (w_value, w_gate), (pair_value, pair_gate))
     proj_wgrad = sum(p.astype(f32) for p in proj_parts) * loss_scale
     value_wgrad, gate_wgrad = last_sums(sums, loss_scale)
     return (

time: 157 us -> 144 us (0.917)
  local copies, waits for them, and re-layouts: 19.9 us -> 5.31 us
    unnamed x66 -> x46, local copies, waits for them, and re-layouts: 18.8 us -> 4.48 us
    convert_element_type x2 -> x3, other arithmetic: 0.28 us -> 2.55 us  [reduce_blocks(): sent = [pick(k).astype(bf16) for k in range(1, r)]]
    pallas_call x4 -> x5, Pallas kernels: 13.6 us -> 11.6 us  [the longest x1 8.52 us: project(): pl.pallas_call(project_kernel, in_specs=[hbm] * 5, out_specs=[HBM_SPEC] *...]
    ppermute x20 -> x23, waiting for transfers between devices: 50.7 us -> 51.7 us  [send(): return lax.ppermute(block, axis, route)]
    ppermute x20 -> x23, starting transfers between devices: 37.3 us -> 38.3 us  [send(): return lax.ppermute(block, axis, route)]
  transfers between devices with their start and end apart: 20 -> 23, of which waited for: 8 -> 10; matrix products, arithmetic and copies ran while one was open for 4% -> 5% of each run, Pallas kernels for 9% -> 9%
where the time goes in v1:
time: 144 us
  waiting for transfers between devices  51.7 us (36%)
  starting transfers between devices  38.3 us (27%)
  Pallas kernels  38.2 us (27%)
  other arithmetic  8.79 us (6%)
  local copies, waits for them, and re-layouts  5.31 us (4%)
    ppermute x23, waiting for transfers between devices, send(): return lax.ppermute(block, axis, route)  51.7 us
    ppermute x23, starting transfers between devices, send(): return lax.ppermute(block, axis, route)  38.3 us
    pallas_call x2, Pallas kernels, back_convolve(): pl.pallas_call(back_conv_kernel, grid=(1,), in_specs=[pl.BlockSpec((tok +...  11.1 us
    pallas_call x1, Pallas kernels, project(): pl.pallas_call(project_kernel, in_specs=[hbm] * 5, out_specs=[HBM_SPEC] *...  8.52 us
    pallas_call x3, Pallas kernels, grad_blocks(): pl.pallas_call(functools.partial(blocks_kernel, gives=gives), in_specs=[S...  7.95 us
    unnamed x46, local copies, waits for them, and re-layouts  4.48 us
    pallas_call x1, Pallas kernels, convolve(): pl.pallas_call(conv_kernel, grid=(ch // LANE,), in_specs=[pl.BlockSpec((t...  3.95 us
    pallas_call x4, Pallas kernels, input_block(): pl.pallas_call(functools.partial(input_kernel, halves=len(grads), fetch=f...  3.08 us
  transfers between devices with their start and end apart: 23, of which 10 were waited for; matrix products, arithmetic and copies ran while one was open for 5% of the time, Pallas kernels for 9%

profile of v1, /device:TPU:0, one launch (start us, length us, event | category | flops | bytes accessed | tf_op | source)
XLA Modules:
  0.0 143.7 jit_solution(3807298183278587677)
XLA Ops:
  0.6 8.5 %project.1 = (bf16[1024,256]{1,0:T(8,128)(2,1)}, bf16[1024,256]{1,0:T(8,128)(2,1)}, bf16[1024,256]{1,0:T(8,128)(2,1)S(1)}, f32[1024,256]{1,0:T(8,128)}) custom-call(bf16[1024,2048]{1,0:T(8,128)(2,1)} %right_ref.4, bf16[2048,256]{1,0:T(8,128)(2,1)} %refs_2_.3, bf16[2048,256]{1,0:T(8,128)(2,1)} %refs_3_.3, bf16[1024,2048]{1,0:T(8,128)(2,1)} %right_ref.5, ...), custom_call_target="tpu_custom_call" | custom-call | flops 3221225472 | bytes 14155776 | tf_op jit(solution)/shard_map/project/pallas_call | solution.py:237
  9.2 0.8 slice.55
  10.0 1.3 collective-permute-start.1
  11.2 5.5 %collective-permute-start = (bf16[32,256]{1,0:T(8,128)(2,1)S(1)}, bf16[32,256]{1,0:T(8,128)(2,1)S(1)}, u32[]{:S(2)}, u32[]{:S(2)}) collective-permute-start(bf16[32,256]{1,0:T(8,128)(2,1)S(1)} %get-tuple-element.69.tail_ref), channel_id=1, source_target_pairs={{0,4},{4,8},{8,12},{12,16},{16,20},{20,24},{24,28},{1,5},{5,9},{9,... | collective-permute-start | bytes 49160 | tf_op jit(solution)/shard_map/ppermute | solution.py:31
  16.8 4.0 %convolve.1.main_ref = f32[1056,256]{1,0:T(8,128)S(1)} custom-call(bf16[1024,256]{1,0:T(8,128)(2,1)S(1)} %get-tuple-element.31.glu_ref, f32[31,256]{1,0:T(8,128)S(1)} %copy-done.14), custom_call_target="tpu_custom_call" | custom-call | flops 162529280 | bytes 1572864 | tf_op jit(solution)/shard_map/convolve/pallas_call | solution.py:308
  21.7 1.1 collective-permute-done.2
  22.8 2.1 %collective-permute-start.3 = (f32[2,1152]{1,0:T(2,128)S(1)}, f32[2,1152]{1,0:T(2,128)S(1)}, u32[]{:S(2)}, u32[]{:S(2)}) collective-permute-start(f32[2,1152]{1,0:T(2,128)S(1)} %fusion.4), channel_id=1, source_target_pairs={{0,2},{1,3},{2,0},{3,1},{4,6},{5,7},{6,4},{7,5},{8,10},{9,11},{10,... | collective-permute-start | bytes 27656 | tf_op jit(solution)/shard_map/ppermute | solution.py:31
  24.8 1.7 %collective-permute-done.3 = f32[2,1152]{1,0:T(2,128)S(1)} collective-permute-done((f32[2,1152]{1,0:T(2,128)S(1)}, f32[2,1152]{1,0:T(2,128)S(1)}, u32[]{:S(2)}, u32[]{:S(2)}) %collective-permute-start.3) | collective-permute-done | bytes 9248 | tf_op jit(solution)/shard_map/ppermute | solution.py:31
  26.6 2.4 %activate.1 = (f32[1056,256]{1,0:T(8,128)S(1)}, f32[1056,256]{1,0:T(8,128)S(1)}, bf16[256,1024]{1,0:T(8,128)(2,1)S(1)}, f32[16,256]{1,0:T(8,128)S(1)}) custom-call(f32[1056,256]{1,0:T(8,128)S(1)} %convolve_ends.1.filtered_ref, f32[8,1152]{1,0:T(8,128)S(1)} %select_maximum_fusion.1.stats_ref, f32[1024,256]{1,0:T(8,128)S(1)} %copy-done.13, ...), custom_call_target="tpu_custom_call" | custom-call | flops 52428800 | bytes 4718592 | tf_op jit(solution)/shard_map/activate/pallas_call | solution.py:417
  29.6 1.1 collective-permute-done.4
  30.7 2.1 %collective-permute-start.5 = (f32[2,1152]{1,0:T(2,128)S(1)}, f32[2,1152]{1,0:T(2,128)S(1)}, u32[]{:S(2)}, u32[]{:S(2)}) collective-permute-start(f32[2,1152]{1,0:T(2,128)S(1)} %fusion.5), channel_id=1, source_target_pairs={{0,2},{1,3},{2,0},{3,1},{4,6},{5,7},{6,4},{7,5},{8,10},{9,11},{10,... | collective-permute-start | bytes 27656 | tf_op jit(solution)/shard_map/ppermute | solution.py:31
  32.8 1.6 %collective-permute-done.5 = f32[2,1152]{1,0:T(2,128)S(1)} collective-permute-done((f32[2,1152]{1,0:T(2,128)S(1)}, f32[2,1152]{1,0:T(2,128)S(1)}, u32[]{:S(2)}, u32[]{:S(2)}) %collective-permute-start.5) | collective-permute-done | bytes 9248 | tf_op jit(solution)/shard_map/ppermute | solution.py:31
  34.5 5.6 %back_convolve.3 = (bf16[1024,256]{1,0:T(8,128)(2,1)S(1)}, bf16[256,1024]{1,0:T(8,128)(2,1)}, f32[32,128]{1,0:T(8,128)S(1)}) custom-call(f32[1056,256]{1,0:T(8,128)S(1)} %get-tuple-element.33.normed_ref, f32[1056,256]{1,0:T(8,128)S(1)} %get-tuple-element.34.gn_ref, f32[8,1152]{1,0:T(8,128)S(1)} %select_maximum_fusion.stats_ref, ...), custom_call_target="tpu_custom_call" | custom-call | flops 162529280 | bytes 2097152 | tf_op jit(solution)/shard_map/back_convolve/pallas_call | solution.py:531
  40.1 0.8 copy-done.10
  40.9 5.5 %back_convolve.2 = (bf16[1024,256]{1,0:T(8,128)(2,1)S(1)}, bf16[256,1024]{1,0:T(8,128)(2,1)S(1)}, f32[32,128]{1,0:T(8,128)S(1)}) custom-call(f32[1056,256]{1,0:T(8,128)S(1)} %get-tuple-element.33.normed_ref, f32[1056,256]{1,0:T(8,128)S(1)} %get-tuple-element.34.gn_ref, f32[8,1152]{1,0:T(8,128)S(1)} %select_maximum_fusion.stats_ref, ...), custom_call_target="tpu_custom_call" | custom-call | flops 162529280 | bytes 2097152 | tf_op jit(solution)/shard_map/back_convolve/pallas_call | solution.py:531
  46.5 2.9 %grad_blocks.4 = (bf16[1072,256]{1,0:T(8,128)(2,1)}, f32[4,256,256]{2,1,0:T(8,128)}) custom-call(s32[8]{0:T(128)S(1)} %pad_add_fusion.ids_ref, bf16[256,1024]{1,0:T(8,128)(2,1)S(1)} %copy-done.17, bf16[1024,2048]{1,0:T(8,128)(2,1)S(1)} %copy-done, bf16[48,256]{1,0:T(8,128)(2,1)S(1)} %pad_maximum_fusion.4.refs_0_), custom_call_target="tpu_custom_call" | custom-call | flops 1073741824 | bytes 6815744 | tf_op jit(solution)/shard_map/grad_blocks/pallas_call | solution.py:101
  49.5 3.0 %collective-permute-start.15 = (bf16[1072,256]{1,0:T(8,128)(2,1)}, bf16[1072,256]{1,0:T(8,128)(2,1)}, u32[]{:S(2)}, u32[]{:S(2)}) collective-permute-start(bf16[1072,256]{1,0:T(8,128)(2,1)} %get-tuple-element.47), channel_id=1, source_target_pairs={{0,4},{4,0},{8,12},{12,8},{16,20},{20,16},{24,28},{28,24},{1,5},{5... | collective-permute-start | bytes 1646600 | tf_op jit(solution)/shard_map/ppermute | solution.py:31
  52.5 2.7 %grad_blocks.5 = (bf16[512,256]{1,0:T(8,128)(2,1)}, bf16[512,256]{1,0:T(8,128)(2,1)}, bf16[512,256]{1,0:T(8,128)(2,1)S(1)}, f32[2,256,256]{2,1,0:T(8,128)}) custom-call(s32[8]{0:T(128)S(1)} %pad_add_fusion.1.ids_ref, bf16[256,1024]{1,0:T(8,128)(2,1)S(1)} %get-tuple-element.50.left_ref, bf16[1024,2048]{1,0:T(8,128)(2,1)S(1)} %copy-done.2), custom_call_target="tpu_custom_call" | custom-call | flops 1073741824 | bytes 6815744 | tf_op jit(solution)/shard_map/grad_blocks/pallas_call | solution.py:101
  55.2 1.6 %collective-permute-start.19 = (bf16[512,256]{1,0:T(8,128)(2,1)}, bf16[512,256]{1,0:T(8,128)(2,1)}, u32[]{:S(2)}, u32[]{:S(2)}) collective-permute-start(bf16[512,256]{1,0:T(8,128)(2,1)} %get-tuple-element.52), channel_id=1, source_target_pairs={{0,8},{4,12},{8,16},{12,20},{16,24},{20,28},{24,0},{28,4},{1,9},{5... | collective-permute-start | bytes 786440 | tf_op jit(solution)/shard_map/ppermute | solution.py:31
  56.8 1.1 collective-permute-start.20
  57.9 2.8 %collective-permute-start.21 = (bf16[512,256]{1,0:T(8,128)(2,1)S(1)}, bf16[512,256]{1,0:T(8,128)(2,1)}, u32[]{:S(2)}, u32[]{:S(2)}) collective-permute-start(bf16[512,256]{1,0:T(8,128)(2,1)S(1)} %get-tuple-element.54), channel_id=1, source_target_pairs={{0,24},{4,28},{8,0},{12,4},{16,8},{20,12},{24,16},{28,20},{1,25},{... | collective-permute-start | bytes 786440 | tf_op jit(solution)/shard_map/ppermute | solution.py:31
  60.8 1.0 copy-done.8
  61.8 1.0 copy-done.11
  62.9 0.7 input_block.4.refs_4_
  63.6 0.7 input_block.6.refs_4_
  64.4 1.4 copy-done.1
  65.9 2.4 %grad_blocks.3 = (bf16[1024,256]{1,0:T(8,128)(2,1)S(1)}, f32[4,256,256]{2,1,0:T(8,128)}) custom-call(s32[8]{0:T(128)S(1)} %pad_add_fusion.ids_ref, bf16[256,1024]{1,0:T(8,128)(2,1)S(1)} %copy-done.16, bf16[1024,2048]{1,0:T(8,128)(2,1)S(1)} %copy-done.1), custom_call_target="tpu_custom_call" | custom-call | flops 1073741824 | bytes 6815744 | tf_op jit(solution)/shard_map/grad_blocks/pallas_call | solution.py:101
  68.9 6.8 %collective-permute-done.20 = bf16[512,256]{1,0:T(8,128)(2,1)} collective-permute-done((bf16[512,256]{1,0:T(8,128)(2,1)}, bf16[512,256]{1,0:T(8,128)(2,1)}, u32[]{:S(2)}, u32[]{:S(2)}) %collective-permute-start.20) | collective-permute-done | bytes 262176 | tf_op jit(solution)/shard_map/ppermute | solution.py:31
  76.1 1.1 add_convert_fusion.1
  77.2 1.8 %collective-permute-start.22 = (bf16[256,256]{1,0:T(8,128)(2,1)S(1)}, bf16[256,256]{1,0:T(8,128)(2,1)S(1)}, u32[]{:S(2)}, u32[]{:S(2)}) collective-permute-start(bf16[256,256]{1,0:T(8,128)(2,1)S(1)} %add_convert_fusion.1), channel_id=1, source_target_pairs={{0,4},{4,0},{8,12},{12,8},{16,20},{20,16},{24,28},{28,24},{1,5},{5... | collective-permute-start | bytes 393224 | tf_op jit(solution)/shard_map/ppermute | solution.py:31
  79.0 0.7 add_convert_fusion.8
  79.8 1.3 add_convert_fusion.2
  81.1 11.7 %collective-permute-done.22 = bf16[256,256]{1,0:T(8,128)(2,1)S(1)} collective-permute-done((bf16[256,256]{1,0:T(8,128)(2,1)S(1)}, bf16[256,256]{1,0:T(8,128)(2,1)S(1)}, u32[]{:S(2)}, u32[]{:S(2)}) %collective-permute-start.22) | collective-permute-done | bytes 131104 | tf_op jit(solution)/shard_map/ppermute | solution.py:31
  92.9 7.2 %collective-permute-start.18 = (bf16[304,256]{1,0:T(8,128)(2,1)S(1)}, bf16[304,256]{1,0:T(8,128)(2,1)S(1)}, u32[]{:S(2)}, u32[]{:S(2)}) collective-permute-start(bf16[304,256]{1,0:T(8,128)(2,1)S(1)} %get-tuple-element.72), channel_id=1, source_target_pairs={{0,24},{4,28},{8,0},{12,4},{16,8},{20,12},{24,16},{28,20},{1,25},{... | collective-permute-start | bytes 466952 | tf_op jit(solution)/shard_map/ppermute | solution.py:31
  100.1 1.8 %add_multiply_fusion = f32[256,256]{1,0:T(8,128)} fusion(bf16[256,256]{1,0:T(8,128)(2,1)S(1)} %collective-permute-done.22, f32[512,256]{1,0:T(8,128)S(1)} %bitcast.23, s32[]{:T(128)S(6)} %select_n.164, bf16[512,256]{1,0:T(8,128)(2,1)} %collective-permute-done.21, bf16[512,256]{1,0:T(8,128)(2,1)} %collective-permute-done.20, ...), kind=kLoop, calls=%fused_computation.3 | loop fusion | flops 589824 | bytes 1048580 | tf_op jit(solution)/shard_map/mul | solution.py:713
  102.1 1.9 %collective-permute-done.18 = bf16[304,256]{1,0:T(8,128)(2,1)S(1)} collective-permute-done((bf16[304,256]{1,0:T(8,128)(2,1)S(1)}, bf16[304,256]{1,0:T(8,128)(2,1)S(1)}, u32[]{:S(2)}, u32[]{:S(2)}) %collective-permute-start.18) | collective-permute-done | bytes 155680 | tf_op jit(solution)/shard_map/ppermute | solution.py:31
  104.0 1.3 collective-permute-start.17
  105.3 3.5 %collective-permute-start.12 = (bf16[256,256]{1,0:T(8,128)(2,1)S(1)}, bf16[256,256]{1,0:T(8,128)(2,1)S(1)}, u32[]{:S(2)}, u32[]{:S(2)}) collective-permute-start(bf16[256,256]{1,0:T(8,128)(2,1)S(1)} %get-tuple-element.65), channel_id=1, source_target_pairs={{0,8},{4,12},{8,16},{12,20},{16,24},{20,28},{24,0},{28,4},{1,9},{5... | collective-permute-start | bytes 393224 | tf_op jit(solution)/shard_map/ppermute | solution.py:31
  108.9 2.4 %collective-permute-start.14 = (bf16[256,256]{1,0:T(8,128)(2,1)S(1)}, bf16[256,256]{1,0:T(8,128)(2,1)S(1)}, u32[]{:S(2)}, u32[]{:S(2)}) collective-permute-start(bf16[256,256]{1,0:T(8,128)(2,1)S(1)} %get-tuple-element.63), channel_id=1, source_target_pairs={{0,24},{4,28},{8,0},{12,4},{16,8},{20,12},{24,16},{28,20},{1,25},{... | collective-permute-start | bytes 393224 | tf_op jit(solution)/shard_map/ppermute | solution.py:31
  111.3 0.8 input_block.7
  112.1 12.0 %collective-permute-done.17 = bf16[304,256]{1,0:T(8,128)(2,1)S(1)} collective-permute-done((bf16[304,256]{1,0:T(8,128)(2,1)S(1)}, bf16[304,256]{1,0:T(8,128)(2,1)S(1)}, u32[]{:S(2)}, u32[]{:S(2)}) %collective-permute-start.17) | collective-permute-done | bytes 155680 | tf_op jit(solution)/shard_map/ppermute | solution.py:31
  124.1 1.5 %collective-permute-start.10 = (bf16[1024,512]{1,0:T(8,128)(2,1)S(1)}, bf16[1024,512]{1,0:T(8,128)(2,1)S(1)}, u32[]{:S(2)}, u32[]{:S(2)}) collective-permute-start(bf16[1024,512]{1,0:T(8,128)(2,1)S(1)} %input_block.7), channel_id=1, source_target_pairs={{0,2},{1,3},{2,0},{3,1},{4,6},{5,7},{6,4},{7,5},{8,10},{9,11},{10,... | collective-permute-start | bytes 3145736 | tf_op jit(solution)/shard_map/ppermute | solution.py:31
  125.6 1.2 collective-permute-done.13.refs_2_
  126.9 1.0 last_sums.1
  128.5 0.6 fusion
  129.1 0.8 input_block.5
  129.9 12.5 %collective-permute-done.10 = bf16[1024,512]{1,0:T(8,128)(2,1)S(1)} collective-permute-done((bf16[1024,512]{1,0:T(8,128)(2,1)S(1)}, bf16[1024,512]{1,0:T(8,128)(2,1)S(1)}, u32[]{:S(2)}, u32[]{:S(2)}) %collective-permute-start.10) | collective-permute-done | bytes 1048608 | tf_op jit(solution)/shard_map/ppermute | solution.py:31
  142.4 1.3 add_convert_fusion
  (102 shorter events, 3.6 us)
Async XLA Ops:
  0.6 16.2 %copy-start.14 = (f32[31,256]{1,0:T(8,128)S(1)}, f32[31,256]{1,0:T(8,128)}, u32[]{:S(2)}) copy-start(f32[31,256]{1,0:T(8,128)} %taps_ref.7) | copy-start | bytes 95236
  10.0 10.8 %collective-permute-start.1 = (f32[64,256]{1,0:T(8,128)S(1)}, f32[64,256]{1,0:T(8,128)S(1)}, u32[]{:S(2)}, u32[]{:S(2)}) collective-permute-start(f32[64,256]{1,0:T(8,128)S(1)} %pad_maximum_fusion.3), channel_id=1, source_target_pairs={{4,0},{8,4},{12,8},{16,12},{20,16},{24,20},{28,24},{5,1},{9,5},{13... | collective-permute-start | bytes 196616 | tf_op jit(solution)/shard_map/ppermute | solution.py:31
  11.2 9.5 %collective-permute-start = (bf16[32,256]{1,0:T(8,128)(2,1)S(1)}, bf16[32,256]{1,0:T(8,128)(2,1)S(1)}, u32[]{:S(2)}, u32[]{:S(2)}) collective-permute-start(bf16[32,256]{1,0:T(8,128)(2,1)S(1)} %get-tuple-element.69.tail_ref), channel_id=1, source_target_pairs={{0,4},{4,8},{8,12},{12,16},{16,20},{20,24},{24,28},{1,5},{5,9},{9,... | collective-permute-start | bytes 49160 | tf_op jit(solution)/shard_map/ppermute | solution.py:31
  21.0 5.5 %copy-start.13 = (f32[1024,256]{1,0:T(8,128)S(1)}, f32[1024,256]{1,0:T(8,128)}, u32[]{:S(2)}) copy-start(f32[1024,256]{1,0:T(8,128)} %get-tuple-element.32.mixed_ref) | copy-start | bytes 3145732
  21.0 5.5 %copy-start.18 = (f32[256]{0:T(256)S(1)}, f32[256]{0:T(256)}, u32[]{:S(2)}) copy-start(f32[256]{0:T(256)} %param.13) | copy-start | bytes 3076
  21.1 5.5 %copy-start.19 = (f32[256]{0:T(256)S(1)}, f32[256]{0:T(256)}, u32[]{:S(2)}) copy-start(f32[256]{0:T(256)} %param.14) | copy-start | bytes 3076
  21.5 1.2 collective-permute-start.2
  22.8 3.7 %collective-permute-start.3 = (f32[2,1152]{1,0:T(2,128)S(1)}, f32[2,1152]{1,0:T(2,128)S(1)}, u32[]{:S(2)}, u32[]{:S(2)}) collective-permute-start(f32[2,1152]{1,0:T(2,128)S(1)} %fusion.4), channel_id=1, source_target_pairs={{0,2},{1,3},{2,0},{3,1},{4,6},{5,7},{6,4},{7,5},{8,10},{9,11},{10,... | collective-permute-start | bytes 27656 | tf_op jit(solution)/shard_map/ppermute | solution.py:31
  29.0 5.5 %copy-start.5 = (bf16[1024,256]{1,0:T(8,128)(2,1)S(1)}, bf16[1024,256]{1,0:T(8,128)(2,1)}, u32[]{:S(2)}) copy-start(bf16[1024,256]{1,0:T(8,128)(2,1)} %get-tuple-element.35.v_ref) | copy-start | bytes 1572868
  29.0 5.5 %copy-start.6 = (bf16[1024,256]{1,0:T(8,128)(2,1)S(1)}, bf16[1024,256]{1,0:T(8,128)(2,1)}, u32[]{:S(2)}) copy-start(bf16[1024,256]{1,0:T(8,128)(2,1)} %get-tuple-element.36.s_ref) | copy-start | bytes 1572868
  29.5 1.2 collective-permute-start.4
  30.7 3.7 %collective-permute-start.5 = (f32[2,1152]{1,0:T(2,128)S(1)}, f32[2,1152]{1,0:T(2,128)S(1)}, u32[]{:S(2)}, u32[]{:S(2)}) collective-permute-start(f32[2,1152]{1,0:T(2,128)S(1)} %fusion.5), channel_id=1, source_target_pairs={{0,2},{1,3},{2,0},{3,1},{4,6},{5,7},{6,4},{7,5},{8,10},{9,11},{10,... | collective-permute-start | bytes 27656 | tf_op jit(solution)/shard_map/ppermute | solution.py:31
  34.5 12.0 %copy-start = (bf16[1024,2048]{1,0:T(8,128)(2,1)S(1)}, bf16[1024,2048]{1,0:T(8,128)(2,1)}, u32[]{:S(2)}) copy-start(bf16[1024,2048]{1,0:T(8,128)(2,1)} %right_ref.4) | copy-start | bytes 12582916
  40.1 0.8 copy-start.10
  40.9 5.6 %copy-start.17 = (bf16[256,1024]{1,0:T(8,128)(2,1)S(1)}, bf16[256,1024]{1,0:T(8,128)(2,1)}, u32[]{:S(2)}) copy-start(bf16[256,1024]{1,0:T(8,128)(2,1)} %get-tuple-element.42.left_ref) | copy-start | bytes 1572868
  46.4 3.0 %copy-start.7 = (bf16[1024,256]{1,0:T(8,128)(2,1)}, bf16[1024,256]{1,0:T(8,128)(2,1)S(1)}, u32[]{:S(2)}) copy-start(bf16[1024,256]{1,0:T(8,128)(2,1)S(1)} %get-tuple-element.37.refs_0_) | copy-start | bytes 1572868
  46.4 3.0 %copy-start.15 = (bf16[256,1024]{1,0:T(8,128)(2,1)}, bf16[256,1024]{1,0:T(8,128)(2,1)S(1)}, u32[]{:S(2)}) copy-start(bf16[256,1024]{1,0:T(8,128)(2,1)S(1)} %get-tuple-element.39.left_ref) | copy-start | bytes 1572868
  46.5 6.0 %copy-start.2 = (bf16[1024,2048]{1,0:T(8,128)(2,1)S(1)}, bf16[1024,2048]{1,0:T(8,128)(2,1)}, u32[]{:S(2)}) copy-start(bf16[1024,2048]{1,0:T(8,128)(2,1)} %right_ref.5) | copy-start | bytes 12582916
  49.5 27.7 %collective-permute-start.15 = (bf16[1072,256]{1,0:T(8,128)(2,1)}, bf16[1072,256]{1,0:T(8,128)(2,1)}, u32[]{:S(2)}, u32[]{:S(2)}) collective-permute-start(bf16[1072,256]{1,0:T(8,128)(2,1)} %get-tuple-element.47), channel_id=1, source_target_pairs={{0,4},{4,0},{8,12},{12,8},{16,20},{20,16},{24,28},{28,24},{1,5},{5... | collective-permute-start | bytes 1646600 | tf_op jit(solution)/shard_map/ppermute | solution.py:31
  52.5 8.3 %copy-start.3 = (bf16[2048,256]{1,0:T(8,128)(2,1)S(1)}, bf16[2048,256]{1,0:T(8,128)(2,1)}, u32[]{:S(2)}) copy-start(bf16[2048,256]{1,0:T(8,128)(2,1)} %refs_2_.3) | copy-start | bytes 3145732
  52.5 8.3 %copy-start.4 = (bf16[2048,256]{1,0:T(8,128)(2,1)S(1)}, bf16[2048,256]{1,0:T(8,128)(2,1)}, u32[]{:S(2)}) copy-start(bf16[2048,256]{1,0:T(8,128)(2,1)} %refs_3_.3) | copy-start | bytes 3145732
  55.2 13.1 %collective-permute-start.19 = (bf16[512,256]{1,0:T(8,128)(2,1)}, bf16[512,256]{1,0:T(8,128)(2,1)}, u32[]{:S(2)}, u32[]{:S(2)}) collective-permute-start(bf16[512,256]{1,0:T(8,128)(2,1)} %get-tuple-element.52), channel_id=1, source_target_pairs={{0,8},{4,12},{8,16},{12,20},{16,24},{20,28},{24,0},{28,4},{1,9},{5... | collective-permute-start | bytes 786440 | tf_op jit(solution)/shard_map/ppermute | solution.py:31
  56.8 18.9 %collective-permute-start.20 = (bf16[512,256]{1,0:T(8,128)(2,1)}, bf16[512,256]{1,0:T(8,128)(2,1)}, u32[]{:S(2)}, u32[]{:S(2)}) collective-permute-start(bf16[512,256]{1,0:T(8,128)(2,1)} %get-tuple-element.53), channel_id=1, source_target_pairs={{0,16},{4,20},{8,24},{12,28},{16,0},{20,4},{24,8},{28,12},{1,17},{... | collective-permute-start | bytes 786440 | tf_op jit(solution)/shard_map/ppermute | solution.py:31
  57.9 17.8 %collective-permute-start.21 = (bf16[512,256]{1,0:T(8,128)(2,1)S(1)}, bf16[512,256]{1,0:T(8,128)(2,1)}, u32[]{:S(2)}, u32[]{:S(2)}) collective-permute-start(bf16[512,256]{1,0:T(8,128)(2,1)S(1)} %get-tuple-element.54), channel_id=1, source_target_pairs={{0,24},{4,28},{8,0},{12,4},{16,8},{20,12},{24,16},{28,20},{1,25},{... | collective-permute-start | bytes 786440 | tf_op jit(solution)/shard_map/ppermute | solution.py:31
  60.8 48.1 %collective-permute-start.8 = (bf16[2048,256]{1,0:T(8,128)(2,1)S(1)}, bf16[2048,256]{1,0:T(8,128)(2,1)S(1)}, u32[]{:S(2)}, u32[]{:S(2)}) collective-permute-start(bf16[2048,256]{1,0:T(8,128)(2,1)S(1)} %copy-done.3), channel_id=1, source_target_pairs={{0,1},{1,0},{2,3},{3,2},{4,5},{5,4},{6,7},{7,6},{8,9},{9,8},{10,11... | collective-permute-start | bytes 3145736 | tf_op jit(solution)/shard_map/ppermute | solution.py:31
  60.8 1.0 copy-start.8
  61.8 1.0 copy-start.11
  63.6 2.2 %copy-start.1 = (bf16[1024,2048]{1,0:T(8,128)(2,1)S(1)}, bf16[1024,2048]{1,0:T(8,128)(2,1)}, u32[]{:S(2)}) copy-start(bf16[1024,2048]{1,0:T(8,128)(2,1)} %right_ref.4) | copy-start | bytes 12582916
  63.6 2.3 %copy-start.16 = (bf16[256,1024]{1,0:T(8,128)(2,1)S(1)}, bf16[256,1024]{1,0:T(8,128)(2,1)}, u32[]{:S(2)}) copy-start(bf16[256,1024]{1,0:T(8,128)(2,1)} %copy-done.15) | copy-start | bytes 1572868
  65.9 9.8 %copy-start.12 = (bf16[1024,256]{1,0:T(8,128)(2,1)S(1)}, bf16[1024,256]{1,0:T(8,128)(2,1)}, u32[]{:S(2)}) copy-start(bf16[1024,256]{1,0:T(8,128)(2,1)} %copy-done.10) | copy-start | bytes 1572868
  65.9 10.2 %copy-start.22 = (f32[2,256,256]{2,1,0:T(8,128)S(1)}, f32[2,256,256]{2,1,0:T(8,128)}, u32[]{:S(2)}) copy-start(f32[2,256,256]{2,1,0:T(8,128)} %get-tuple-element.51) | copy-start | bytes 1572868
  65.9 13.8 %copy-start.21 = (f32[4,256,256]{2,1,0:T(8,128)S(1)}, f32[4,256,256]{2,1,0:T(8,128)}, u32[]{:S(2)}) copy-start(f32[4,256,256]{2,1,0:T(8,128)} %get-tuple-element.46) | copy-start | bytes 3145732
  68.3 43.0 %collective-permute-start.9 = (bf16[2048,256]{1,0:T(8,128)(2,1)S(1)}, bf16[2048,256]{1,0:T(8,128)(2,1)S(1)}, u32[]{:S(2)}, u32[]{:S(2)}) collective-permute-start(bf16[2048,256]{1,0:T(8,128)(2,1)S(1)} %copy-done.4), channel_id=1, source_target_pairs={{0,1},{1,0},{2,3},{3,2},{4,5},{5,4},{6,7},{7,6},{8,9},{9,8},{10,11... | collective-permute-start | bytes 3145736 | tf_op jit(solution)/shard_map/ppermute | solution.py:31
  75.7 29.6 %collective-permute-start.7 = (bf16[1024,256]{1,0:T(8,128)(2,1)S(1)}, bf16[1024,256]{1,0:T(8,128)(2,1)S(1)}, u32[]{:S(2)}, u32[]{:S(2)}) collective-permute-start(bf16[1024,256]{1,0:T(8,128)(2,1)S(1)} %copy-done.12), channel_id=1, source_target_pairs={{0,1},{1,0},{2,3},{3,2},{4,5},{5,4},{6,7},{7,6},{8,9},{9,8},{10,11... | collective-permute-start | bytes 1572872 | tf_op jit(solution)/shard_map/ppermute | solution.py:31
  75.7 17.2 %collective-permute-start.11 = (bf16[1024,256]{1,0:T(8,128)(2,1)S(1)}, bf16[1024,256]{1,0:T(8,128)(2,1)S(1)}, u32[]{:S(2)}, u32[]{:S(2)}) collective-permute-start(bf16[1024,256]{1,0:T(8,128)(2,1)S(1)} %get-tuple-element.41), channel_id=1, source_target_pairs={{0,4},{4,0},{8,12},{12,8},{16,20},{20,16},{24,28},{28,24},{1,5},{5... | collective-permute-start | bytes 1572872 | tf_op jit(solution)/shard_map/ppermute | solution.py:31
  77.2 15.7 %collective-permute-start.22 = (bf16[256,256]{1,0:T(8,128)(2,1)S(1)}, bf16[256,256]{1,0:T(8,128)(2,1)S(1)}, u32[]{:S(2)}, u32[]{:S(2)}) collective-permute-start(bf16[256,256]{1,0:T(8,128)(2,1)S(1)} %add_convert_fusion.1), channel_id=1, source_target_pairs={{0,4},{4,0},{8,12},{12,8},{16,20},{20,16},{24,28},{28,24},{1,5},{5... | collective-permute-start | bytes 393224 | tf_op jit(solution)/shard_map/ppermute | solution.py:31
  79.7 13.1 %copy-start.9 = (bf16[1024,256]{1,0:T(8,128)(2,1)S(1)}, bf16[1024,256]{1,0:T(8,128)(2,1)}, u32[]{:S(2)}) copy-start(bf16[1024,256]{1,0:T(8,128)(2,1)} %copy-done.7) | copy-start | bytes 1572868
  81.1 20.9 %copy-start.20 = (f32[4,256,256]{2,1,0:T(8,128)S(1)}, f32[4,256,256]{2,1,0:T(8,128)}, u32[]{:S(2)}) copy-start(f32[4,256,256]{2,1,0:T(8,128)} %get-tuple-element.40) | copy-start | bytes 3145732
  92.9 16.0 %collective-permute-start.6 = (bf16[1024,256]{1,0:T(8,128)(2,1)S(1)}, bf16[1024,256]{1,0:T(8,128)(2,1)S(1)}, u32[]{:S(2)}, u32[]{:S(2)}) collective-permute-start(bf16[1024,256]{1,0:T(8,128)(2,1)S(1)} %copy-done.9), channel_id=1, source_target_pairs={{0,1},{1,0},{2,3},{3,2},{4,5},{5,4},{6,7},{7,6},{8,9},{9,8},{10,11... | collective-permute-start | bytes 1572872 | tf_op jit(solution)/shard_map/ppermute | solution.py:31
  92.9 11.1 %collective-permute-start.18 = (bf16[304,256]{1,0:T(8,128)(2,1)S(1)}, bf16[304,256]{1,0:T(8,128)(2,1)S(1)}, u32[]{:S(2)}, u32[]{:S(2)}) collective-permute-start(bf16[304,256]{1,0:T(8,128)(2,1)S(1)} %get-tuple-element.72), channel_id=1, source_target_pairs={{0,24},{4,28},{8,0},{12,4},{16,8},{20,12},{24,16},{28,20},{1,25},{... | collective-permute-start | bytes 466952 | tf_op jit(solution)/shard_map/ppermute | solution.py:31
  104.0 20.1 %collective-permute-start.17 = (bf16[304,256]{1,0:T(8,128)(2,1)S(1)}, bf16[304,256]{1,0:T(8,128)(2,1)S(1)}, u32[]{:S(2)}, u32[]{:S(2)}) collective-permute-start(bf16[304,256]{1,0:T(8,128)(2,1)S(1)} %get-tuple-element.73), channel_id=1, source_target_pairs={{0,16},{4,20},{8,24},{12,28},{16,0},{20,4},{24,8},{28,12},{1,17},{... | collective-permute-start | bytes 466952 | tf_op jit(solution)/shard_map/ppermute | solution.py:31
  105.3 20.3 %collective-permute-start.12 = (bf16[256,256]{1,0:T(8,128)(2,1)S(1)}, bf16[256,256]{1,0:T(8,128)(2,1)S(1)}, u32[]{:S(2)}, u32[]{:S(2)}) collective-permute-start(bf16[256,256]{1,0:T(8,128)(2,1)S(1)} %get-tuple-element.65), channel_id=1, source_target_pairs={{0,8},{4,12},{8,16},{12,20},{16,24},{20,28},{24,0},{28,4},{1,9},{5... | collective-permute-start | bytes 393224 | tf_op jit(solution)/shard_map/ppermute | solution.py:31
  108.9 18.0 %collective-permute-start.13 = (bf16[256,256]{1,0:T(8,128)(2,1)S(1)}, bf16[256,256]{1,0:T(8,128)(2,1)S(1)}, u32[]{:S(2)}, u32[]{:S(2)}) collective-permute-start(bf16[256,256]{1,0:T(8,128)(2,1)S(1)} %get-tuple-element.64), channel_id=1, source_target_pairs={{0,16},{4,20},{8,24},{12,28},{16,0},{20,4},{24,8},{28,12},{1,17},{... | collective-permute-start | bytes 393224 | tf_op jit(solution)/shard_map/ppermute | solution.py:31
  108.9 18.0 %collective-permute-start.14 = (bf16[256,256]{1,0:T(8,128)(2,1)S(1)}, bf16[256,256]{1,0:T(8,128)(2,1)S(1)}, u32[]{:S(2)}, u32[]{:S(2)}) collective-permute-start(bf16[256,256]{1,0:T(8,128)(2,1)S(1)} %get-tuple-element.63), channel_id=1, source_target_pairs={{0,24},{4,28},{8,0},{12,4},{16,8},{20,12},{24,16},{28,20},{1,25},{... | collective-permute-start | bytes 393224 | tf_op jit(solution)/shard_map/ppermute | solution.py:31
  111.3 14.3 %collective-permute-start.16 = (bf16[304,256]{1,0:T(8,128)(2,1)S(1)}, bf16[304,256]{1,0:T(8,128)(2,1)S(1)}, u32[]{:S(2)}, u32[]{:S(2)}) collective-permute-start(bf16[304,256]{1,0:T(8,128)(2,1)S(1)} %get-tuple-element.74), channel_id=1, source_target_pairs={{0,8},{4,12},{8,16},{12,20},{16,24},{20,28},{24,0},{28,4},{1,9},{5... | collective-permute-start | bytes 466952 | tf_op jit(solution)/shard_map/ppermute | solution.py:31
  124.1 18.3 %collective-permute-start.10 = (bf16[1024,512]{1,0:T(8,128)(2,1)S(1)}, bf16[1024,512]{1,0:T(8,128)(2,1)S(1)}, u32[]{:S(2)}, u32[]{:S(2)}) collective-permute-start(bf16[1024,512]{1,0:T(8,128)(2,1)S(1)} %input_block.7), channel_id=1, source_target_pairs={{0,2},{1,3},{2,0},{3,1},{4,6},{5,7},{6,4},{7,5},{8,10},{9,11},{10,... | collective-permute-start | bytes 3145736 | tf_op jit(solution)/shard_map/ppermute | solution.py:31

commit v2 on v1

--- a/solution.py
+++ b/solution.py
@@ -185,26 +185,23 @@
 
 
 def project_kernel(
-    x_hbm, wv_hbm, wg_hbm, g_hbm, wp_hbm, v_hbm, s_hbm, u_out, m_hbm, x_buf, g_buf, wv_buf, wg_buf, wp_buf, v_out, s_out, m_out, sems
+    x_hbm, wv_hbm, wg_hbm, g_hbm, wp_hbm, v_hbm, s_hbm, u_out, m_out, x_buf, g_buf, wv_buf, wg_buf, wp_buf, v_out, s_out, sems
 ):
     count, block, _ = x_buf.shape
-
-    def copies(at, hbm, buf):
-        return [
-            pltpu.make_async_copy(hbm.at[pl.ds(k * block, block), :], buf.at[k], sems.at[at, k])
-            for k in range(count)
-        ]
-
     weights = [
-        pltpu.make_async_copy(hbm, buf, sems.at[2, k])
+        pltpu.make_async_copy(hbm, buf, sems.at[1, k])
         for k, (hbm, buf) in enumerate(((wv_hbm, wv_buf), (wg_hbm, wg_buf), (wp_hbm, wp_buf)))
     ]
-    inputs = copies(0, x_hbm, x_buf)
-    grads = copies(1, g_hbm, g_buf)
-    for copy in weights[:2] + inputs + weights[2:] + grads:
+    edge = pltpu.make_async_copy(g_hbm.at[pl.ds(0, HALO), :], g_buf, sems.at[2, 0])
+    inputs = [
+        pltpu.make_async_copy(x_hbm.at[pl.ds(k * block, block), :], x_buf.at[k], sems.at[0, k])
+        for k in range(count)
+    ]
+    for copy in weights[:2] + inputs + weights[2:] + [edge]:
         copy.start()
     weights[0].wait()
     weights[1].wait()
+    leaving = []
     for k in range(count):
         inputs[k].wait()
         rows = pl.ds(k * block, block)
@@ -213,19 +210,12 @@
         v_out[rows, :] = v
         s_out[rows, :] = s
         u_out[rows, :] = (v.astype(f32) * jax.nn.sigmoid(s.astype(f32))).astype(bf16)
-    leaving = [
-        pltpu.make_async_copy(v_out, v_hbm, sems.at[3, 0]),
-        pltpu.make_async_copy(s_out, s_hbm, sems.at[3, 1]),
-    ]
-    for copy in leaving:
-        copy.start()
+        for at, (buf, hbm) in enumerate(((v_out, v_hbm), (s_out, s_hbm))):
+            leaving.append(pltpu.make_async_copy(buf.at[rows, :], hbm.at[rows, :], sems.at[3 + at, k]))
+            leaving[-1].start()
     weights[2].wait()
-    for k in range(count):
-        grads[k].wait()
-        rows = pl.ds(k * block, block)
-        m_out[rows, :] = right_product(g_buf[k], wp_buf[...])
-        leaving.append(pltpu.make_async_copy(m_out.at[rows, :], m_hbm.at[rows, :], sems.at[4, k]))
-        leaving[-1].start()
+    edge.wait()
+    m_out[...] = right_product(g_buf[...], wp_buf[...])
     for copy in leaving:
         copy.wait()
 
@@ -237,39 +227,49 @@
     return pl.pallas_call(
         project_kernel,
         in_specs=[hbm] * 5,
-        out_specs=[HBM_SPEC] * 2 + [VMEM_SPEC, HBM_SPEC],
-        out_shape=[pltpu.HBM((t, c), bf16)] * 2 + [jax.ShapeDtypeStruct((t, c), bf16), pltpu.HBM((t, c), f32)],
+        out_specs=[HBM_SPEC] * 2 + [VMEM_SPEC] * 2,
+        out_shape=[pltpu.HBM((t, c), bf16)] * 2
+        + [jax.ShapeDtypeStruct((t, c), bf16), jax.ShapeDtypeStruct((HALO, c), f32)],
         scratch_shapes=[
             pltpu.VMEM((count, t // count, d), bf16),
-            pltpu.VMEM((count, t // count, d), bf16),
+            pltpu.VMEM((HALO, d), bf16),
             pltpu.VMEM((d, c), bf16),
             pltpu.VMEM((d, c), bf16),
             pltpu.VMEM((c, d), bf16),
             pltpu.VMEM((t, c), bf16),
             pltpu.VMEM((t, c), bf16),
-            pltpu.VMEM((t, c), f32),
             pltpu.SemaphoreType.DMA((5, max(3, count))),
         ],
-        compiler_params=limit(20),
+        compiler_params=limit(16),
         cost_estimate=pl.CostEstimate(
-            flops=6 * t * d * c, transcendentals=t * c, bytes_accessed=2 * (2 * t * d + 3 * d * c + 5 * t * c)
+            flops=4 * t * d * c, transcendentals=t * c, bytes_accessed=2 * (t * d + 3 * d * c + 3 * t * c)
         ),
         name="project",
     )(*(in_hbm(a) for a in (x, wv, wg, g, wp)))
 
 
+def back_kernel(g_ref, w_ref, out_ref):
+    out_ref[...] = right_product(g_ref[...], w_ref[...])
+
+
+def back_project(g, w):
+    t, d = g.shape
+    c = w.shape[0]
+    return pl.pallas_call(
+        back_kernel,
+        in_specs=[VMEM_SPEC, VMEM_SPEC],
+        out_specs=VMEM_SPEC,
+        out_shape=jax.ShapeDtypeStruct((t, c), f32),
+        compiler_params=limit(8),
+        cost_estimate=pl.CostEstimate(
+            flops=2 * t * d * c, transcendentals=0, bytes_accessed=2 * t * d + 2 * d * c + 4 * t * c
+        ),
+        name="back_project",
+    )(g, w)
+
+
 def chunk_of(rows, most):
     return max(c for c in range(16, most + 1, 16) if rows % c == 0)
-
-
-def fill_extended(ext_ref, before, glu, after, tok):
-    ext_ref[pl.ds(0, HALO), :] = before.astype(f32)
-    ext_ref[pl.ds(HALO, tok), :] = glu.astype(f32)
-    ext_ref[pl.ds(HALO + tok, HALO), :] = after
-
-
-def tap_rows(taps_ref, taps):
-    return [jnp.broadcast_to(taps_ref[pl.ds(k, 1), :], (8, LANE)) for k in range(taps)]
 
 
 def conv_rows(ext_ref, weights, base, chunk):
@@ -285,36 +285,39 @@
     return acc
 
 
+def tap_rows(taps_ref, cols):
+    return [jnp.broadcast_to(taps_ref[pl.ds(k, 1), cols], (8, LANE)) for k in range(taps_ref.shape[0])]
+
+
 def conv_kernel(glu_ref, taps_ref, out_ref, wide_ref):
-    tok = glu_ref.shape[0]
+    tok, ch = glu_ref.shape
     rows = tok - HALO
     chunk = chunk_of(rows, 96)
-    wide_ref[...] = glu_ref[...].astype(f32)
-    weights = tap_rows(taps_ref, taps_ref.shape[0])
-
-    def step(i, carry):
-        base = pl.multiple_of(i * chunk, chunk)
-        for j, part in enumerate(conv_rows(wide_ref, weights, base, chunk)):
-            out_ref[pl.ds(base + HALO + 8 * j, 8), :] = part
-        return carry
-
-    lax.fori_loop(0, rows // chunk, step, 0)
+    for h in range(ch // LANE):
+        cols = pl.ds(h * LANE, LANE)
+        wide_ref[...] = glu_ref[:, cols].astype(f32)
+        weights = tap_rows(taps_ref, cols)
+
+        def step(i, carry):
+            base = pl.multiple_of(i * chunk, chunk)
+            for j, part in enumerate(conv_rows(wide_ref, weights, base, chunk)):
+                out_ref[pl.ds(base + HALO + 8 * j, 8), cols] = part
+            return carry
+
+        lax.fori_loop(0, rows // chunk, step, 0)
 
 
 def convolve(glu, conv_taps):
     tok, ch = glu.shape
-    taps = conv_taps.shape[0]
-    column = lambda i: (0, i)
     return pl.pallas_call(
         conv_kernel,
-        grid=(ch // LANE,),
-        in_specs=[pl.BlockSpec((tok, LANE), column), pl.BlockSpec((taps, LANE), column)],
-        out_specs=pl.BlockSpec((tok + HALO, LANE), column),
+        in_specs=[VMEM_SPEC, VMEM_SPEC],
+        out_specs=VMEM_SPEC,
         out_shape=jax.ShapeDtypeStruct((tok + HALO, ch), f32),
         scratch_shapes=[pltpu.VMEM((tok, LANE), f32)],
         compiler_params=limit(6),
         cost_estimate=pl.CostEstimate(
-            flops=20 * taps * tok * ch, transcendentals=0, bytes_accessed=6 * tok * ch
+            flops=20 * conv_taps.shape[0] * tok * ch, transcendentals=0, bytes_accessed=6 * tok * ch
         ),
         name="convolve",
     )(glu, conv_taps)
@@ -325,7 +328,7 @@
     rows = main_ref.shape[0]
     for h in range(ch // LANE):
         cols = pl.ds(h * LANE, LANE)
-        weights = [jnp.broadcast_to(taps_ref[pl.ds(k, 1), cols], (8, LANE)) for k in range(taps_ref.shape[0])]
+        weights = tap_rows(taps_ref, cols)
         for m, (first, second) in enumerate(((before_ref, head_ref), (tail_ref, after_ref))):
             ext_ref[pl.ds(0, HALO), :] = first[:, cols].astype(f32)
             ext_ref[pl.ds(HALO, HALO), :] = second[pl.ds(0, HALO), cols].astype(f32)
@@ -359,7 +362,7 @@
 
 
 def act_kernel(
-    filtered_ref, stats_ref, mixed_ref, edge_ref, gain_ref, shift_ref,
+    filtered_ref, stats_ref, mixed_ref, after_ref, gain_ref, shift_ref,
     normed_ref, grad_ref, turned_ref, sums_ref, col_ref, out_ref,
 ):
     ch = filtered_ref.shape[1]
@@ -400,7 +403,7 @@
 
     zero = jnp.zeros((8, LANE), f32)
     sums = lax.fori_loop(0, tok // chunk, step, (zero,) * (2 * (ch // LANE)))
-    some_rows(tok, HALO, edge_ref[...], False)
+    some_rows(tok, HALO, after_ref[pl.ds(HALO, HALO), :], False)
     sums_ref[...] = jnp.zeros_like(sums_ref)
     for h in range(ch // LANE):
         for m in range(2):
@@ -413,24 +416,10 @@
     rows, ch = filtered.shape
     tok = mixed.shape[0]
     wide = stats.shape[1]
-    whole = lambda i: (0, 0)
     return pl.pallas_call(
         act_kernel,
-        grid=(1,),
-        in_specs=[
-            pl.BlockSpec((rows, ch), whole),
-            pl.BlockSpec((8, wide), whole),
-            pl.BlockSpec((tok, ch), whole),
-            pl.BlockSpec((HALO, ch), lambda i: (1, 0)),
-            pl.BlockSpec((1, ch), whole),
-            pl.BlockSpec((1, ch), whole),
-        ],
-        out_specs=[
-            pl.BlockSpec((rows, ch), whole),
-            pl.BlockSpec((rows, ch), whole),
-            pl.BlockSpec((ch, tok), whole),
-            pl.BlockSpec((16, ch), whole),
-        ],
+        in_specs=[VMEM_SPEC] * 6,
+        out_specs=[VMEM_SPEC] * 4,
         out_shape=[
             jax.ShapeDtypeStruct((rows, ch), f32),
             jax.ShapeDtypeStruct((rows, ch), f32),
@@ -447,15 +436,24 @@
 
 
 def back_conv_kernel(
-    normed_ref, gn_ref, stats_ref, before_ref, glu_ref, after_ref, v_ref, s_ref, taps_ref,
-    out_ref, turned_out, small_ref, ext_ref, grad_ref, col_ref, *leave,
+    normed_ref, gn_ref, stats_ref, before_ref, glu_ref, after_ref, v_hbm, s_hbm, taps_ref,
+    out_ref, turned_out, small_ref, ext_ref, grad_ref, col_ref, v_ref, s_ref, sems, *leave, h,
 ):
     turned_ref = leave[0] if leave else turned_out
     tok = glu_ref.shape[0]
     rows = tok + HALO
     taps = taps_ref.shape[0]
+    cols = pl.ds(h * LANE, LANE)
+    coming = [
+        pltpu.make_async_copy(hbm.at[:, cols], ref, sems.at[m])
+        for m, (hbm, ref) in enumerate(((v_hbm, v_ref), (s_hbm, s_ref)))
+    ]
+    for copy in coming:
+        copy.start()
     col_ref[...] = stats_ref[...].T
-    fill_extended(ext_ref, before_ref[...], glu_ref[...], after_ref[...], tok)
+    ext_ref[pl.ds(0, HALO), :] = before_ref[:, cols].astype(f32)
+    ext_ref[pl.ds(HALO, tok), :] = glu_ref[:, cols].astype(f32)
+    ext_ref[pl.ds(HALO + tok, HALO), :] = after_ref[pl.ds(0, HALO), cols]
     part_rows = chunk_of(rows, 96)
 
     def filtered_grad(i, carry):
@@ -463,12 +461,14 @@
         scale, first, second = (
             jnp.broadcast_to(col_ref[here, pl.ds(m, 1)], (part_rows, LANE)) for m in range(3)
         )
-        grad_ref[here, :] = scale * (gn_ref[here, :] - first - normed_ref[here, :] * second)
+        grad_ref[here, :] = scale * (gn_ref[here, cols] - first - normed_ref[here, cols] * second)
         return carry
 
     lax.fori_loop(0, rows // part_rows, filtered_grad, 0)
-    weights = tap_rows(taps_ref, taps)
-    chunk = chunk_of(tok, 64)
+    for copy in coming:
+        copy.wait()
+    weights = tap_rows(taps_ref, cols)
+    chunk = chunk_of(tok, 128)
 
     def spread(i, carry):
         base = pl.multiple_of(i * chunk, chunk)
@@ -496,7 +496,7 @@
         leaving = pltpu.make_async_copy(turned_ref, turned_out, leave[1])
         leaving.start()
 
-    width = chunk_of(tok, 32)
+    width = chunk_of(tok, 128)
 
     def gather(i, sums):
         base = pl.multiple_of(i * width, width)
@@ -525,28 +525,12 @@
     tok, _ = glu.shape
     taps = conv_taps.shape[0]
     wide = stats.shape[1]
-    column = lambda i: (0, h)
-    first = lambda i: (0, 0)
     kept = -(-taps // 8) * 8
-    return pl.pallas_call(
-        back_conv_kernel,
-        grid=(1,),
-        in_specs=[
-            pl.BlockSpec((tok + HALO, LANE), column),
-            pl.BlockSpec((tok + HALO, LANE), column),
-            pl.BlockSpec((8, wide), first),
-            pl.BlockSpec((HALO, LANE), column),
-            pl.BlockSpec((tok, LANE), column),
-            pl.BlockSpec((HALO, LANE), column),
-            pl.BlockSpec((tok, LANE), column),
-            pl.BlockSpec((tok, LANE), column),
-            pl.BlockSpec((taps, LANE), column),
-        ],
-        out_specs=[
-            pl.BlockSpec((tok, 2 * LANE), first),
-            HBM_SPEC if leave else pl.BlockSpec((2 * LANE, tok), first),
-            pl.BlockSpec((kept, LANE), first),
-        ],
+    hbm = pl.BlockSpec(memory_space=pl.ANY)
+    return pl.pallas_call(
+        functools.partial(back_conv_kernel, h=h),
+        in_specs=[VMEM_SPEC] * 6 + [hbm] * 2 + [VMEM_SPEC],
+        out_specs=[VMEM_SPEC, HBM_SPEC if leave else VMEM_SPEC, VMEM_SPEC],
         out_shape=[
             jax.ShapeDtypeStruct((tok, 2 * LANE), bf16),
             (pltpu.HBM if leave else jax.ShapeDtypeStruct)((2 * LANE, tok), bf16),
@@ -556,6 +540,9 @@
             pltpu.VMEM((tok + 2 * HALO, LANE), f32),
             pltpu.VMEM((tok + HALO, LANE), f32),
             pltpu.VMEM((wide, 8), f32),
+            pltpu.VMEM((tok, LANE), bf16),
+            pltpu.VMEM((tok, LANE), bf16),
+            pltpu.SemaphoreType.DMA((2,)),
         ]
         + ([pltpu.VMEM((2 * LANE, tok), bf16), pltpu.SemaphoreType.DMA] if leave else []),
         compiler_params=limit(12),
@@ -673,16 +660,17 @@
     n_sp = lax.axis_size("sp")
     channels = ch * n_tp
     loss_scale = 1.0 / math.sqrt(tok * n_sp)
-    value_proj, gate_proj, gated_input, own_mixed = project(
+    value_proj, gate_proj, gated_input, edge_mixed = project(
         block_input, w_value, w_gate, out_grad, w_proj, 4
     )
-    after = send(jnp.concatenate([gated_input[:HALO].astype(f32), own_mixed[:HALO]], axis=0), "sp", lambda i: i - 1)
+    after = send(jnp.concatenate([gated_input[:HALO].astype(f32), edge_mixed], axis=0), "sp", lambda i: i - 1)
     before = send(gated_input[tok - HALO :], "sp", lambda i: i + 1)
     pair_value = send(w_value, "tp", lambda i: i ^ 1)
     pair_gate = send(w_gate, "tp", lambda i: i ^ 1)
     inner = convolve(gated_input, conv_taps)
     filtered = convolve_ends(inner, before, gated_input, after, conv_taps)
     stats = all_sum(row_sums(filtered, filtered * filtered), "tp")
+    own_mixed = back_project(out_grad, w_proj)
     row_mean = stats[0] / channels
     row_scale = lax.rsqrt(stats[1] / channels - row_mean * row_mean + EPS)
     normed, grad_normed, turned, edge_sums = activate(
@@ -698,7 +686,7 @@
     small = []
     for h in range(halves):
         grad, turn, tap_sums = back_convolve(
-            normed, grad_normed, stats, before, gated_input, after, value_proj, gate_proj, conv_taps, h, h > 0
+            normed, grad_normed, stats, before, gated_input, after, value_proj, gate_proj, conv_taps, h, False
         )
         grads.append(grad)
         pair_grads.append(send(grad, "tp", lambda i: i ^ 1))

time: 144 us -> 141 us (0.979)
  Pallas kernels: 38.2 us -> 35.5 us
  local copies, waits for them, and re-layouts: 5.31 us -> 7.33 us
  starting transfers between devices: 38.3 us -> 36.6 us
    unnamed x46, local copies, waits for them, and re-layouts: 4.48 us -> 7.27 us
    pallas_call x1, Pallas kernels: 8.52 us -> 5.8 us  [project(): pl.pallas_call(project_kernel, in_specs=[hbm] * 5, out_specs=[HBM_SPEC] *...]
    ppermute x23, starting transfers between devices: 38.3 us -> 36.6 us  [send(): return lax.ppermute(block, axis, route)]
    pallas_call x4 -> x5, Pallas kernels: 17.5 us -> 17.5 us  [the longest x2 10.1 us: back_convolve(): pl.pallas_call(functools.partial(back_conv_kernel, h=h), in_specs=[VMEM_S...]
  transfers between devices with their start and end apart: 23 -> 23, of which waited for: 10 -> 9; matrix products, arithmetic and copies ran while one was open for 5% -> 5% of each run, Pallas kernels for 9% -> 10%
where the time goes in v2:
time: 141 us
  waiting for transfers between devices  51.4 us (36%)
  starting transfers between devices  36.6 us (26%)
  Pallas kernels  35.5 us (25%)
  other arithmetic  8.8 us (6%)
  local copies, waits for them, and re-layouts  7.33 us (5%)
    ppermute x23, waiting for transfers between devices, send(): return lax.ppermute(block, axis, route)  51.4 us
    ppermute x23, starting transfers between devices, send(): return lax.ppermute(block, axis, route)  36.6 us
    pallas_call x2, Pallas kernels, back_convolve(): pl.pallas_call(functools.partial(back_conv_kernel, h=h), in_specs=[VMEM_S...  10.1 us
    pallas_call x3, Pallas kernels, grad_blocks(): pl.pallas_call(functools.partial(blocks_kernel, gives=gives), in_specs=[S...  7.94 us
    unnamed x46, local copies, waits for them, and re-layouts  7.27 us
    pallas_call x1, Pallas kernels, project(): pl.pallas_call(project_kernel, in_specs=[hbm] * 5, out_specs=[HBM_SPEC] *...  5.8 us
    pallas_call x1, Pallas kernels, convolve(): pl.pallas_call(conv_kernel, in_specs=[VMEM_SPEC, VMEM_SPEC], out_specs=VM...  3.74 us
    pallas_call x4, Pallas kernels, input_block(): pl.pallas_call(functools.partial(input_kernel, halves=len(grads), fetch=f...  3.08 us
  transfers between devices with their start and end apart: 23, of which 9 were waited for; matrix products, arithmetic and copies ran while one was open for 5% of the time, Pallas kernels for 10%

profile of v2, /device:TPU:0, one launch (start us, length us, event | category | flops | bytes accessed | tf_op | source)
XLA Modules:
  0.0 140.9 jit_solution(6574200349249283356)
XLA Ops:
  0.6 5.8 %project.1 = (bf16[1024,256]{1,0:T(8,128)(2,1)}, bf16[1024,256]{1,0:T(8,128)(2,1)}, bf16[1024,256]{1,0:T(8,128)(2,1)S(1)}, f32[32,256]{1,0:T(8,128)S(1)}) custom-call(bf16[1024,2048]{1,0:T(8,128)(2,1)} %right_ref.4, bf16[2048,256]{1,0:T(8,128)(2,1)} %refs_2_.3, bf16[2048,256]{1,0:T(8,128)(2,1)} %refs_3_.3, bf16[1024,2048]{1,0:T(8,128)(2,1)} %right_ref.5, ...), custom_call_target="tpu_custom_call" | custom-call | flops 2147483648 | bytes 8912896 | tf_op jit(solution)/shard_map/project/pallas_call | solution.py:227
  6.5 1.3 collective-permute-start.1
  7.8 5.5 %collective-permute-start = (bf16[32,256]{1,0:T(8,128)(2,1)S(1)}, bf16[32,256]{1,0:T(8,128)(2,1)S(1)}, u32[]{:S(2)}, u32[]{:S(2)}) collective-permute-start(bf16[32,256]{1,0:T(8,128)(2,1)S(1)} %get-tuple-element.69.tail_ref), channel_id=1, source_target_pairs={{0,4},{4,8},{8,12},{12,16},{16,20},{20,24},{24,28},{1,5},{5,9},{9,... | collective-permute-start | bytes 49160 | tf_op jit(solution)/shard_map/ppermute | solution.py:31
  13.4 3.7 %convolve.1.main_ref = f32[1056,256]{1,0:T(8,128)S(1)} custom-call(bf16[1024,256]{1,0:T(8,128)(2,1)S(1)} %get-tuple-element.31.glu_ref, f32[31,256]{1,0:T(8,128)S(1)} %copy-done.15), custom_call_target="tpu_custom_call" | custom-call | flops 162529280 | bytes 1572864 | tf_op jit(solution)/shard_map/convolve/pallas_call | solution.py:312
  18.0 1.1 collective-permute-done.2
  19.1 2.1 %collective-permute-start.3 = (f32[2,1152]{1,0:T(2,128)S(1)}, f32[2,1152]{1,0:T(2,128)S(1)}, u32[]{:S(2)}, u32[]{:S(2)}) collective-permute-start(f32[2,1152]{1,0:T(2,128)S(1)} %fusion.4), channel_id=1, source_target_pairs={{0,2},{1,3},{2,0},{3,1},{4,6},{5,7},{6,4},{7,5},{8,10},{9,11},{10,... | collective-permute-start | bytes 27656 | tf_op jit(solution)/shard_map/ppermute | solution.py:31
  21.2 1.2 copy-done.6
  22.4 1.3 back_project.1.mixed_ref
  23.8 2.4 %activate.1 = (f32[1056,256]{1,0:T(8,128)S(1)}, f32[1056,256]{1,0:T(8,128)S(1)}, bf16[256,1024]{1,0:T(8,128)(2,1)S(1)}, f32[16,256]{1,0:T(8,128)S(1)}) custom-call(f32[1056,256]{1,0:T(8,128)S(1)} %convolve_ends.1.filtered_ref, f32[8,1152]{1,0:T(8,128)S(1)} %select_maximum_fusion.1.stats_ref, f32[1024,256]{1,0:T(8,128)S(1)} %back_project.1.mixed_ref, ...), custom_call_target="tpu_custom_call" | custom-call | flops 52428800 | bytes 4718592 | tf_op jit(solution)/shard_map/activate/pallas_call | solution.py:419
  26.8 1.1 collective-permute-done.4
  28.0 1.2 collective-permute-start.5
  29.2 2.5 %collective-permute-done.5 = f32[2,1152]{1,0:T(2,128)S(1)} collective-permute-done((f32[2,1152]{1,0:T(2,128)S(1)}, f32[2,1152]{1,0:T(2,128)S(1)}, u32[]{:S(2)}, u32[]{:S(2)}) %collective-permute-start.5) | collective-permute-done | bytes 9248 | tf_op jit(solution)/shard_map/ppermute | solution.py:31
  31.8 5.0 %back_convolve.3 = (bf16[1024,256]{1,0:T(8,128)(2,1)S(1)}, bf16[256,1024]{1,0:T(8,128)(2,1)S(1)}, f32[32,128]{1,0:T(8,128)S(1)}) custom-call(f32[1056,256]{1,0:T(8,128)S(1)} %get-tuple-element.33.normed_ref, f32[1056,256]{1,0:T(8,128)S(1)} %get-tuple-element.34.gn_ref, f32[8,1152]{1,0:T(8,128)S(1)} %select_maximum_fusion.stats_ref, ...), custom_call_target="tpu_custom_call" | custom-call | flops 162529280 | bytes 2097152 | tf_op jit(solution)/shard_map/back_convolve/pallas_call | solution.py:530
  36.8 0.8 copy-done.12
  37.6 5.0 %back_convolve.2 = (bf16[1024,256]{1,0:T(8,128)(2,1)S(1)}, bf16[256,1024]{1,0:T(8,128)(2,1)S(1)}, f32[32,128]{1,0:T(8,128)S(1)}) custom-call(f32[1056,256]{1,0:T(8,128)S(1)} %get-tuple-element.33.normed_ref, f32[1056,256]{1,0:T(8,128)S(1)} %get-tuple-element.34.gn_ref, f32[8,1152]{1,0:T(8,128)S(1)} %select_maximum_fusion.stats_ref, ...), custom_call_target="tpu_custom_call" | custom-call | flops 162529280 | bytes 2097152 | tf_op jit(solution)/shard_map/back_convolve/pallas_call | solution.py:530
  42.6 0.8 copy-done.9
  43.4 0.8 copy-done.16
  44.3 2.9 %grad_blocks.4 = (bf16[1072,256]{1,0:T(8,128)(2,1)}, f32[4,256,256]{2,1,0:T(8,128)}) custom-call(s32[8]{0:T(128)S(1)} %pad_add_fusion.ids_ref, bf16[256,1024]{1,0:T(8,128)(2,1)S(1)} %get-tuple-element.42.left_ref, bf16[1024,2048]{1,0:T(8,128)(2,1)S(1)} %copy-done.2, bf16[48,256]{1,0:T(8,128)(2,1)S(1)} %pad_maximum_fusion.4.refs_0_), custom_call_target="tpu_custom_call" | custom-call | flops 1073741824 | bytes 6815744 | tf_op jit(solution)/shard_map/grad_blocks/pallas_call | solution.py:101
  47.2 2.5 %collective-permute-start.15 = (bf16[1072,256]{1,0:T(8,128)(2,1)}, bf16[1072,256]{1,0:T(8,128)(2,1)}, u32[]{:S(2)}, u32[]{:S(2)}) collective-permute-start(bf16[1072,256]{1,0:T(8,128)(2,1)} %get-tuple-element.47), channel_id=1, source_target_pairs={{0,4},{4,0},{8,12},{12,8},{16,20},{20,16},{24,28},{28,24},{1,5},{5... | collective-permute-start | bytes 1646600 | tf_op jit(solution)/shard_map/ppermute | solution.py:31
  49.8 2.7 %grad_blocks.5 = (bf16[512,256]{1,0:T(8,128)(2,1)}, bf16[512,256]{1,0:T(8,128)(2,1)}, bf16[512,256]{1,0:T(8,128)(2,1)S(1)}, f32[2,256,256]{2,1,0:T(8,128)}) custom-call(s32[8]{0:T(128)S(1)} %pad_add_fusion.1.ids_ref, bf16[256,1024]{1,0:T(8,128)(2,1)S(1)} %get-tuple-element.50.left_ref, bf16[1024,2048]{1,0:T(8,128)(2,1)S(1)} %copy-done.1), custom_call_target="tpu_custom_call" | custom-call | flops 1073741824 | bytes 6815744 | tf_op jit(solution)/shard_map/grad_blocks/pallas_call | solution.py:101
  52.4 1.6 %collective-permute-start.19 = (bf16[512,256]{1,0:T(8,128)(2,1)}, bf16[512,256]{1,0:T(8,128)(2,1)}, u32[]{:S(2)}, u32[]{:S(2)}) collective-permute-start(bf16[512,256]{1,0:T(8,128)(2,1)} %get-tuple-element.52), channel_id=1, source_target_pairs={{0,8},{4,12},{8,16},{12,20},{16,24},{20,28},{24,0},{28,4},{1,9},{5... | collective-permute-start | bytes 786440 | tf_op jit(solution)/shard_map/ppermute | solution.py:31
  54.1 1.1 collective-permute-start.20
  55.2 2.8 %collective-permute-start.21 = (bf16[512,256]{1,0:T(8,128)(2,1)S(1)}, bf16[512,256]{1,0:T(8,128)(2,1)}, u32[]{:S(2)}, u32[]{:S(2)}) collective-permute-start(bf16[512,256]{1,0:T(8,128)(2,1)S(1)} %get-tuple-element.54), channel_id=1, source_target_pairs={{0,24},{4,28},{8,0},{12,4},{16,8},{20,12},{24,16},{28,20},{1,25},{... | collective-permute-start | bytes 786440 | tf_op jit(solution)/shard_map/ppermute | solution.py:31
  58.0 1.0 copy-done.10
  59.1 1.0 copy-done.13
  60.9 0.7 input_block.6.refs_4_
  61.6 1.4 %copy-done.3 = bf16[1024,2048]{1,0:T(8,128)(2,1)S(1)} copy-done((bf16[1024,2048]{1,0:T(8,128)(2,1)S(1)}, bf16[1024,2048]{1,0:T(8,128)(2,1)}, u32[]{:S(2)}) %copy-start.3) | copy-done | bytes 4194328
  63.2 2.4 %grad_blocks.3 = (bf16[1024,256]{1,0:T(8,128)(2,1)S(1)}, f32[4,256,256]{2,1,0:T(8,128)}) custom-call(s32[8]{0:T(128)S(1)} %pad_add_fusion.ids_ref, bf16[256,1024]{1,0:T(8,128)(2,1)S(1)} %copy-done.17, bf16[1024,2048]{1,0:T(8,128)(2,1)S(1)} %copy-done.3), custom_call_target="tpu_custom_call" | custom-call | flops 1073741824 | bytes 6815744 | tf_op jit(solution)/shard_map/grad_blocks/pallas_call | solution.py:101
  66.1 6.8 %collective-permute-done.20 = bf16[512,256]{1,0:T(8,128)(2,1)} collective-permute-done((bf16[512,256]{1,0:T(8,128)(2,1)}, bf16[512,256]{1,0:T(8,128)(2,1)}, u32[]{:S(2)}, u32[]{:S(2)}) %collective-permute-start.20) | collective-permute-done | bytes 262176 | tf_op jit(solution)/shard_map/ppermute | solution.py:31
  73.3 1.1 add_convert_fusion.1
  74.4 1.8 %collective-permute-start.22 = (bf16[256,256]{1,0:T(8,128)(2,1)S(1)}, bf16[256,256]{1,0:T(8,128)(2,1)S(1)}, u32[]{:S(2)}, u32[]{:S(2)}) collective-permute-start(bf16[256,256]{1,0:T(8,128)(2,1)S(1)} %add_convert_fusion.1), channel_id=1, source_target_pairs={{0,4},{4,0},{8,12},{12,8},{16,20},{20,16},{24,28},{28,24},{1,5},{5... | collective-permute-start | bytes 393224 | tf_op jit(solution)/shard_map/ppermute | solution.py:31
  76.2 0.7 add_convert_fusion.8
  77.0 1.3 add_convert_fusion.2
  78.3 11.7 %collective-permute-done.22 = bf16[256,256]{1,0:T(8,128)(2,1)S(1)} collective-permute-done((bf16[256,256]{1,0:T(8,128)(2,1)S(1)}, bf16[256,256]{1,0:T(8,128)(2,1)S(1)}, u32[]{:S(2)}, u32[]{:S(2)}) %collective-permute-start.22) | collective-permute-done | bytes 131104 | tf_op jit(solution)/shard_map/ppermute | solution.py:31
  90.1 7.2 %collective-permute-start.18 = (bf16[304,256]{1,0:T(8,128)(2,1)S(1)}, bf16[304,256]{1,0:T(8,128)(2,1)S(1)}, u32[]{:S(2)}, u32[]{:S(2)}) collective-permute-start(bf16[304,256]{1,0:T(8,128)(2,1)S(1)} %get-tuple-element.72), channel_id=1, source_target_pairs={{0,24},{4,28},{8,0},{12,4},{16,8},{20,12},{24,16},{28,20},{1,25},{... | collective-permute-start | bytes 466952 | tf_op jit(solution)/shard_map/ppermute | solution.py:31
  97.3 1.8 %add_multiply_fusion = f32[256,256]{1,0:T(8,128)} fusion(bf16[256,256]{1,0:T(8,128)(2,1)S(1)} %collective-permute-done.22, f32[512,256]{1,0:T(8,128)S(1)} %bitcast.23, s32[]{:T(128)S(6)} %select_n.164, bf16[512,256]{1,0:T(8,128)(2,1)} %collective-permute-done.21, bf16[512,256]{1,0:T(8,128)(2,1)} %collective-permute-done.20, ...), kind=kLoop, calls=%fused_computation.3 | loop fusion | flops 589824 | bytes 1048580 | tf_op jit(solution)/shard_map/mul | solution.py:701
  99.3 1.9 %collective-permute-done.18 = bf16[304,256]{1,0:T(8,128)(2,1)S(1)} collective-permute-done((bf16[304,256]{1,0:T(8,128)(2,1)S(1)}, bf16[304,256]{1,0:T(8,128)(2,1)S(1)}, u32[]{:S(2)}, u32[]{:S(2)}) %collective-permute-start.18) | collective-permute-done | bytes 155680 | tf_op jit(solution)/shard_map/ppermute | solution.py:31
  101.2 1.3 collective-permute-start.17
  102.5 3.5 %collective-permute-start.12 = (bf16[256,256]{1,0:T(8,128)(2,1)S(1)}, bf16[256,256]{1,0:T(8,128)(2,1)S(1)}, u32[]{:S(2)}, u32[]{:S(2)}) collective-permute-start(bf16[256,256]{1,0:T(8,128)(2,1)S(1)} %get-tuple-element.65), channel_id=1, source_target_pairs={{0,8},{4,12},{8,16},{12,20},{16,24},{20,28},{24,0},{28,4},{1,9},{5... | collective-permute-start | bytes 393224 | tf_op jit(solution)/shard_map/ppermute | solution.py:31
  106.1 2.4 %collective-permute-start.14 = (bf16[256,256]{1,0:T(8,128)(2,1)S(1)}, bf16[256,256]{1,0:T(8,128)(2,1)S(1)}, u32[]{:S(2)}, u32[]{:S(2)}) collective-permute-start(bf16[256,256]{1,0:T(8,128)(2,1)S(1)} %get-tuple-element.63), channel_id=1, source_target_pairs={{0,24},{4,28},{8,0},{12,4},{16,8},{20,12},{24,16},{28,20},{1,25},{... | collective-permute-start | bytes 393224 | tf_op jit(solution)/shard_map/ppermute | solution.py:31
  108.5 0.8 input_block.7
  109.3 12.0 %collective-permute-done.17 = bf16[304,256]{1,0:T(8,128)(2,1)S(1)} collective-permute-done((bf16[304,256]{1,0:T(8,128)(2,1)S(1)}, bf16[304,256]{1,0:T(8,128)(2,1)S(1)}, u32[]{:S(2)}, u32[]{:S(2)}) %collective-permute-start.17) | collective-permute-done | bytes 155680 | tf_op jit(solution)/shard_map/ppermute | solution.py:31
  121.3 1.1 collective-permute-start.10
  122.5 1.6 %collective-permute-done.13.refs_2_ = bf16[256,256]{1,0:T(8,128)(2,1)S(1)} collective-permute-done((bf16[256,256]{1,0:T(8,128)(2,1)S(1)}, bf16[256,256]{1,0:T(8,128)(2,1)S(1)}, u32[]{:S(2)}, u32[]{:S(2)}) %collective-permute-start.13) | collective-permute-done | bytes 131104 | tf_op jit(solution)/shard_map/ppermute | solution.py:31
  124.1 1.0 last_sums.1
  126.3 0.8 input_block.5
  127.1 12.5 %collective-permute-done.10 = bf16[1024,512]{1,0:T(8,128)(2,1)S(1)} collective-permute-done((bf16[1024,512]{1,0:T(8,128)(2,1)S(1)}, bf16[1024,512]{1,0:T(8,128)(2,1)S(1)}, u32[]{:S(2)}, u32[]{:S(2)}) %collective-permute-start.10) | collective-permute-done | bytes 1048608 | tf_op jit(solution)/shard_map/ppermute | solution.py:31
  139.6 1.3 add_convert_fusion
  (102 shorter events, 4.9 us)
Async XLA Ops:
  0.6 12.8 %copy-start.15 = (f32[31,256]{1,0:T(8,128)S(1)}, f32[31,256]{1,0:T(8,128)}, u32[]{:S(2)}) copy-start(f32[31,256]{1,0:T(8,128)} %taps_ref.7) | copy-start | bytes 95236
  6.5 10.7 %collective-permute-start.1 = (f32[64,256]{1,0:T(8,128)S(1)}, f32[64,256]{1,0:T(8,128)S(1)}, u32[]{:S(2)}, u32[]{:S(2)}) collective-permute-start(f32[64,256]{1,0:T(8,128)S(1)} %pad_maximum_fusion.3), channel_id=1, source_target_pairs={{4,0},{8,4},{12,8},{16,12},{20,16},{24,20},{28,24},{5,1},{9,5},{13... | collective-permute-start | bytes 196616 | tf_op jit(solution)/shard_map/ppermute | solution.py:31
  7.8 9.4 %collective-permute-start = (bf16[32,256]{1,0:T(8,128)(2,1)S(1)}, bf16[32,256]{1,0:T(8,128)(2,1)S(1)}, u32[]{:S(2)}, u32[]{:S(2)}) collective-permute-start(bf16[32,256]{1,0:T(8,128)(2,1)S(1)} %get-tuple-element.69.tail_ref), channel_id=1, source_target_pairs={{0,4},{4,8},{8,12},{12,16},{16,20},{20,24},{24,28},{1,5},{5,9},{9,... | collective-permute-start | bytes 49160 | tf_op jit(solution)/shard_map/ppermute | solution.py:31
  13.4 7.7 %copy-start = (bf16[1024,2048]{1,0:T(8,128)(2,1)S(1)}, bf16[1024,2048]{1,0:T(8,128)(2,1)}, u32[]{:S(2)}) copy-start(bf16[1024,2048]{1,0:T(8,128)(2,1)} %right_ref.5) | copy-start | bytes 12582916
  17.9 1.2 collective-permute-start.2
  19.1 4.6 %collective-permute-start.3 = (f32[2,1152]{1,0:T(2,128)S(1)}, f32[2,1152]{1,0:T(2,128)S(1)}, u32[]{:S(2)}, u32[]{:S(2)}) collective-permute-start(f32[2,1152]{1,0:T(2,128)S(1)} %fusion.4), channel_id=1, source_target_pairs={{0,2},{1,3},{2,0},{3,1},{4,6},{5,7},{6,4},{7,5},{8,10},{9,11},{10,... | collective-permute-start | bytes 27656 | tf_op jit(solution)/shard_map/ppermute | solution.py:31
  21.2 1.2 copy-start.6
  22.4 1.4 %copy-start.18 = (f32[256]{0:T(256)S(1)}, f32[256]{0:T(256)}, u32[]{:S(2)}) copy-start(f32[256]{0:T(256)} %param.13) | copy-start | bytes 3076
  22.4 1.4 %copy-start.19 = (f32[256]{0:T(256)S(1)}, f32[256]{0:T(256)}, u32[]{:S(2)}) copy-start(f32[256]{0:T(256)} %param.14) | copy-start | bytes 3076
  26.3 5.5 %copy-start.7 = (bf16[1024,256]{1,0:T(8,128)(2,1)S(1)}, bf16[1024,256]{1,0:T(8,128)(2,1)}, u32[]{:S(2)}) copy-start(bf16[1024,256]{1,0:T(8,128)(2,1)} %get-tuple-element.35.v_hbm) | copy-start | bytes 1572868
  26.3 5.5 %copy-start.8 = (bf16[1024,256]{1,0:T(8,128)(2,1)S(1)}, bf16[1024,256]{1,0:T(8,128)(2,1)}, u32[]{:S(2)}) copy-start(bf16[1024,256]{1,0:T(8,128)(2,1)} %get-tuple-element.36.s_hbm) | copy-start | bytes 1572868
  26.7 1.2 collective-permute-start.4
  28.0 3.7 %collective-permute-start.5 = (f32[2,1152]{1,0:T(2,128)S(1)}, f32[2,1152]{1,0:T(2,128)S(1)}, u32[]{:S(2)}, u32[]{:S(2)}) collective-permute-start(f32[2,1152]{1,0:T(2,128)S(1)} %fusion.5), channel_id=1, source_target_pairs={{0,2},{1,3},{2,0},{3,1},{4,6},{5,7},{6,4},{7,5},{8,10},{9,11},{10,... | collective-permute-start | bytes 27656 | tf_op jit(solution)/shard_map/ppermute | solution.py:31
  31.8 12.5 %copy-start.2 = (bf16[1024,2048]{1,0:T(8,128)(2,1)S(1)}, bf16[1024,2048]{1,0:T(8,128)(2,1)}, u32[]{:S(2)}) copy-start(bf16[1024,2048]{1,0:T(8,128)(2,1)} %right_ref.4) | copy-start | bytes 12582916
  36.8 0.8 copy-start.12
  42.6 0.8 copy-start.9
  43.4 0.8 copy-start.16
  44.2 5.5 %copy-start.1 = (bf16[1024,2048]{1,0:T(8,128)(2,1)S(1)}, bf16[1024,2048]{1,0:T(8,128)(2,1)}, u32[]{:S(2)}) copy-start(bf16[1024,2048]{1,0:T(8,128)(2,1)} %right_ref.5) | copy-start | bytes 12582916
  47.2 27.2 %collective-permute-start.15 = (bf16[1072,256]{1,0:T(8,128)(2,1)}, bf16[1072,256]{1,0:T(8,128)(2,1)}, u32[]{:S(2)}, u32[]{:S(2)}) collective-permute-start(bf16[1072,256]{1,0:T(8,128)(2,1)} %get-tuple-element.47), channel_id=1, source_target_pairs={{0,4},{4,0},{8,12},{12,8},{16,20},{20,16},{24,28},{28,24},{1,5},{5... | collective-permute-start | bytes 1646600 | tf_op jit(solution)/shard_map/ppermute | solution.py:31
  49.8 8.2 %copy-start.4 = (bf16[2048,256]{1,0:T(8,128)(2,1)S(1)}, bf16[2048,256]{1,0:T(8,128)(2,1)}, u32[]{:S(2)}) copy-start(bf16[2048,256]{1,0:T(8,128)(2,1)} %refs_2_.3) | copy-start | bytes 3145732
  49.8 8.2 %copy-start.5 = (bf16[2048,256]{1,0:T(8,128)(2,1)S(1)}, bf16[2048,256]{1,0:T(8,128)(2,1)}, u32[]{:S(2)}) copy-start(bf16[2048,256]{1,0:T(8,128)(2,1)} %refs_3_.3) | copy-start | bytes 3145732
  52.4 13.1 %collective-permute-start.19 = (bf16[512,256]{1,0:T(8,128)(2,1)}, bf16[512,256]{1,0:T(8,128)(2,1)}, u32[]{:S(2)}, u32[]{:S(2)}) collective-permute-start(bf16[512,256]{1,0:T(8,128)(2,1)} %get-tuple-element.52), channel_id=1, source_target_pairs={{0,8},{4,12},{8,16},{12,20},{16,24},{20,28},{24,0},{28,4},{1,9},{5... | collective-permute-start | bytes 786440 | tf_op jit(solution)/shard_map/ppermute | solution.py:31
  54.1 18.9 %collective-permute-start.20 = (bf16[512,256]{1,0:T(8,128)(2,1)}, bf16[512,256]{1,0:T(8,128)(2,1)}, u32[]{:S(2)}, u32[]{:S(2)}) collective-permute-start(bf16[512,256]{1,0:T(8,128)(2,1)} %get-tuple-element.53), channel_id=1, source_target_pairs={{0,16},{4,20},{8,24},{12,28},{16,0},{20,4},{24,8},{28,12},{1,17},{... | collective-permute-start | bytes 786440 | tf_op jit(solution)/shard_map/ppermute | solution.py:31
  55.2 17.8 %collective-permute-start.21 = (bf16[512,256]{1,0:T(8,128)(2,1)S(1)}, bf16[512,256]{1,0:T(8,128)(2,1)}, u32[]{:S(2)}, u32[]{:S(2)}) collective-permute-start(bf16[512,256]{1,0:T(8,128)(2,1)S(1)} %get-tuple-element.54), channel_id=1, source_target_pairs={{0,24},{4,28},{8,0},{12,4},{16,8},{20,12},{24,16},{28,20},{1,25},{... | collective-permute-start | bytes 786440 | tf_op jit(solution)/shard_map/ppermute | solution.py:31
  58.0 48.1 %collective-permute-start.8 = (bf16[2048,256]{1,0:T(8,128)(2,1)S(1)}, bf16[2048,256]{1,0:T(8,128)(2,1)S(1)}, u32[]{:S(2)}, u32[]{:S(2)}) collective-permute-start(bf16[2048,256]{1,0:T(8,128)(2,1)S(1)} %copy-done.4), channel_id=1, source_target_pairs={{0,1},{1,0},{2,3},{3,2},{4,5},{5,4},{6,7},{7,6},{8,9},{9,8},{10,11... | collective-permute-start | bytes 3145736 | tf_op jit(solution)/shard_map/ppermute | solution.py:31
  58.0 1.0 copy-start.10
  59.1 1.0 copy-start.13
  60.8 2.2 %copy-start.3 = (bf16[1024,2048]{1,0:T(8,128)(2,1)S(1)}, bf16[1024,2048]{1,0:T(8,128)(2,1)}, u32[]{:S(2)}) copy-start(bf16[1024,2048]{1,0:T(8,128)(2,1)} %right_ref.4) | copy-start | bytes 12582916
  60.9 2.3 %copy-start.17 = (bf16[256,1024]{1,0:T(8,128)(2,1)S(1)}, bf16[256,1024]{1,0:T(8,128)(2,1)}, u32[]{:S(2)}) copy-start(bf16[256,1024]{1,0:T(8,128)(2,1)} %copy-done.16) | copy-start | bytes 1572868
  63.1 9.8 %copy-start.14 = (bf16[1024,256]{1,0:T(8,128)(2,1)S(1)}, bf16[1024,256]{1,0:T(8,128)(2,1)}, u32[]{:S(2)}) copy-start(bf16[1024,256]{1,0:T(8,128)(2,1)} %copy-done.12) | copy-start | bytes 1572868
  63.2 10.2 %copy-start.22 = (f32[2,256,256]{2,1,0:T(8,128)S(1)}, f32[2,256,256]{2,1,0:T(8,128)}, u32[]{:S(2)}) copy-start(f32[2,256,256]{2,1,0:T(8,128)} %get-tuple-element.51) | copy-start | bytes 1572868
  63.2 13.8 %copy-start.21 = (f32[4,256,256]{2,1,0:T(8,128)S(1)}, f32[4,256,256]{2,1,0:T(8,128)}, u32[]{:S(2)}) copy-start(f32[4,256,256]{2,1,0:T(8,128)} %get-tuple-element.46) | copy-start | bytes 3145732
  65.5 43.0 %collective-permute-start.9 = (bf16[2048,256]{1,0:T(8,128)(2,1)S(1)}, bf16[2048,256]{1,0:T(8,128)(2,1)S(1)}, u32[]{:S(2)}, u32[]{:S(2)}) collective-permute-start(bf16[2048,256]{1,0:T(8,128)(2,1)S(1)} %copy-done.5), channel_id=1, source_target_pairs={{0,1},{1,0},{2,3},{3,2},{4,5},{5,4},{6,7},{7,6},{8,9},{9,8},{10,11... | collective-permute-start | bytes 3145736 | tf_op jit(solution)/shard_map/ppermute | solution.py:31
  72.9 29.6 %collective-permute-start.7 = (bf16[1024,256]{1,0:T(8,128)(2,1)S(1)}, bf16[1024,256]{1,0:T(8,128)(2,1)S(1)}, u32[]{:S(2)}, u32[]{:S(2)}) collective-permute-start(bf16[1024,256]{1,0:T(8,128)(2,1)S(1)} %copy-done.14), channel_id=1, source_target_pairs={{0,1},{1,0},{2,3},{3,2},{4,5},{5,4},{6,7},{7,6},{8,9},{9,8},{10,11... | collective-permute-start | bytes 1572872 | tf_op jit(solution)/shard_map/ppermute | solution.py:31
  72.9 17.2 %collective-permute-start.11 = (bf16[1024,256]{1,0:T(8,128)(2,1)S(1)}, bf16[1024,256]{1,0:T(8,128)(2,1)S(1)}, u32[]{:S(2)}, u32[]{:S(2)}) collective-permute-start(bf16[1024,256]{1,0:T(8,128)(2,1)S(1)} %get-tuple-element.41), channel_id=1, source_target_pairs={{0,4},{4,0},{8,12},{12,8},{16,20},{20,16},{24,28},{28,24},{1,5},{5... | collective-permute-start | bytes 1572872 | tf_op jit(solution)/shard_map/ppermute | solution.py:31
  74.4 15.7 %collective-permute-start.22 = (bf16[256,256]{1,0:T(8,128)(2,1)S(1)}, bf16[256,256]{1,0:T(8,128)(2,1)S(1)}, u32[]{:S(2)}, u32[]{:S(2)}) collective-permute-start(bf16[256,256]{1,0:T(8,128)(2,1)S(1)} %add_convert_fusion.1), channel_id=1, source_target_pairs={{0,4},{4,0},{8,12},{12,8},{16,20},{20,16},{24,28},{28,24},{1,5},{5... | collective-permute-start | bytes 393224 | tf_op jit(solution)/shard_map/ppermute | solution.py:31
  77.0 13.1 %copy-start.11 = (bf16[1024,256]{1,0:T(8,128)(2,1)S(1)}, bf16[1024,256]{1,0:T(8,128)(2,1)}, u32[]{:S(2)}) copy-start(bf16[1024,256]{1,0:T(8,128)(2,1)} %copy-done.9) | copy-start | bytes 1572868
  78.3 20.9 %copy-start.20 = (f32[4,256,256]{2,1,0:T(8,128)S(1)}, f32[4,256,256]{2,1,0:T(8,128)}, u32[]{:S(2)}) copy-start(f32[4,256,256]{2,1,0:T(8,128)} %get-tuple-element.40) | copy-start | bytes 3145732
  90.1 16.0 %collective-permute-start.6 = (bf16[1024,256]{1,0:T(8,128)(2,1)S(1)}, bf16[1024,256]{1,0:T(8,128)(2,1)S(1)}, u32[]{:S(2)}, u32[]{:S(2)}) collective-permute-start(bf16[1024,256]{1,0:T(8,128)(2,1)S(1)} %copy-done.11), channel_id=1, source_target_pairs={{0,1},{1,0},{2,3},{3,2},{4,5},{5,4},{6,7},{7,6},{8,9},{9,8},{10,11... | collective-permute-start | bytes 1572872 | tf_op jit(solution)/shard_map/ppermute | solution.py:31
  90.1 11.1 %collective-permute-start.18 = (bf16[304,256]{1,0:T(8,128)(2,1)S(1)}, bf16[304,256]{1,0:T(8,128)(2,1)S(1)}, u32[]{:S(2)}, u32[]{:S(2)}) collective-permute-start(bf16[304,256]{1,0:T(8,128)(2,1)S(1)} %get-tuple-element.72), channel_id=1, source_target_pairs={{0,24},{4,28},{8,0},{12,4},{16,8},{20,12},{24,16},{28,20},{1,25},{... | collective-permute-start | bytes 466952 | tf_op jit(solution)/shard_map/ppermute | solution.py:31
  101.2 20.1 %collective-permute-start.17 = (bf16[304,256]{1,0:T(8,128)(2,1)S(1)}, bf16[304,256]{1,0:T(8,128)(2,1)S(1)}, u32[]{:S(2)}, u32[]{:S(2)}) collective-permute-start(bf16[304,256]{1,0:T(8,128)(2,1)S(1)} %get-tuple-element.73), channel_id=1, source_target_pairs={{0,16},{4,20},{8,24},{12,28},{16,0},{20,4},{24,8},{28,12},{1,17},{... | collective-permute-start | bytes 466952 | tf_op jit(solution)/shard_map/ppermute | solution.py:31
  102.5 19.9 %collective-permute-start.12 = (bf16[256,256]{1,0:T(8,128)(2,1)S(1)}, bf16[256,256]{1,0:T(8,128)(2,1)S(1)}, u32[]{:S(2)}, u32[]{:S(2)}) collective-permute-start(bf16[256,256]{1,0:T(8,128)(2,1)S(1)} %get-tuple-element.65), channel_id=1, source_target_pairs={{0,8},{4,12},{8,16},{12,20},{16,24},{20,28},{24,0},{28,4},{1,9},{5... | collective-permute-start | bytes 393224 | tf_op jit(solution)/shard_map/ppermute | solution.py:31
  106.1 18.0 %collective-permute-start.13 = (bf16[256,256]{1,0:T(8,128)(2,1)S(1)}, bf16[256,256]{1,0:T(8,128)(2,1)S(1)}, u32[]{:S(2)}, u32[]{:S(2)}) collective-permute-start(bf16[256,256]{1,0:T(8,128)(2,1)S(1)} %get-tuple-element.64), channel_id=1, source_target_pairs={{0,16},{4,20},{8,24},{12,28},{16,0},{20,4},{24,8},{28,12},{1,17},{... | collective-permute-start | bytes 393224 | tf_op jit(solution)/shard_map/ppermute | solution.py:31
  106.1 18.0 %collective-permute-start.14 = (bf16[256,256]{1,0:T(8,128)(2,1)S(1)}, bf16[256,256]{1,0:T(8,128)(2,1)S(1)}, u32[]{:S(2)}, u32[]{:S(2)}) collective-permute-start(bf16[256,256]{1,0:T(8,128)(2,1)S(1)} %get-tuple-element.63), channel_id=1, source_target_pairs={{0,24},{4,28},{8,0},{12,4},{16,8},{20,12},{24,16},{28,20},{1,25},{... | collective-permute-start | bytes 393224 | tf_op jit(solution)/shard_map/ppermute | solution.py:31
  108.5 13.9 %collective-permute-start.16 = (bf16[304,256]{1,0:T(8,128)(2,1)S(1)}, bf16[304,256]{1,0:T(8,128)(2,1)S(1)}, u32[]{:S(2)}, u32[]{:S(2)}) collective-permute-start(bf16[304,256]{1,0:T(8,128)(2,1)S(1)} %get-tuple-element.74), channel_id=1, source_target_pairs={{0,8},{4,12},{8,16},{12,20},{16,24},{20,28},{24,0},{28,4},{1,9},{5... | collective-permute-start | bytes 466952 | tf_op jit(solution)/shard_map/ppermute | solution.py:31
  121.3 18.3 %collective-permute-start.10 = (bf16[1024,512]{1,0:T(8,128)(2,1)S(1)}, bf16[1024,512]{1,0:T(8,128)(2,1)S(1)}, u32[]{:S(2)}, u32[]{:S(2)}) collective-permute-start(bf16[1024,512]{1,0:T(8,128)(2,1)S(1)} %input_block.7), channel_id=1, source_target_pairs={{0,2},{1,3},{2,0},{3,1},{4,6},{5,7},{6,4},{7,5},{8,10},{9,11},{10,... | collective-permute-start | bytes 3145736 | tf_op jit(solution)/shard_map/ppermute | solution.py:31

commit v3 on v2

--- a/solution.py
+++ b/solution.py
@@ -72,7 +72,7 @@
 
     leaving = [pltpu.make_async_copy(own.at[j], own_hbm.at[j], sems.at[j]) for j in range(count)]
     for j in range(count):
-        own[j] = block(len(outs) * count + j)
+        own[j] = block(len(outs) * count + j).astype(bf16)
         leaving[j].start()
     for i, out in enumerate(outs):
         for j in range(count):
@@ -103,8 +103,8 @@
         in_specs=[SMEM_SPEC] + [VMEM_SPEC] * (2 + len(rider)),
         out_specs=[VMEM_SPEC] * gives + [HBM_SPEC],
         out_shape=[jax.ShapeDtypeStruct((count * rows + extra, width), bf16)] * gives
-        + [pltpu.HBM((count, rows, width), f32)],
-        scratch_shapes=[pltpu.VMEM((count, rows, width), f32), pltpu.SemaphoreType.DMA((count,))],
+        + [pltpu.HBM((count, rows, width), bf16)],
+        scratch_shapes=[pltpu.VMEM((count, rows, width), bf16), pltpu.SemaphoreType.DMA((count,))],
         compiler_params=limit(10),
         cost_estimate=pl.CostEstimate(
             flops=2 * rows * tok * count * width * len(ids),
@@ -368,7 +368,7 @@
     ch = filtered_ref.shape[1]
     tok = mixed_ref.shape[0]
     col_ref[...] = stats_ref[...].T
-    chunk = chunk_of(tok, 64)
+    chunk = chunk_of(tok, 128)
 
     def some_rows(base, count, mixed, own):
         here = pl.ds(base, count)
@@ -465,6 +465,27 @@
         return carry
 
     lax.fori_loop(0, rows // part_rows, filtered_grad, 0)
+    width = chunk_of(tok, 128)
+
+    def gather(i, sums):
+        base = pl.multiple_of(i * width, width)
+        g = grad_ref[pl.ds(base, width), :]
+        x = ext_ref[pl.ds(base, width + HALO), :]
+        sums = list(sums)
+        for r in range(8):
+            moved = x if r == 0 else pltpu.roll(x, r, 0)
+            for k in range(r, taps, 8):
+                for j in range(width // 8):
+                    low = HALO + 8 * j - (k - r)
+                    sums[k] = sums[k] + g[8 * j : 8 * j + 8] * moved[low : low + 8]
+        return tuple(sums)
+
+    zero = jnp.zeros((8, LANE), f32)
+    sums = lax.fori_loop(0, tok // width, gather, (zero,) * taps)
+    for k in range(taps):
+        small_ref[pl.ds(k, 1), :] = jnp.sum(sums[k], axis=0, keepdims=True)
+    for k in range(taps, small_ref.shape[0]):
+        small_ref[pl.ds(k, 1), :] = jnp.zeros((1, LANE), f32)
     for copy in coming:
         copy.wait()
     weights = tap_rows(taps_ref, cols)
@@ -495,28 +516,6 @@
     if leave:
         leaving = pltpu.make_async_copy(turned_ref, turned_out, leave[1])
         leaving.start()
-
-    width = chunk_of(tok, 128)
-
-    def gather(i, sums):
-        base = pl.multiple_of(i * width, width)
-        g = grad_ref[pl.ds(base, width), :]
-        x = ext_ref[pl.ds(base, width + HALO), :]
-        sums = list(sums)
-        for r in range(8):
-            moved = x if r == 0 else pltpu.roll(x, r, 0)
-            for k in range(r, taps, 8):
-                for j in range(width // 8):
-                    low = HALO + 8 * j - (k - r)
-                    sums[k] = sums[k] + g[8 * j : 8 * j + 8] * moved[low : low + 8]
-        return tuple(sums)
-
-    zero = jnp.zeros((8, LANE), f32)
-    sums = lax.fori_loop(0, tok // width, gather, (zero,) * taps)
-    for k in range(taps):
-        small_ref[pl.ds(k, 1), :] = jnp.sum(sums[k], axis=0, keepdims=True)
-    for k in range(taps, small_ref.shape[0]):
-        small_ref[pl.ds(k, 1), :] = jnp.zeros((1, LANE), f32)
     if leave:
         leaving.wait()
 
@@ -553,57 +552,55 @@
     )(normed, gn, stats, before, glu, after, v, s, conv_taps)
 
 
-def input_kernel(index_ref, *refs, halves, fetch):
+def input_kernel(index_ref, *refs, halves):
     grads = refs[:halves]
-    if fetch:
-        value_hbm, gate_hbm, add_ref, out_ref, value_ref, gate_ref, sems = refs[halves:]
-        copies = []
-        for m, (hbm, ref) in enumerate(((value_hbm, value_ref), (gate_hbm, gate_ref))):
-            start = pl.multiple_of(index_ref[0] * ref.shape[0], 16)
-            copies.append(pltpu.make_async_copy(hbm.at[pl.ds(start, ref.shape[0]), :], ref, sems.at[m]))
-        for copy in copies:
-            copy.start()
-        for copy in copies:
-            copy.wait()
-        rows = slice(None)
-    else:
-        value_ref, gate_ref, out_ref = refs[halves:]
-        rows = pl.ds(pl.multiple_of(index_ref[0] * out_ref.shape[1], 16), out_ref.shape[1])
-    weight = []
-    for h in range(halves):
-        cols = pl.ds(h * LANE, LANE)
-        weight += [value_ref[rows, cols], gate_ref[rows, cols]]
-    total = right_product(
-        jnp.concatenate([g[...] for g in grads], axis=1), jnp.concatenate(weight, axis=1)
-    )
-    if fetch:
-        total = total + add_ref[...]
-    out_ref[...] = total.astype(out_ref.dtype)
-
-
-def input_block(grads, value, gate, block, n, add=None):
+    pair_grads = refs[halves : 2 * halves]
+    value_ref, gate_ref, *pair_hbm, out_ref, pair_value, pair_gate, sems = refs[2 * halves :]
+    _, width = out_ref.shape
+    rows = pl.ds(pl.multiple_of(index_ref[0] * width, 16), width)
+    copies = [
+        pltpu.make_async_copy(hbm.at[rows, :], ref, sems.at[m])
+        for m, (hbm, ref) in enumerate(zip(pair_hbm, (pair_value, pair_gate)))
+    ]
+    for copy in copies:
+        copy.start()
+
+    def product(grads, values, gates):
+        weight = []
+        for h in range(halves):
+            cols = slice(h * LANE, (h + 1) * LANE)
+            weight += [values[:, cols], gates[:, cols]]
+        return right_product(
+            jnp.concatenate([g[...] for g in grads], axis=1), jnp.concatenate(weight, axis=1)
+        )
+
+    total = product(grads, value_ref[rows, :], gate_ref[rows, :])
+    for copy in copies:
+        copy.wait()
+    out_ref[...] = (total + product(pair_grads, pair_value[...], pair_gate[...])).astype(bf16)
+
+
+def input_block(grads, pair_grads, weights, pair_weights, block, n):
     t = grads[0].shape[0]
-    d, c = value.shape
+    d, c = weights[0].shape
     width = d // n
-    fetch = add is not None
-    weights = [pl.BlockSpec(memory_space=pl.ANY)] * 2 + [VMEM_SPEC] if fetch else [VMEM_SPEC] * 2
-    scratch = [
-        pltpu.VMEM((width, c), bf16),
-        pltpu.VMEM((width, c), bf16),
-        pltpu.SemaphoreType.DMA((2,)),
-    ]
-    return pl.pallas_call(
-        functools.partial(input_kernel, halves=len(grads), fetch=fetch),
-        in_specs=[SMEM_SPEC] + [VMEM_SPEC] * len(grads) + weights,
+    hbm = pl.BlockSpec(memory_space=pl.ANY)
+    return pl.pallas_call(
+        functools.partial(input_kernel, halves=len(grads)),
+        in_specs=[SMEM_SPEC] + [VMEM_SPEC] * (2 * len(grads) + 2) + [hbm] * 2,
         out_specs=VMEM_SPEC,
-        out_shape=jax.ShapeDtypeStruct((t, width), bf16 if fetch else f32),
-        scratch_shapes=scratch if fetch else [],
-        compiler_params=limit(14),
+        out_shape=jax.ShapeDtypeStruct((t, width), bf16),
+        scratch_shapes=[
+            pltpu.VMEM((width, c), bf16),
+            pltpu.VMEM((width, c), bf16),
+            pltpu.SemaphoreType.DMA((2,)),
+        ],
+        compiler_params=limit(16),
         cost_estimate=pl.CostEstimate(
-            flops=4 * t * c * width, transcendentals=0, bytes_accessed=2 * (2 * t * c + 2 * width * c + 3 * t * width)
+            flops=8 * t * c * width, transcendentals=0, bytes_accessed=2 * (4 * t * c + 4 * width * c + t * width)
         ),
         name="input_block",
-    )(block.reshape(1).astype(jnp.int32), *grads, value, gate, *([add] if fetch else []))
+    )(block.reshape(1).astype(jnp.int32), *grads, *pair_grads, *weights, *pair_weights)
 
 
 def input_gradient(grads, pair_grads, weights, pair_weights):
@@ -611,8 +608,7 @@
     me = lax.axis_index("tp")
 
     def both(block):
-        own = input_block(grads, *weights, block, n)
-        return input_block(pair_grads, *pair_weights, block, n, own)
+        return input_block(grads, pair_grads, weights, pair_weights, block, n)
 
     parts = []
     for k in range(1, n // 2):

time: 141 us -> 137 us (0.972)
  starting transfers between devices: 36.6 us -> 34.1 us
  local copies, waits for them, and re-layouts: 7.33 us -> 5.39 us
    ppermute x23, starting transfers between devices: 36.6 us -> 34.1 us  [send(): return lax.ppermute(block, axis, route)]
    unnamed x46 -> x34, local copies, waits for them, and re-layouts: 7.27 us -> 5.33 us
    pallas_call x4 -> x2, Pallas kernels: 3.08 us -> 2.87 us  [input_block(): pl.pallas_call(functools.partial(input_kernel, halves=len(grads)), in_spe...]
  transfers between devices with their start and end apart: 23 -> 23, of which waited for: 9 -> 10; matrix products, arithmetic and copies ran while one was open for 5% -> 5% of each run, Pallas kernels for 10% -> 10%
where the time goes in v3:
time: 137 us; the launch traced here: 136 us
  waiting for transfers between devices  52.2 us (38%)
  Pallas kernels  34.5 us (25%)
  starting transfers between devices  34.1 us (25%)
  other arithmetic  8.71 us (6%)
  local copies, waits for them, and re-layouts  5.39 us (4%)
    ppermute x23, waiting for transfers between devices, send(): return lax.ppermute(block, axis, route)  52.2 us
    ppermute x23, starting transfers between devices, send(): return lax.ppermute(block, axis, route)  34.1 us
    pallas_call x2, Pallas kernels, back_convolve(): pl.pallas_call(functools.partial(back_conv_kernel, h=h), in_specs=[VMEM_S...  10.1 us
    pallas_call x3, Pallas kernels, grad_blocks(): pl.pallas_call(functools.partial(blocks_kernel, gives=gives), in_specs=[S...  7.78 us
    pallas_call x1, Pallas kernels, project(): pl.pallas_call(project_kernel, in_specs=[hbm] * 5, out_specs=[HBM_SPEC] *...  5.81 us
    unnamed x34, local copies, waits for them, and re-layouts  5.33 us
    pallas_call x1, Pallas kernels, convolve(): pl.pallas_call(conv_kernel, in_specs=[VMEM_SPEC, VMEM_SPEC], out_specs=VM...  3.74 us
    pallas_call x2, Pallas kernels, input_block(): pl.pallas_call(functools.partial(input_kernel, halves=len(grads)), in_spe...  2.87 us
  transfers between devices with their start and end apart: 23, of which 10 were waited for; matrix products, arithmetic and copies ran while one was open for 5% of the time, Pallas kernels for 10%

profile of v3, /device:TPU:0, one launch (start us, length us, event | category | flops | bytes accessed | tf_op | source)
XLA Modules:
  0.0 136.2 jit_solution(15740310260064440598)
XLA Ops:
  0.6 5.8 %project.1 = (bf16[1024,256]{1,0:T(8,128)(2,1)}, bf16[1024,256]{1,0:T(8,128)(2,1)}, bf16[1024,256]{1,0:T(8,128)(2,1)S(1)}, f32[32,256]{1,0:T(8,128)S(1)}) custom-call(bf16[1024,2048]{1,0:T(8,128)(2,1)} %right_ref.4, bf16[2048,256]{1,0:T(8,128)(2,1)} %refs_4_.3, bf16[2048,256]{1,0:T(8,128)(2,1)} %refs_5_.3, bf16[1024,2048]{1,0:T(8,128)(2,1)} %right_ref.5, ...), custom_call_target="tpu_custom_call" | custom-call | flops 2147483648 | bytes 8912896 | tf_op jit(solution)/shard_map/project/pallas_call | solution.py:227
  6.5 1.3 collective-permute-start.1
  7.8 5.5 %collective-permute-start = (bf16[32,256]{1,0:T(8,128)(2,1)S(1)}, bf16[32,256]{1,0:T(8,128)(2,1)S(1)}, u32[]{:S(2)}, u32[]{:S(2)}) collective-permute-start(bf16[32,256]{1,0:T(8,128)(2,1)S(1)} %get-tuple-element.69.tail_ref), channel_id=1, source_target_pairs={{0,4},{4,8},{8,12},{12,16},{16,20},{20,24},{24,28},{1,5},{5,9},{9,... | collective-permute-start | bytes 49160 | tf_op jit(solution)/shard_map/ppermute | solution.py:31
  13.5 3.7 %convolve.1.main_ref = f32[1056,256]{1,0:T(8,128)S(1)} custom-call(bf16[1024,256]{1,0:T(8,128)(2,1)S(1)} %get-tuple-element.31.glu_ref, f32[31,256]{1,0:T(8,128)S(1)} %copy-done.9), custom_call_target="tpu_custom_call" | custom-call | flops 162529280 | bytes 1572864 | tf_op jit(solution)/shard_map/convolve/pallas_call | solution.py:312
  17.4 0.4 fusion.7
  18.0 1.1 collective-permute-done.2
  19.1 2.1 %collective-permute-start.3 = (f32[2,1152]{1,0:T(2,128)S(1)}, f32[2,1152]{1,0:T(2,128)S(1)}, u32[]{:S(2)}, u32[]{:S(2)}) collective-permute-start(f32[2,1152]{1,0:T(2,128)S(1)} %fusion.4), channel_id=1, source_target_pairs={{0,2},{1,3},{2,0},{3,1},{4,6},{5,7},{6,4},{7,5},{8,10},{9,11},{10,... | collective-permute-start | bytes 27656 | tf_op jit(solution)/shard_map/ppermute | solution.py:31
  21.2 1.2 copy-done.6
  22.4 1.3 back_project.1.mixed_ref
  23.8 1.8 %activate.1 = (f32[1056,256]{1,0:T(8,128)S(1)}, f32[1056,256]{1,0:T(8,128)S(1)}, bf16[256,1024]{1,0:T(8,128)(2,1)S(1)}, f32[16,256]{1,0:T(8,128)S(1)}) custom-call(f32[1056,256]{1,0:T(8,128)S(1)} %convolve_ends.1.filtered_ref, f32[8,1152]{1,0:T(8,128)S(1)} %select_maximum_fusion.1.stats_ref, f32[1024,256]{1,0:T(8,128)S(1)} %back_project.1.mixed_ref, ...), custom_call_target="tpu_custom_call" | custom-call | flops 52428800 | bytes 4718592 | tf_op jit(solution)/shard_map/activate/pallas_call | solution.py:419
  25.6 0.4 fusion.6
  26.2 1.1 collective-permute-done.4
  27.3 1.2 collective-permute-start.5
  28.6 2.5 %collective-permute-done.5 = f32[2,1152]{1,0:T(2,128)S(1)} collective-permute-done((f32[2,1152]{1,0:T(2,128)S(1)}, f32[2,1152]{1,0:T(2,128)S(1)}, u32[]{:S(2)}, u32[]{:S(2)}) %collective-permute-start.5) | collective-permute-done | bytes 9248 | tf_op jit(solution)/shard_map/ppermute | solution.py:31
  31.1 5.0 %back_convolve.3 = (bf16[1024,256]{1,0:T(8,128)(2,1)S(1)}, bf16[256,1024]{1,0:T(8,128)(2,1)S(1)}, f32[32,128]{1,0:T(8,128)S(1)}) custom-call(f32[1056,256]{1,0:T(8,128)S(1)} %get-tuple-element.33.normed_ref, f32[1056,256]{1,0:T(8,128)S(1)} %get-tuple-element.34.gn_ref, f32[8,1152]{1,0:T(8,128)S(1)} %select_maximum_fusion.stats_ref, ...), custom_call_target="tpu_custom_call" | custom-call | flops 162529280 | bytes 2097152 | tf_op jit(solution)/shard_map/back_convolve/pallas_call | solution.py:529
  36.2 5.0 %back_convolve.2 = (bf16[1024,256]{1,0:T(8,128)(2,1)S(1)}, bf16[256,1024]{1,0:T(8,128)(2,1)S(1)}, f32[32,128]{1,0:T(8,128)S(1)}) custom-call(f32[1056,256]{1,0:T(8,128)S(1)} %get-tuple-element.33.normed_ref, f32[1056,256]{1,0:T(8,128)S(1)} %get-tuple-element.34.gn_ref, f32[8,1152]{1,0:T(8,128)S(1)} %select_maximum_fusion.stats_ref, ...), custom_call_target="tpu_custom_call" | custom-call | flops 162529280 | bytes 2097152 | tf_op jit(solution)/shard_map/back_convolve/pallas_call | solution.py:529
  41.2 0.8 copy-done.10
  42.1 2.8 %grad_blocks.4 = (bf16[1072,256]{1,0:T(8,128)(2,1)}, bf16[4,256,256]{2,1,0:T(8,128)(2,1)}) custom-call(s32[8]{0:T(128)S(1)} %pad_add_fusion.ids_ref, bf16[256,1024]{1,0:T(8,128)(2,1)S(1)} %get-tuple-element.42.left_ref, bf16[1024,2048]{1,0:T(8,128)(2,1)S(1)} %copy-done.2, bf16[48,256]{1,0:T(8,128)(2,1)S(1)} %pad_maximum_fusion.4.refs_0_), custom_call_target="tpu_custom_call" | custom-call | flops 1073741824 | bytes 6815744 | tf_op jit(solution)/shard_map/grad_blocks/pallas_call | solution.py:101
  44.9 2.5 %collective-permute-start.15 = (bf16[1072,256]{1,0:T(8,128)(2,1)}, bf16[1072,256]{1,0:T(8,128)(2,1)}, u32[]{:S(2)}, u32[]{:S(2)}) collective-permute-start(bf16[1072,256]{1,0:T(8,128)(2,1)} %get-tuple-element.47), channel_id=1, source_target_pairs={{0,4},{4,0},{8,12},{12,8},{16,20},{20,16},{24,28},{28,24},{1,5},{5... | collective-permute-start | bytes 1646600 | tf_op jit(solution)/shard_map/ppermute | solution.py:31
  47.5 2.7 %grad_blocks.5 = (bf16[512,256]{1,0:T(8,128)(2,1)}, bf16[512,256]{1,0:T(8,128)(2,1)}, bf16[512,256]{1,0:T(8,128)(2,1)S(1)}, bf16[2,256,256]{2,1,0:T(8,128)(2,1)}) custom-call(s32[8]{0:T(128)S(1)} %pad_add_fusion.1.ids_ref, bf16[256,1024]{1,0:T(8,128)(2,1)S(1)} %get-tuple-element.50.left_ref, bf16[1024,2048]{1,0:T(8,128)(2,1)S(1)} %copy-done.1), custom_call_target="tpu_custom_call" | custom-call | flops 1073741824 | bytes 6815744 | tf_op jit(solution)/shard_map/grad_blocks/pallas_call | solution.py:101
  50.1 1.6 %collective-permute-start.19 = (bf16[512,256]{1,0:T(8,128)(2,1)}, bf16[512,256]{1,0:T(8,128)(2,1)}, u32[]{:S(2)}, u32[]{:S(2)}) collective-permute-start(bf16[512,256]{1,0:T(8,128)(2,1)} %get-tuple-element.52), channel_id=1, source_target_pairs={{0,8},{4,12},{8,16},{12,20},{16,24},{20,28},{24,0},{28,4},{1,9},{5... | collective-permute-start | bytes 786440 | tf_op jit(solution)/shard_map/ppermute | solution.py:31
  51.8 1.1 collective-permute-start.20
  52.9 2.8 %collective-permute-start.21 = (bf16[512,256]{1,0:T(8,128)(2,1)S(1)}, bf16[512,256]{1,0:T(8,128)(2,1)}, u32[]{:S(2)}, u32[]{:S(2)}) collective-permute-start(bf16[512,256]{1,0:T(8,128)(2,1)S(1)} %get-tuple-element.54), channel_id=1, source_target_pairs={{0,24},{4,28},{8,0},{12,4},{16,8},{20,12},{24,16},{28,20},{1,25},{... | collective-permute-start | bytes 786440 | tf_op jit(solution)/shard_map/ppermute | solution.py:31
  55.7 2.2 %copy-done.3 = bf16[1024,2048]{1,0:T(8,128)(2,1)S(1)} copy-done((bf16[1024,2048]{1,0:T(8,128)(2,1)S(1)}, bf16[1024,2048]{1,0:T(8,128)(2,1)}, u32[]{:S(2)}) %copy-start.3) | copy-done | bytes 4194328
  57.9 1.0 copy-done.11
  58.9 2.3 %grad_blocks.3 = (bf16[1024,256]{1,0:T(8,128)(2,1)S(1)}, bf16[4,256,256]{2,1,0:T(8,128)(2,1)}) custom-call(s32[8]{0:T(128)S(1)} %pad_add_fusion.ids_ref, bf16[256,1024]{1,0:T(8,128)(2,1)S(1)} %copy-done.11, bf16[1024,2048]{1,0:T(8,128)(2,1)S(1)} %copy-done.3), custom_call_target="tpu_custom_call" | custom-call | flops 1073741824 | bytes 6815744 | tf_op jit(solution)/shard_map/grad_blocks/pallas_call | solution.py:101
  61.9 8.8 %collective-permute-done.20 = bf16[512,256]{1,0:T(8,128)(2,1)} collective-permute-done((bf16[512,256]{1,0:T(8,128)(2,1)}, bf16[512,256]{1,0:T(8,128)(2,1)}, u32[]{:S(2)}, u32[]{:S(2)}) %collective-permute-start.20) | collective-permute-done | bytes 262176 | tf_op jit(solution)/shard_map/ppermute | solution.py:31
  70.9 1.1 add_convert_fusion.1
  72.1 1.8 %collective-permute-start.22 = (bf16[256,256]{1,0:T(8,128)(2,1)S(1)}, bf16[256,256]{1,0:T(8,128)(2,1)S(1)}, u32[]{:S(2)}, u32[]{:S(2)}) collective-permute-start(bf16[256,256]{1,0:T(8,128)(2,1)S(1)} %add_convert_fusion.1), channel_id=1, source_target_pairs={{0,4},{4,0},{8,12},{12,8},{16,20},{20,16},{24,28},{28,24},{1,5},{5... | collective-permute-start | bytes 393224 | tf_op jit(solution)/shard_map/ppermute | solution.py:31
  73.9 0.7 add_convert_fusion.8
  74.6 1.2 add_convert_fusion.2
  75.9 11.3 %collective-permute-done.22 = bf16[256,256]{1,0:T(8,128)(2,1)S(1)} collective-permute-done((bf16[256,256]{1,0:T(8,128)(2,1)S(1)}, bf16[256,256]{1,0:T(8,128)(2,1)S(1)}, u32[]{:S(2)}, u32[]{:S(2)}) %collective-permute-start.22) | collective-permute-done | bytes 131104 | tf_op jit(solution)/shard_map/ppermute | solution.py:31
  87.2 5.1 %collective-permute-start.18 = (bf16[304,256]{1,0:T(8,128)(2,1)S(1)}, bf16[304,256]{1,0:T(8,128)(2,1)S(1)}, u32[]{:S(2)}, u32[]{:S(2)}) collective-permute-start(bf16[304,256]{1,0:T(8,128)(2,1)S(1)} %get-tuple-element.72), channel_id=1, source_target_pairs={{0,24},{4,28},{8,0},{12,4},{16,8},{20,12},{24,16},{28,20},{1,25},{... | collective-permute-start | bytes 466952 | tf_op jit(solution)/shard_map/ppermute | solution.py:31
  92.3 1.8 %add_multiply_fusion = f32[256,256]{1,0:T(8,128)} fusion(bf16[256,256]{1,0:T(8,128)(2,1)S(1)} %collective-permute-done.22, bf16[512,256]{1,0:T(8,128)(2,1)} %collective-permute-done.21, s32[]{:T(128)S(6)} %select_n.164, bf16[512,256]{1,0:T(8,128)(2,1)} %collective-permute-done.20, bf16[512,256]{1,0:T(8,128)(2,1)} %collective-permute-done.19, ...), kind=kLoop, calls=%fused_computation.3 | loop fusion | flops 655360 | bytes 917508 | tf_op jit(solution)/shard_map/mul | solution.py:697
  94.3 2.0 %collective-permute-done.18 = bf16[304,256]{1,0:T(8,128)(2,1)S(1)} collective-permute-done((bf16[304,256]{1,0:T(8,128)(2,1)S(1)}, bf16[304,256]{1,0:T(8,128)(2,1)S(1)}, u32[]{:S(2)}, u32[]{:S(2)}) %collective-permute-start.18) | collective-permute-done | bytes 155680 | tf_op jit(solution)/shard_map/ppermute | solution.py:31
  96.3 1.3 collective-permute-start.17
  97.6 3.5 %collective-permute-start.12 = (bf16[256,256]{1,0:T(8,128)(2,1)S(1)}, bf16[256,256]{1,0:T(8,128)(2,1)S(1)}, u32[]{:S(2)}, u32[]{:S(2)}) collective-permute-start(bf16[256,256]{1,0:T(8,128)(2,1)S(1)} %get-tuple-element.65), channel_id=1, source_target_pairs={{0,8},{4,12},{8,16},{12,20},{16,24},{20,28},{24,0},{28,4},{1,9},{5... | collective-permute-start | bytes 393224 | tf_op jit(solution)/shard_map/ppermute | solution.py:31
  101.2 2.4 %collective-permute-start.14 = (bf16[256,256]{1,0:T(8,128)(2,1)S(1)}, bf16[256,256]{1,0:T(8,128)(2,1)S(1)}, u32[]{:S(2)}, u32[]{:S(2)}) collective-permute-start(bf16[256,256]{1,0:T(8,128)(2,1)S(1)} %get-tuple-element.63), channel_id=1, source_target_pairs={{0,24},{4,28},{8,0},{12,4},{16,8},{20,12},{24,16},{28,20},{1,25},{... | collective-permute-start | bytes 393224 | tf_op jit(solution)/shard_map/ppermute | solution.py:31
  103.6 1.4 %input_block.3 = bf16[1024,512]{1,0:T(8,128)(2,1)S(1)} custom-call(s32[1]{0:T(128)} %bitcast.3.index_ref, bf16[1024,256]{1,0:T(8,128)(2,1)S(1)} %get-tuple-element.37.refs_0_, bf16[1024,256]{1,0:T(8,128)(2,1)S(1)} %get-tuple-element.38.refs_1_, bf16[1024,256]{1,0:T(8,128)(2,1)S(1)} %collective-permute-done.6.refs_2_, ...), custom_call_target="tpu_custom_call" | custom-call | flops 1073741824 | bytes 4194304 | tf_op jit(solution)/shard_map/input_block/pallas_call | solution.py:588
  105.0 11.3 %collective-permute-done.17 = bf16[304,256]{1,0:T(8,128)(2,1)S(1)} collective-permute-done((bf16[304,256]{1,0:T(8,128)(2,1)S(1)}, bf16[304,256]{1,0:T(8,128)(2,1)S(1)}, u32[]{:S(2)}, u32[]{:S(2)}) %collective-permute-start.17) | collective-permute-done | bytes 155680 | tf_op jit(solution)/shard_map/ppermute | solution.py:31
  116.4 1.1 collective-permute-start.10
  117.5 1.6 %collective-permute-done.13.refs_2_ = bf16[256,256]{1,0:T(8,128)(2,1)S(1)} collective-permute-done((bf16[256,256]{1,0:T(8,128)(2,1)S(1)}, bf16[256,256]{1,0:T(8,128)(2,1)S(1)}, u32[]{:S(2)}, u32[]{:S(2)}) %collective-permute-start.13) | collective-permute-done | bytes 131104 | tf_op jit(solution)/shard_map/ppermute | solution.py:31
  119.2 1.0 last_sums.1
  120.2 0.6 slice_multiply_fusion.3
  120.8 0.6 fusion
  121.4 1.4 %input_block.2 = bf16[1024,512]{1,0:T(8,128)(2,1)S(1)} custom-call(s32[1]{0:T(128)} %bitcast.index_ref, bf16[1024,256]{1,0:T(8,128)(2,1)S(1)} %get-tuple-element.37.refs_0_, bf16[1024,256]{1,0:T(8,128)(2,1)S(1)} %get-tuple-element.38.refs_1_, bf16[1024,256]{1,0:T(8,128)(2,1)S(1)} %collective-permute-done.6.refs_2_, ...), custom_call_target="tpu_custom_call" | custom-call | flops 1073741824 | bytes 4194304 | tf_op jit(solution)/shard_map/input_block/pallas_call | solution.py:588
  122.8 12.1 %collective-permute-done.10 = bf16[1024,512]{1,0:T(8,128)(2,1)S(1)} collective-permute-done((bf16[1024,512]{1,0:T(8,128)(2,1)S(1)}, bf16[1024,512]{1,0:T(8,128)(2,1)S(1)}, u32[]{:S(2)}, u32[]{:S(2)}) %collective-permute-start.10) | collective-permute-done | bytes 1048608 | tf_op jit(solution)/shard_map/ppermute | solution.py:31
  134.9 1.3 add_convert_fusion
  (88 shorter events, 2.0 us)
Async XLA Ops:
  0.6 12.8 %copy-start.9 = (f32[31,256]{1,0:T(8,128)S(1)}, f32[31,256]{1,0:T(8,128)}, u32[]{:S(2)}) copy-start(f32[31,256]{1,0:T(8,128)} %taps_ref.7) | copy-start | bytes 95236
  6.5 10.7 %collective-permute-start.1 = (f32[64,256]{1,0:T(8,128)S(1)}, f32[64,256]{1,0:T(8,128)S(1)}, u32[]{:S(2)}, u32[]{:S(2)}) collective-permute-start(f32[64,256]{1,0:T(8,128)S(1)} %pad_maximum_fusion.3), channel_id=1, source_target_pairs={{4,0},{8,4},{12,8},{16,12},{20,16},{24,20},{28,24},{5,1},{9,5},{13... | collective-permute-start | bytes 196616 | tf_op jit(solution)/shard_map/ppermute | solution.py:31
  7.8 9.4 %collective-permute-start = (bf16[32,256]{1,0:T(8,128)(2,1)S(1)}, bf16[32,256]{1,0:T(8,128)(2,1)S(1)}, u32[]{:S(2)}, u32[]{:S(2)}) collective-permute-start(bf16[32,256]{1,0:T(8,128)(2,1)S(1)} %get-tuple-element.69.tail_ref), channel_id=1, source_target_pairs={{0,4},{4,8},{8,12},{12,16},{16,20},{20,24},{24,28},{1,5},{5,9},{9,... | collective-permute-start | bytes 49160 | tf_op jit(solution)/shard_map/ppermute | solution.py:31
  13.4 7.7 %copy-start = (bf16[1024,2048]{1,0:T(8,128)(2,1)S(1)}, bf16[1024,2048]{1,0:T(8,128)(2,1)}, u32[]{:S(2)}) copy-start(bf16[1024,2048]{1,0:T(8,128)(2,1)} %right_ref.5) | copy-start | bytes 12582916
  17.9 1.2 collective-permute-start.2
  19.1 4.6 %collective-permute-start.3 = (f32[2,1152]{1,0:T(2,128)S(1)}, f32[2,1152]{1,0:T(2,128)S(1)}, u32[]{:S(2)}, u32[]{:S(2)}) collective-permute-start(f32[2,1152]{1,0:T(2,128)S(1)} %fusion.4), channel_id=1, source_target_pairs={{0,2},{1,3},{2,0},{3,1},{4,6},{5,7},{6,4},{7,5},{8,10},{9,11},{10,... | collective-permute-start | bytes 27656 | tf_op jit(solution)/shard_map/ppermute | solution.py:31
  21.2 1.2 copy-start.6
  22.4 1.4 %copy-start.12 = (f32[256]{0:T(256)S(1)}, f32[256]{0:T(256)}, u32[]{:S(2)}) copy-start(f32[256]{0:T(256)} %param.13) | copy-start | bytes 3076
  22.4 1.4 %copy-start.13 = (f32[256]{0:T(256)S(1)}, f32[256]{0:T(256)}, u32[]{:S(2)}) copy-start(f32[256]{0:T(256)} %param.14) | copy-start | bytes 3076
  25.6 5.5 %copy-start.7 = (bf16[1024,256]{1,0:T(8,128)(2,1)S(1)}, bf16[1024,256]{1,0:T(8,128)(2,1)}, u32[]{:S(2)}) copy-start(bf16[1024,256]{1,0:T(8,128)(2,1)} %get-tuple-element.35.v_hbm) | copy-start | bytes 1572868
  25.6 5.5 %copy-start.8 = (bf16[1024,256]{1,0:T(8,128)(2,1)S(1)}, bf16[1024,256]{1,0:T(8,128)(2,1)}, u32[]{:S(2)}) copy-start(bf16[1024,256]{1,0:T(8,128)(2,1)} %get-tuple-element.36.s_hbm) | copy-start | bytes 1572868
  26.1 1.2 collective-permute-start.4
  27.3 3.7 %collective-permute-start.5 = (f32[2,1152]{1,0:T(2,128)S(1)}, f32[2,1152]{1,0:T(2,128)S(1)}, u32[]{:S(2)}, u32[]{:S(2)}) collective-permute-start(f32[2,1152]{1,0:T(2,128)S(1)} %fusion.5), channel_id=1, source_target_pairs={{0,2},{1,3},{2,0},{3,1},{4,6},{5,7},{6,4},{7,5},{8,10},{9,11},{10,... | collective-permute-start | bytes 27656 | tf_op jit(solution)/shard_map/ppermute | solution.py:31
  31.1 10.9 %copy-start.2 = (bf16[1024,2048]{1,0:T(8,128)(2,1)S(1)}, bf16[1024,2048]{1,0:T(8,128)(2,1)}, u32[]{:S(2)}) copy-start(bf16[1024,2048]{1,0:T(8,128)(2,1)} %right_ref.4) | copy-start | bytes 12582916
  41.2 0.8 copy-start.10
  42.1 5.4 %copy-start.1 = (bf16[1024,2048]{1,0:T(8,128)(2,1)S(1)}, bf16[1024,2048]{1,0:T(8,128)(2,1)}, u32[]{:S(2)}) copy-start(bf16[1024,2048]{1,0:T(8,128)(2,1)} %right_ref.5) | copy-start | bytes 12582916
  44.9 27.1 %collective-permute-start.15 = (bf16[1072,256]{1,0:T(8,128)(2,1)}, bf16[1072,256]{1,0:T(8,128)(2,1)}, u32[]{:S(2)}, u32[]{:S(2)}) collective-permute-start(bf16[1072,256]{1,0:T(8,128)(2,1)} %get-tuple-element.47), channel_id=1, source_target_pairs={{0,4},{4,0},{8,12},{12,8},{16,20},{20,16},{24,28},{28,24},{1,5},{5... | collective-permute-start | bytes 1646600 | tf_op jit(solution)/shard_map/ppermute | solution.py:31
  47.5 8.2 %copy-start.4 = (bf16[2048,256]{1,0:T(8,128)(2,1)S(1)}, bf16[2048,256]{1,0:T(8,128)(2,1)}, u32[]{:S(2)}) copy-start(bf16[2048,256]{1,0:T(8,128)(2,1)} %refs_4_.3) | copy-start | bytes 3145732
  50.1 11.4 %collective-permute-start.19 = (bf16[512,256]{1,0:T(8,128)(2,1)}, bf16[512,256]{1,0:T(8,128)(2,1)}, u32[]{:S(2)}, u32[]{:S(2)}) collective-permute-start(bf16[512,256]{1,0:T(8,128)(2,1)} %get-tuple-element.52), channel_id=1, source_target_pairs={{0,8},{4,12},{8,16},{12,20},{16,24},{20,28},{24,0},{28,4},{1,9},{5... | collective-permute-start | bytes 786440 | tf_op jit(solution)/shard_map/ppermute | solution.py:31
  51.8 18.9 %collective-permute-start.20 = (bf16[512,256]{1,0:T(8,128)(2,1)}, bf16[512,256]{1,0:T(8,128)(2,1)}, u32[]{:S(2)}, u32[]{:S(2)}) collective-permute-start(bf16[512,256]{1,0:T(8,128)(2,1)} %get-tuple-element.53), channel_id=1, source_target_pairs={{0,16},{4,20},{8,24},{12,28},{16,0},{20,4},{24,8},{28,12},{1,17},{... | collective-permute-start | bytes 786440 | tf_op jit(solution)/shard_map/ppermute | solution.py:31
  52.9 18.1 %collective-permute-start.21 = (bf16[512,256]{1,0:T(8,128)(2,1)S(1)}, bf16[512,256]{1,0:T(8,128)(2,1)}, u32[]{:S(2)}, u32[]{:S(2)}) collective-permute-start(bf16[512,256]{1,0:T(8,128)(2,1)S(1)} %get-tuple-element.54), channel_id=1, source_target_pairs={{0,24},{4,28},{8,0},{12,4},{16,8},{20,12},{24,16},{28,20},{1,25},{... | collective-permute-start | bytes 786440 | tf_op jit(solution)/shard_map/ppermute | solution.py:31
  55.7 45.5 %collective-permute-start.8 = (bf16[2048,256]{1,0:T(8,128)(2,1)S(1)}, bf16[2048,256]{1,0:T(8,128)(2,1)S(1)}, u32[]{:S(2)}, u32[]{:S(2)}) collective-permute-start(bf16[2048,256]{1,0:T(8,128)(2,1)S(1)} %copy-done.4), channel_id=1, source_target_pairs={{0,1},{1,0},{2,3},{3,2},{4,5},{5,4},{6,7},{7,6},{8,9},{9,8},{10,11... | collective-permute-start | bytes 3145736 | tf_op jit(solution)/shard_map/ppermute | solution.py:31
  55.7 2.2 %copy-start.3 = (bf16[1024,2048]{1,0:T(8,128)(2,1)S(1)}, bf16[1024,2048]{1,0:T(8,128)(2,1)}, u32[]{:S(2)}) copy-start(bf16[1024,2048]{1,0:T(8,128)(2,1)} %right_ref.4) | copy-start | bytes 12582916
  57.9 1.0 copy-start.11
  58.9 2.7 %copy-start.5 = (bf16[2048,256]{1,0:T(8,128)(2,1)S(1)}, bf16[2048,256]{1,0:T(8,128)(2,1)}, u32[]{:S(2)}) copy-start(bf16[2048,256]{1,0:T(8,128)(2,1)} %refs_5_.3) | copy-start | bytes 3145732
  58.9 12.0 %copy-start.16 = (bf16[2,256,256]{2,1,0:T(8,128)(2,1)S(1)}, bf16[2,256,256]{2,1,0:T(8,128)(2,1)}, u32[]{:S(2)}) copy-start(bf16[2,256,256]{2,1,0:T(8,128)(2,1)} %get-tuple-element.51) | copy-start | bytes 786436
  61.3 13.3 %copy-start.14 = (bf16[4,256,256]{2,1,0:T(8,128)(2,1)S(1)}, bf16[4,256,256]{2,1,0:T(8,128)(2,1)}, u32[]{:S(2)}) copy-start(bf16[4,256,256]{2,1,0:T(8,128)(2,1)} %get-tuple-element.46) | copy-start | bytes 1572868
  61.6 42.0 %collective-permute-start.9 = (bf16[2048,256]{1,0:T(8,128)(2,1)S(1)}, bf16[2048,256]{1,0:T(8,128)(2,1)S(1)}, u32[]{:S(2)}, u32[]{:S(2)}) collective-permute-start(bf16[2048,256]{1,0:T(8,128)(2,1)S(1)} %copy-done.5), channel_id=1, source_target_pairs={{0,1},{1,0},{2,3},{3,2},{4,5},{5,4},{6,7},{7,6},{8,9},{9,8},{10,11... | collective-permute-start | bytes 3145736 | tf_op jit(solution)/shard_map/ppermute | solution.py:31
  70.6 16.6 %collective-permute-start.11 = (bf16[1024,256]{1,0:T(8,128)(2,1)S(1)}, bf16[1024,256]{1,0:T(8,128)(2,1)S(1)}, u32[]{:S(2)}, u32[]{:S(2)}) collective-permute-start(bf16[1024,256]{1,0:T(8,128)(2,1)S(1)} %get-tuple-element.41), channel_id=1, source_target_pairs={{0,4},{4,0},{8,12},{12,8},{16,20},{20,16},{24,28},{28,24},{1,5},{5... | collective-permute-start | bytes 1572872 | tf_op jit(solution)/shard_map/ppermute | solution.py:31
  70.9 26.7 %collective-permute-start.7 = (bf16[1024,256]{1,0:T(8,128)(2,1)S(1)}, bf16[1024,256]{1,0:T(8,128)(2,1)S(1)}, u32[]{:S(2)}, u32[]{:S(2)}) collective-permute-start(bf16[1024,256]{1,0:T(8,128)(2,1)S(1)} %get-tuple-element.38.refs_1_), channel_id=1, source_target_pairs={{0,1},{1,0},{2,3},{3,2},{4,5},{5,4},{6,7},{7,6},{8,9},{9,8},{10,11... | collective-permute-start | bytes 1572872 | tf_op jit(solution)/shard_map/ppermute | solution.py:31
  72.1 15.1 %collective-permute-start.22 = (bf16[256,256]{1,0:T(8,128)(2,1)S(1)}, bf16[256,256]{1,0:T(8,128)(2,1)S(1)}, u32[]{:S(2)}, u32[]{:S(2)}) collective-permute-start(bf16[256,256]{1,0:T(8,128)(2,1)S(1)} %add_convert_fusion.1), channel_id=1, source_target_pairs={{0,4},{4,0},{8,12},{12,8},{16,20},{20,16},{24,28},{28,24},{1,5},{5... | collective-permute-start | bytes 393224 | tf_op jit(solution)/shard_map/ppermute | solution.py:31
  75.8 18.3 %copy-start.15 = (bf16[4,256,256]{2,1,0:T(8,128)(2,1)S(1)}, bf16[4,256,256]{2,1,0:T(8,128)(2,1)}, u32[]{:S(2)}) copy-start(bf16[4,256,256]{2,1,0:T(8,128)(2,1)} %get-tuple-element.40) | copy-start | bytes 1572868
  87.2 13.9 %collective-permute-start.6 = (bf16[1024,256]{1,0:T(8,128)(2,1)S(1)}, bf16[1024,256]{1,0:T(8,128)(2,1)S(1)}, u32[]{:S(2)}, u32[]{:S(2)}) collective-permute-start(bf16[1024,256]{1,0:T(8,128)(2,1)S(1)} %get-tuple-element.37.refs_0_), channel_id=1, source_target_pairs={{0,1},{1,0},{2,3},{3,2},{4,5},{5,4},{6,7},{7,6},{8,9},{9,8},{10,11... | collective-permute-start | bytes 1572872 | tf_op jit(solution)/shard_map/ppermute | solution.py:31
  87.2 9.1 %collective-permute-start.18 = (bf16[304,256]{1,0:T(8,128)(2,1)S(1)}, bf16[304,256]{1,0:T(8,128)(2,1)S(1)}, u32[]{:S(2)}, u32[]{:S(2)}) collective-permute-start(bf16[304,256]{1,0:T(8,128)(2,1)S(1)} %get-tuple-element.72), channel_id=1, source_target_pairs={{0,24},{4,28},{8,0},{12,4},{16,8},{20,12},{24,16},{28,20},{1,25},{... | collective-permute-start | bytes 466952 | tf_op jit(solution)/shard_map/ppermute | solution.py:31
  96.3 20.1 %collective-permute-start.17 = (bf16[304,256]{1,0:T(8,128)(2,1)S(1)}, bf16[304,256]{1,0:T(8,128)(2,1)S(1)}, u32[]{:S(2)}, u32[]{:S(2)}) collective-permute-start(bf16[304,256]{1,0:T(8,128)(2,1)S(1)} %get-tuple-element.73), channel_id=1, source_target_pairs={{0,16},{4,20},{8,24},{12,28},{16,0},{20,4},{24,8},{28,12},{1,17},{... | collective-permute-start | bytes 466952 | tf_op jit(solution)/shard_map/ppermute | solution.py:31
  97.6 19.9 %collective-permute-start.12 = (bf16[256,256]{1,0:T(8,128)(2,1)S(1)}, bf16[256,256]{1,0:T(8,128)(2,1)S(1)}, u32[]{:S(2)}, u32[]{:S(2)}) collective-permute-start(bf16[256,256]{1,0:T(8,128)(2,1)S(1)} %get-tuple-element.65), channel_id=1, source_target_pairs={{0,8},{4,12},{8,16},{12,20},{16,24},{20,28},{24,0},{28,4},{1,9},{5... | collective-permute-start | bytes 393224 | tf_op jit(solution)/shard_map/ppermute | solution.py:31
  101.1 18.0 %collective-permute-start.13 = (bf16[256,256]{1,0:T(8,128)(2,1)S(1)}, bf16[256,256]{1,0:T(8,128)(2,1)S(1)}, u32[]{:S(2)}, u32[]{:S(2)}) collective-permute-start(bf16[256,256]{1,0:T(8,128)(2,1)S(1)} %get-tuple-element.64), channel_id=1, source_target_pairs={{0,16},{4,20},{8,24},{12,28},{16,0},{20,4},{24,8},{28,12},{1,17},{... | collective-permute-start | bytes 393224 | tf_op jit(solution)/shard_map/ppermute | solution.py:31
  101.2 18.0 %collective-permute-start.14 = (bf16[256,256]{1,0:T(8,128)(2,1)S(1)}, bf16[256,256]{1,0:T(8,128)(2,1)S(1)}, u32[]{:S(2)}, u32[]{:S(2)}) collective-permute-start(bf16[256,256]{1,0:T(8,128)(2,1)S(1)} %get-tuple-element.63), channel_id=1, source_target_pairs={{0,24},{4,28},{8,0},{12,4},{16,8},{20,12},{24,16},{28,20},{1,25},{... | collective-permute-start | bytes 393224 | tf_op jit(solution)/shard_map/ppermute | solution.py:31
  103.6 13.9 %collective-permute-start.16 = (bf16[304,256]{1,0:T(8,128)(2,1)S(1)}, bf16[304,256]{1,0:T(8,128)(2,1)S(1)}, u32[]{:S(2)}, u32[]{:S(2)}) collective-permute-start(bf16[304,256]{1,0:T(8,128)(2,1)S(1)} %get-tuple-element.74), channel_id=1, source_target_pairs={{0,8},{4,12},{8,16},{12,20},{16,24},{20,28},{24,0},{28,4},{1,9},{5... | collective-permute-start | bytes 466952 | tf_op jit(solution)/shard_map/ppermute | solution.py:31
  116.4 18.5 %collective-permute-start.10 = (bf16[1024,512]{1,0:T(8,128)(2,1)S(1)}, bf16[1024,512]{1,0:T(8,128)(2,1)S(1)}, u32[]{:S(2)}, u32[]{:S(2)}) collective-permute-start(bf16[1024,512]{1,0:T(8,128)(2,1)S(1)} %input_block.3), channel_id=1, source_target_pairs={{0,2},{1,3},{2,0},{3,1},{4,6},{5,7},{6,4},{7,5},{8,10},{9,11},{10,... | collective-permute-start | bytes 3145736 | tf_op jit(solution)/shard_map/ppermute | solution.py:31
